TPU v7x, 512 devices: a whole 4x4x16 slice. The times are simulated.
512 devices in a mesh: sp: 64 (over z, y), tp: 8 (over x, core).
Axes of the slice: x: 4, y: 4, z: 16, core: 2. Of those that a mesh axis runs over, the one named last changes fastest.
Arguments:
- residual: bfloat16 [16384, 2048], P('sp'), may hold values from -6 to 6
- queries: bfloat16 [16384, 1024], P('sp', 'tp'), may hold values from -6 to 6
- forget_gate_logits: bfloat16 [16384, 1024], P('sp', 'tp'), may hold values from -5 to 5
- projected_values: bfloat16 [16384, 1024], P('sp', 'tp'), may hold values from -6 to 6
- output_gate_logits: bfloat16 [16384, 1024], P('sp', 'tp'), may hold values from -6 to 6
- lower_bound_margin: float32 [1024], P('tp'), may hold values from 6.1035156e-05 to 0.08
- extra_forget_logs: float32 [16384, 1024], P('sp', 'tp'), may hold values from -0.7 to 0
- per_head_norm_gain: float32 [128], replicated, may hold values from 0.1 to 1.9
- output_weight: bfloat16 [1024, 2048], P('tp'), may hold values from -0.1875 to 0.1875
- feedforward_norm_gain: float32 [2048], replicated, may hold values from 0.1 to 1.9
- gate_weight: bfloat16 [2048, 5632], P('sp', 'tp'), may hold values from -0.125 to 0.125
- up_weight: bfloat16 [2048, 5632], P('sp', 'tp'), may hold values from -0.125 to 0.125
- down_weight: bfloat16 [5632, 2048], P('tp', 'sp'), may hold values from -0.078125 to 0.078125
Outputs:
- layer_out: bfloat16 [16384, 2048], P('sp')
All inputs are finite; a program needn't handle non-finite values.
Results may differ from a plain program's by a relative error of at most 0.015.
Values may be sent and summed in bfloat16 or wider, within the bound.
No kernel may reach another device: no remote copies, remote signals or barrier semaphores. Data moves between devices by JAX's collectives and lax.ppermute only.
A program may use at most 64 MiB of HBM per device.

v0:
```python
import jax
import jax.numpy as jnp
from jax import lax
from jax.sharding import Mesh
from jax.sharding import PartitionSpec as P

HD = 128
BLOCK = 64
SP = ("sp_0", "sp_1")


eps = 1e-06


def gather_turned(arrays, axis, dims):
    turned = [jnp.moveaxis(a, dim, 0) for a, dim in zip(arrays, dims)]
    widths = [t[0].size for t in turned]
    both = jnp.concatenate([t.reshape(-1, w) for t, w in zip(turned, widths)], axis=1)
    filled = lax.all_gather(both, axis, axis=0, tiled=True)
    parts = jnp.split(filled, [sum(widths[:k]) for k in range(1, len(widths))], axis=1)
    return tuple(
        (
            jnp.moveaxis(b.reshape(-1, *t.shape[1:]), 0, dim)
            for b, t, dim in zip(parts, turned, dims)
        )
    )


def nothing_yet(value, identity):
    return jax.tree.map(
        lambda a, e: jnp.broadcast_to(jnp.asarray(e, a.dtype), a.shape), value, identity
    )


def gathered_once(value, axis):
    leaves = jax.tree.leaves(value)
    order = sorted(range(len(leaves)), key=lambda k: -leaves[k].size)
    width = (1, *leaves[order[0]].shape)[-1]
    lines = [
        jnp.pad(leaves[k].reshape(-1), (0, -leaves[k].size % width)).reshape(-1, width)
        for k in order
    ]
    both, at, found = (lax.all_gather(jnp.concatenate(lines), axis), 0, {})
    for k, line in zip(order, lines):
        section = both[:, at : at + len(line)].reshape(len(both), -1)
        found[k] = section[:, : leaves[k].size].reshape(-1, *leaves[k].shape)
        at += len(line)
    numbers = iter(range(len(leaves)))
    return jax.tree.map(lambda _: found[next(numbers)], value)


def carried_in_2(value, axes, combine, identity):
    before = start = nothing_yet(value, identity)
    running = value
    for axis in reversed(axes):
        length, place = (lax.axis_size(axis), lax.axis_index(axis))
        pieces = gathered_once(
            jax.tree.map(
                lambda part, kind: part.astype(kind), running, (jnp.bfloat16, jnp.bfloat16)
            ),
            axis,
        )
        inside, running = (start, start)
        for k in range(length):
            passed = k < place
            running = combine(
                running, jax.tree.map(lambda part, own: part[k].astype(own.dtype), pieces, value)
            )
            inside = jax.tree.map(lambda new, old: jnp.where(passed, new, old), running, inside)
        before = combine(inside, before)
    return before


def cut_along(value, dim, length):
    shape = value.shape
    parts = value.reshape(*shape[:dim], length, shape[dim] // length, *shape[dim + 1 :])
    return jnp.moveaxis(parts, dim, 0)


def sum_at_owner(value, axis, dim):
    parts = cut_along(value, dim, lax.axis_size(axis))
    arrived = lax.all_to_all(parts, axis, split_axis=0, concat_axis=0, tiled=True)
    return arrived.astype(jnp.float32).sum(axis=0)


def copy_for_each(value, axis):
    copies = jnp.broadcast_to(value, (lax.axis_size(axis), *value.shape))
    return lax.all_to_all(copies, axis, split_axis=0, concat_axis=0, tiled=True)


def laid_out(parts, dim):
    shape = list(parts.shape[1:])
    shape[dim] *= parts.shape[0]
    return jnp.moveaxis(parts, 0, dim).reshape(shape)


def collect(value, axis, dim):
    parts = copy_for_each(value, axis)
    return laid_out(parts, dim)


def block_update(carried_in, inputs):
    recurrent_state, offset = carried_in
    queries, state_increment, value_rows, retain_log_factor = inputs
    running_state = jnp.cumsum(retain_log_factor, axis=1)
    causal = jnp.tril(
        jnp.ones((retain_log_factor.shape[1], retain_log_factor.shape[1]), dtype=bool)
    )
    carried_over_state = jnp.einsum(
        "uqw,uwa->uqa", queries * jnp.exp(running_state), recurrent_state
    )
    spread = running_state[:, :, None, :] - running_state[:, None, :, :]
    weights = jnp.exp(jnp.where(causal[None, :, :, None], spread, -jnp.inf))
    scores = jnp.einsum("htk,htsk,hsk->hts", queries, weights, state_increment)
    output_rows = carried_over_state + jnp.einsum("hts,hsv->htv", scores, value_rows)
    final_state = running_state[:, -1:, :]
    updated_state = jnp.exp(final_state[:, 0, :])[:, :, None] * recurrent_state + jnp.einsum(
        "erb,erc->ebc", state_increment * jnp.exp(final_state - running_state), value_rows
    )
    rescaled_state = queries * jnp.exp(running_state + offset[:, None, :])
    return ((updated_state, offset + final_state[:, 0, :]), (output_rows, rescaled_state))


def join_states(earlier, later):
    earlier_sum, earlier_memory = earlier
    later_sum, later_memory = later
    return (earlier_sum + later_sum, jnp.exp(later_sum)[:, :, None] * earlier_memory + later_memory)


def local(
    residual,
    queries,
    forget_gate_logits,
    projected_values,
    output_gate_logits,
    lower_bound_margin,
    extra_forget_logs,
    per_head_norm_gain,
    output_weight,
    feedforward_norm_gain,
    gate_weight,
    up_weight,
    down_weight,
):
    gate_full, up_full, down_full = gather_turned(
        (gate_weight, up_weight, down_weight), SP, (0, 0, 1)
    )
    length = queries.shape[0]
    head_count = queries.shape[1] // HD
    state_increment = lower_bound_margin * jax.nn.sigmoid(-forget_gate_logits.astype(jnp.float32))
    retain_log_factor = jnp.log1p(-state_increment) + extra_forget_logs

    def to_blocks(source):
        return source.reshape(length // BLOCK, BLOCK, head_count, HD).transpose(0, 2, 1, 3)

    initial = (
        jnp.zeros((head_count, HD, HD), jnp.float32),
        jnp.zeros((head_count, HD), jnp.float32),
    )
    block_inputs = (
        to_blocks(queries.astype(jnp.float32)),
        to_blocks(state_increment),
        to_blocks(projected_values.astype(jnp.float32)),
        to_blocks(retain_log_factor),
    )
    (recurrent_state, decay_sum), (output_rows, rescaled_state) = lax.scan(
        block_update, initial, block_inputs
    )
    identity = (jnp.zeros_like(decay_sum), jnp.zeros_like(recurrent_state))
    incoming_state = carried_in_2((decay_sum, recurrent_state), SP, join_states, identity)[1]
    output_rows = output_rows + jnp.einsum("sjey,jyx->sjex", rescaled_state, incoming_state)
    mixed = output_rows.transpose(0, 2, 1, 3).reshape(length, head_count, HD)
    normed_heads = (
        mixed
        * lax.rsqrt(jnp.mean(mixed * mixed, axis=-1, keepdims=True) + eps)
        * per_head_norm_gain
    )
    gating = jax.nn.silu(output_gate_logits.astype(jnp.float32)).reshape(length, head_count, HD)
    gated = (normed_heads * gating).reshape(length, head_count * HD).astype(jnp.bfloat16)
    row_count = residual.shape[0] // lax.axis_size("tp")
    own_rows = lax.dynamic_slice_in_dim(residual, lax.axis_index("tp") * row_count, row_count, 0)
    rows_here = gated
    projected = sum_at_owner(
        jnp.dot(rows_here, output_weight, preferred_element_type=jnp.float32).astype(jnp.bfloat16),
        "tp",
        0,
    )
    after_mixer = (own_rows.astype(jnp.float32) + projected).astype(jnp.bfloat16)
    widened = after_mixer.astype(jnp.float32)
    normed = (
        widened
        * lax.rsqrt(jnp.mean(widened * widened, axis=-1, keepdims=True) + eps)
        * feedforward_norm_gain
    ).astype(jnp.bfloat16)
    row_piece = collect(normed, "tp", 0)
    gate_part = jnp.dot(row_piece, gate_full, preferred_element_type=jnp.float32)
    up_part = jnp.dot(row_piece, up_full, preferred_element_type=jnp.float32)
    hidden = (jax.nn.silu(gate_part) * up_part).astype(jnp.bfloat16)
    rows_here = hidden
    ffn_sum = sum_at_owner(
        jnp.dot(rows_here, down_full, preferred_element_type=jnp.float32).astype(jnp.bfloat16),
        "tp",
        0,
    )
    finished = (after_mixer.astype(jnp.float32) + 0.5 * ffn_sum).astype(jnp.bfloat16)
    return collect(finished, "tp", 0)


def solution(mesh):
    finer = Mesh(mesh.devices.reshape(16, 4, mesh.shape["tp"]), ("sp_0", "sp_1", "tp"))
    placed = (
        P(SP, None),
        P(SP, "tp"),
        P(SP, "tp"),
        P(SP, "tp"),
        P(SP, "tp"),
        P("tp"),
        P(SP, "tp"),
        P(),
        P("tp", None),
        P(),
        P(SP, "tp"),
        P(SP, "tp"),
        P("tp", SP),
    )
    return jax.shard_map(local, mesh=finer, in_specs=placed, out_specs=P(SP, None), check_vma=False)
```

profile of v0, /device:TPU:1, one launch (start us, length us, event | category | flops | bytes accessed | tf_op | source)
XLA Modules:
  0.0 229.9 jit_solution(110097667597470803)
XLA Ops:
  6.5 1.7 concatenate.11
  8.3 0.9 convert.7
  9.2 1.1 divide_multiply_fusion
  10.2 6.6 %while.17 = (s32[]{:T(128)}, f32[1,128,128]{2,1,0:T(8,128)S(1)}, f32[1,128]{1,0:T(1,128)S(1)}, f32[4,1,64,128]{3,2,1,0:T(8,128)S(1)}, bf16[4,1,64,128]{3,2,1,0:T...) while((s32[]{:T(128)}, f32[1,128,128]{2,1,0:T(8,128)S(1)}, ...), condition=%wide.region_2.3_spmd.clone, body=%wide.region_0.2_spmd.clone.sunk | while | flops 8499459 | bytes 1212596 | solution.py:166
  10.5 0.9 fusion.282
  11.6 0.2 fusion.278
  12.1 0.9 fusion.282
  13.2 0.2 fusion.278
  13.8 0.9 fusion.282
  15.4 0.9 fusion.282
  16.9 10.5 %all-gather.2 = bf16[4,129,128]{2,1,0:T(8,128)(2,1)S(1)} all-gather(bf16[1,129,128]{2,1,0:T(8,128)(2,1)S(1)} %maximum_bitcast_fusion), channel_id=2, replica_groups=mesh['sp_0'=16,'sp_1'=4,'tp'=8] {'sp_1'}, dimensions={0}, use_global_device_ids=true | all-gather | bytes 165120 | tf_op jit(solution)/shard_map/all_gather | solution.py:43
  27.5 33.0 %all-gather.3 = bf16[16,129,128]{2,1,0:T(8,128)(2,1)S(1)} all-gather(bf16[1,129,128]{2,1,0:T(8,128)(2,1)S(1)} %maximum_bitcast_fusion.1), channel_id=3, replica_groups=mesh['sp_0'=16,'sp_1'=4,'tp'=8] {'sp_0'}, dimensions={0}, use_global_device_ids=true | all-gather | bytes 561408 | tf_op jit(solution)/shard_map/all_gather | solution.py:43
  60.6 0.7 multiply_reduce_fusion
  61.5 1.4 convolution_convert_fusion
  62.9 14.1 %all-to-all-start = ((bf16[8,32,2048]{2,1,0:T(8,128)(2,1)}), bf16[8,32,2048]{2,1,0:T(8,128)(2,1)S(1)}, u32[]{:S(2)}, u32[]{:S(2)}) async-start(bf16[8,32,2048]{2,1,0:T(8,128)(2,1)} %bitcast.37), calls=%async_computation | async-start | bytes 2097152 | tf_op jit(solution)/shard_map/all_to_all | solution.py:82
  77.1 15.0 %all-to-all-done = bf16[8,32,2048]{2,1,0:T(8,128)(2,1)S(1)} async-done(((bf16[8,32,2048]{2,1,0:T(8,128)(2,1)}), bf16[8,32,2048]{2,1,0:T(8,128)(2,1)S(1)}, u32[]{:S(2)}, u32[]{:S(2)}) %all-to-all-start) | async-done | bytes 1048608 | tf_op jit(solution)/shard_map/all_to_all | solution.py:82
  92.2 1.1 fusion.65
  93.5 18.4 %all_to_all.20 = bf16[8,32,2048]{2,1,0:T(8,128)(2,1)S(1)} all-to-all(bf16[8,32,2048]{2,1,0:T(8,128)(2,1)S(1)} %broadcast_in_dim.28), channel_id=1, replica_groups=mesh['sp_0'=16,'sp_1'=4,'tp'=8] {'tp'}, dimensions={0} | all-to-all | bytes 2097152 | tf_op jit(solution)/shard_map/all_to_all | solution.py:88
  111.9 53.7 %all-gather.6.cloned.1.call-done = bf16[2048,2112]{1,0:T(8,128)(2,1)} async-done(((bf16[32,2112]{1,0:T(8,128)(2,1)}), bf16[2048,2112]{1,0:T(8,128)(2,1)}) %all-gather.6.cloned.1.call-update) | async-done | bytes 8650768 | tf_op jit(solution)/shard_map/all_gather | solution.py:19
  165.5 3.2 %fusion.45 = f32[256,704]{0,1:T(8,128)S(1)} fusion(bf16[256,2048]{1,0:T(8,128)(2,1)S(1)} %bitcast.209, bf16[2048,2112]{1,0:T(8,128)(2,1)} %all-gather.6.cloned.1.call-done), kind=kOutput, calls=%fused_computation.55 | convolution fusion | flops 738197504 | bytes 4915200 | tf_op jit(solution)/shard_map/dot_general | solution.py:196
  168.8 7.4 %fusion.47 = bf16[256,2048]{1,0:T(8,128)(2,1)S(1)} fusion(bf16[2048,2112]{1,0:T(8,128)(2,1)} %all-gather.6.cloned.1.call-done, bf16[256,2048]{1,0:T(8,128)(2,1)S(1)} %bitcast.210, f32[256,704]{0,1:T(8,128)S(1)} %fusion.45), kind=kOutput, calls=%fused_computation.58 | convolution fusion | flops 1478000640 | bytes 9109504 | tf_op jit(solution)/shard_map/dot_general | solution.py:201
  176.1 27.3 %all_to_all.21 = bf16[8,32,2048]{2,1,0:T(8,128)(2,1)S(1)} all-to-all(bf16[8,32,2048]{2,1,0:T(8,128)(2,1)S(1)} %bitcast.211), channel_id=1, replica_groups=mesh['sp_0'=16,'sp_1'=4,'tp'=8] {'tp'}, dimensions={0} | all-to-all | bytes 2097152 | tf_op jit(solution)/shard_map/all_to_all | solution.py:82
  203.7 18.4 %all_to_all.22 = bf16[8,32,2048]{2,1,0:T(8,128)(2,1)S(1)} all-to-all(bf16[8,32,2048]{2,1,0:T(8,128)(2,1)S(1)} %broadcast_in_dim.29), channel_id=1, replica_groups=mesh['sp_0'=16,'sp_1'=4,'tp'=8] {'tp'}, dimensions={0} | all-to-all | bytes 2097152 | tf_op jit(solution)/shard_map/all_to_all | solution.py:88
  222.1 1.0 copy.36
  (81 shorter events, 3.3 us)
Async XLA Ops:
  6.5 55.0 %copy-start = (bf16[128,2048]{1,0:T(8,128)(2,1)S(1)}, bf16[128,2048]{1,0:T(8,128)(2,1)}, u32[]{:S(2)}) copy-start(bf16[128,2048]{1,0:T(8,128)(2,1)} %param.23) | copy-start | bytes 1572868
  6.5 159.0 %all-gather.6.cloned.1.call-start = ((), (), s32[]{:S(2)}) async-start(), calls=%async_computation.4 | async-start | bytes 9052160 | tf_op jit(solution)/shard_map/all_gather | solution.py:19
  10.2 1.3 copy-start.1
  11.9 1.3 copy-start.1
  13.5 1.3 copy-start.1
  15.2 1.3 copy-start.1
  16.8 44.6 %copy-start.2 = (bf16[256,128]{1,0:T(8,128)(2,1)S(1)}, bf16[256,128]{1,0:T(8,128)(2,1)}, u32[]{:S(2)}) copy-start(bf16[256,128]{1,0:T(8,128)(2,1)} %param.19) | copy-start | bytes 196612
  16.8 44.6 %copy-start.4 = (f32[128]{0:T(128)S(1)}, f32[128]{0:T(128)}, u32[]{:S(2)}) copy-start(f32[128]{0:T(128)} %param.22) | copy-start | bytes 1540
  61.3 31.9 %copy-start.3 = (f32[2048]{0:T(1024)S(1)}, f32[2048]{0:T(1024)}, u32[]{:S(2)}) copy-start(f32[2048]{0:T(1024)} %param.24) | copy-start | bytes 24580
  62.9 29.1 %all-to-all-start = ((bf16[8,32,2048]{2,1,0:T(8,128)(2,1)}), bf16[8,32,2048]{2,1,0:T(8,128)(2,1)S(1)}, u32[]{:S(2)}, u32[]{:S(2)}) async-start(bf16[8,32,2048]{2,1,0:T(8,128)(2,1)} %bitcast.37), calls=%async_computation | async-start | bytes 2097152 | tf_op jit(solution)/shard_map/all_to_all | solution.py:82
Sparse Core Ops, SparseCore 0:
  10.3 155.2 all-gather.5
where the time goes:
time: 230 us
  blocking collectives  108 us (47%)
  waiting for transfers between devices  68.6 us (30%)
  matrix products  18.4 us (8%)
  starting transfers between devices  14.1 us (6%)
  between operations  13.6 us (6%)
  other arithmetic  4.28 us (2%)
  local copies, waits for them, and re-layouts  3.11 us (1%)
    all_gather x1, waiting for transfers between devices, gather_turned(): filled = lax.all_gather(both, axis, axis=0, tiled=True)  53.7 us
    all_gather x2, blocking collectives, gathered_once(): both, at, found = (lax.all_gather(jnp.concatenate(lines), axis), 0, {})  43.5 us
    all_to_all x2, blocking collectives, copy_for_each(): return lax.all_to_all(copies, axis, split_axis=0, concat_axis=0, tiled=True)  36.8 us
    all_to_all x1, blocking collectives, sum_at_owner(): lax.all_to_all(parts, axis, split_axis=0, concat_axis=0, tiled=True)  27.3 us
    all_to_all x1, waiting for transfers between devices, sum_at_owner(): lax.all_to_all(parts, axis, split_axis=0, concat_axis=0, tiled=True)  15 us
    all_to_all x1, starting transfers between devices, sum_at_owner(): lax.all_to_all(parts, axis, split_axis=0, concat_axis=0, tiled=True)  14.1 us
    dot_general x1, matrix products, local(): jnp.dot(rows_here, down_full, preferred_element_type=jnp.float32)  7.35 us
  transfers between devices with their start and end apart: 2, of which 2 were waited for; matrix products, arithmetic and copies ran while one was open for 5% of the time, Pallas kernels for 0%

commit v1 on v0

--- a/solution.py
+++ b/solution.py
@@ -1,29 +1,19 @@
 import jax
 import jax.numpy as jnp
 from jax import lax
+from jax.experimental import pallas as pl
+from jax.experimental.pallas import tpu as pltpu
 from jax.sharding import Mesh
 from jax.sharding import PartitionSpec as P
 
 HD = 128
 BLOCK = 64
-SP = ("sp_0", "sp_1")
+SP = ("z", "y")
+TP = ("x", "c")
+SCALE = 2.0**18
 
 
 eps = 1e-06
-
-
-def gather_turned(arrays, axis, dims):
-    turned = [jnp.moveaxis(a, dim, 0) for a, dim in zip(arrays, dims)]
-    widths = [t[0].size for t in turned]
-    both = jnp.concatenate([t.reshape(-1, w) for t, w in zip(turned, widths)], axis=1)
-    filled = lax.all_gather(both, axis, axis=0, tiled=True)
-    parts = jnp.split(filled, [sum(widths[:k]) for k in range(1, len(widths))], axis=1)
-    return tuple(
-        (
-            jnp.moveaxis(b.reshape(-1, *t.shape[1:]), 0, dim)
-            for b, t, dim in zip(parts, turned, dims)
-        )
-    )
 
 
 def nothing_yet(value, identity):
@@ -71,34 +61,6 @@
     return before
 
 
-def cut_along(value, dim, length):
-    shape = value.shape
-    parts = value.reshape(*shape[:dim], length, shape[dim] // length, *shape[dim + 1 :])
-    return jnp.moveaxis(parts, dim, 0)
-
-
-def sum_at_owner(value, axis, dim):
-    parts = cut_along(value, dim, lax.axis_size(axis))
-    arrived = lax.all_to_all(parts, axis, split_axis=0, concat_axis=0, tiled=True)
-    return arrived.astype(jnp.float32).sum(axis=0)
-
-
-def copy_for_each(value, axis):
-    copies = jnp.broadcast_to(value, (lax.axis_size(axis), *value.shape))
-    return lax.all_to_all(copies, axis, split_axis=0, concat_axis=0, tiled=True)
-
-
-def laid_out(parts, dim):
-    shape = list(parts.shape[1:])
-    shape[dim] *= parts.shape[0]
-    return jnp.moveaxis(parts, 0, dim).reshape(shape)
-
-
-def collect(value, axis, dim):
-    parts = copy_for_each(value, axis)
-    return laid_out(parts, dim)
-
-
 def block_update(carried_in, inputs):
     recurrent_state, offset = carried_in
     queries, state_increment, value_rows, retain_log_factor = inputs
@@ -125,6 +87,73 @@
     earlier_sum, earlier_memory = earlier
     later_sum, later_memory = later
     return (earlier_sum + later_sum, jnp.exp(later_sum)[:, :, None] * earlier_memory + later_memory)
+
+
+def shifted(value, axis, step):
+    size = lax.axis_size(axis)
+    return lax.ppermute(value, axis, [(k, (k + step) % size) for k in range(size)])
+
+
+def ffn_kernel(y_ref, rows_ref, own_ref, down1_ref, up1_ref, low_ref, high_ref, out_ref, weights, hidden):
+    y = y_ref[0]
+    places = [lax.rem(y + k, 4) for k in range(4)]
+
+    def place(ref, at, z_from, z_to, offset):
+        @pl.loop(z_from, z_to)
+        def _(z):
+            start = pl.multiple_of(z * 128 + at * 32, 32)
+            source = pl.multiple_of((z - offset) * 32, 32)
+            weights[pl.ds(start, 32), :] = ref[pl.ds(source, 32), :]
+
+    place(own_ref, places[0], 0, 16, 0)
+    place(up1_ref, places[1], 0, 16, 0)
+    place(down1_ref, places[3], 0, 16, 0)
+    place(low_ref, places[2], 0, 8, 0)
+    place(high_ref, places[2], 8, 16, 8)
+    rows = rows_ref[...]
+
+    @pl.loop(0, 5)
+    def _(n):
+        gate_at = pl.multiple_of(n * 128, 128)
+        up_at = pl.multiple_of(640 + n * 128, 128)
+        gate = jnp.dot(rows, weights[:, pl.ds(gate_at, 128)], preferred_element_type=jnp.float32)
+        up = jnp.dot(rows, weights[:, pl.ds(up_at, 128)], preferred_element_type=jnp.float32)
+        hidden[:, pl.ds(gate_at, 128)] = (gate * jax.nn.sigmoid(gate) * up).astype(jnp.bfloat16)
+
+    both = jnp.dot(rows, weights[:, 1280:1408], preferred_element_type=jnp.float32)
+    gate, up = both[:, :64], both[:, 64:]
+    hidden[:, 640:704] = (gate * jax.nn.sigmoid(gate) * up).astype(jnp.bfloat16)
+    inner = hidden[:, :704]
+
+    @pl.loop(0, 8)
+    def _(n):
+        at = pl.multiple_of(n * 256, 256)
+        part = lax.dot_general(
+            inner,
+            weights[pl.ds(at, 256), 1408:2112],
+            (((1,), (1,)), ((), ())),
+            preferred_element_type=jnp.float32,
+        )
+        out_ref[:, pl.ds(at, 256)] = part.astype(jnp.bfloat16)
+
+
+def ffn(y, rows, own, down1, up1, low, high):
+    vmem = pl.BlockSpec(memory_space=pltpu.VMEM)
+    return pl.pallas_call(
+        ffn_kernel,
+        out_shape=jax.ShapeDtypeStruct((256, 2048), jnp.bfloat16),
+        in_specs=[pl.BlockSpec(memory_space=pltpu.SMEM)] + [vmem] * 6,
+        out_specs=vmem,
+        scratch_shapes=[
+            pltpu.VMEM((2048, 2176), jnp.bfloat16),
+            pltpu.VMEM((256, 768), jnp.bfloat16),
+        ],
+        compiler_params=pltpu.CompilerParams(vmem_limit_bytes=50 * 2**20),
+        cost_estimate=pl.CostEstimate(
+            flops=2 * 256 * 2048 * 2112, bytes_accessed=11 * 2**20, transcendentals=256 * 704
+        ),
+        name="ffn",
+    )(y, rows, own, down1, up1, low, high)
 
 
 def local(
@@ -142,9 +171,26 @@
     up_weight,
     down_weight,
 ):
-    gate_full, up_full, down_full = gather_turned(
-        (gate_weight, up_weight, down_weight), SP, (0, 0, 1)
-    )
+    packed = jnp.concatenate(
+        [
+            gate_weight[:, :640],
+            up_weight[:, :640],
+            gate_weight[:, 640:],
+            up_weight[:, 640:],
+            down_weight.T,
+            jnp.zeros((32, 64), jnp.bfloat16),
+        ],
+        axis=1,
+    )
+    packed = (packed.astype(jnp.float32) * SCALE).astype(jnp.float16)
+    along_z = lax.all_gather(packed, "z", axis=0, tiled=True)
+    own = (along_z.astype(jnp.float32) * (1.0 / SCALE)).astype(jnp.bfloat16)
+    out_copies = jnp.broadcast_to(output_weight, (8, *output_weight.shape))
+    out_full = lax.all_to_all(out_copies, TP, split_axis=0, concat_axis=0, tiled=True)
+    out_full = out_full.reshape(1024, 2048)
+    down1 = shifted(own, "y", 1)
+    up1 = shifted(own, "y", -1)
+
     length = queries.shape[0]
     head_count = queries.shape[1] // HD
     state_increment = lower_bound_margin * jax.nn.sigmoid(-forget_gate_logits.astype(jnp.float32))
@@ -168,6 +214,9 @@
     )
     identity = (jnp.zeros_like(decay_sum), jnp.zeros_like(recurrent_state))
     incoming_state = carried_in_2((decay_sum, recurrent_state), SP, join_states, identity)[1]
+    incoming_state, down1, up1 = lax.optimization_barrier((incoming_state, down1, up1))
+    low = shifted(down1[:256], "y", 1)
+    high = shifted(up1[256:], "y", -1)
     output_rows = output_rows + jnp.einsum("sjey,jyx->sjex", rescaled_state, incoming_state)
     mixed = output_rows.transpose(0, 2, 1, 3).reshape(length, head_count, HD)
     normed_heads = (
@@ -177,50 +226,52 @@
     )
     gating = jax.nn.silu(output_gate_logits.astype(jnp.float32)).reshape(length, head_count, HD)
     gated = (normed_heads * gating).reshape(length, head_count * HD).astype(jnp.bfloat16)
-    row_count = residual.shape[0] // lax.axis_size("tp")
-    own_rows = lax.dynamic_slice_in_dim(residual, lax.axis_index("tp") * row_count, row_count, 0)
-    rows_here = gated
-    projected = sum_at_owner(
-        jnp.dot(rows_here, output_weight, preferred_element_type=jnp.float32).astype(jnp.bfloat16),
-        "tp",
-        0,
-    )
-    after_mixer = (own_rows.astype(jnp.float32) + projected).astype(jnp.bfloat16)
+    gated_all = lax.all_gather(gated, TP)
+    gated_all = gated_all.transpose(1, 0, 2).reshape(256, 1024)
+    projected = jnp.dot(gated_all, out_full, preferred_element_type=jnp.float32)
+    after_mixer = (residual.astype(jnp.float32) + projected).astype(jnp.bfloat16)
     widened = after_mixer.astype(jnp.float32)
     normed = (
         widened
         * lax.rsqrt(jnp.mean(widened * widened, axis=-1, keepdims=True) + eps)
         * feedforward_norm_gain
     ).astype(jnp.bfloat16)
-    row_piece = collect(normed, "tp", 0)
-    gate_part = jnp.dot(row_piece, gate_full, preferred_element_type=jnp.float32)
-    up_part = jnp.dot(row_piece, up_full, preferred_element_type=jnp.float32)
-    hidden = (jax.nn.silu(gate_part) * up_part).astype(jnp.bfloat16)
-    rows_here = hidden
-    ffn_sum = sum_at_owner(
-        jnp.dot(rows_here, down_full, preferred_element_type=jnp.float32).astype(jnp.bfloat16),
-        "tp",
-        0,
-    )
-    finished = (after_mixer.astype(jnp.float32) + 0.5 * ffn_sum).astype(jnp.bfloat16)
-    return collect(finished, "tp", 0)
+    y = lax.axis_index("y").reshape(1)
+    part = ffn(y, normed, own, down1, up1, low, high)
+
+    core = lax.axis_index("c")
+    part = part.reshape(4, 2, 32, 2048)
+    theirs = lax.dynamic_index_in_dim(part, 1 - core, 1, keepdims=False)
+    mine = lax.dynamic_index_in_dim(part, core, 1, keepdims=False)
+    swapped = shifted(theirs, "c", 1)
+    pair = (mine.astype(jnp.float32) + swapped.astype(jnp.float32)).astype(jnp.bfloat16)
+    arrived = lax.all_to_all(pair, "x", split_axis=0, concat_axis=0, tiled=True)
+    ffn_sum = arrived.astype(jnp.float32).sum(axis=0)
+    place = lax.axis_index(TP) * 32
+    own_rows = lax.dynamic_slice_in_dim(after_mixer, place, 32, 0)
+    finished = (own_rows.astype(jnp.float32) + 0.5 * ffn_sum).astype(jnp.bfloat16)
+    along_x = lax.all_gather(finished, "x")
+    others = shifted(along_x, "c", 1)
+    first = jnp.where(core == 0, along_x, others)
+    second = jnp.where(core == 0, others, along_x)
+    return jnp.stack([first, second], axis=1).reshape(256, 2048)
 
 
 def solution(mesh):
-    finer = Mesh(mesh.devices.reshape(16, 4, mesh.shape["tp"]), ("sp_0", "sp_1", "tp"))
+    finer = Mesh(mesh.devices.reshape(16, 4, 4, 2), ("z", "y", "x", "c"))
     placed = (
         P(SP, None),
-        P(SP, "tp"),
-        P(SP, "tp"),
-        P(SP, "tp"),
-        P(SP, "tp"),
-        P("tp"),
-        P(SP, "tp"),
+        P(SP, TP),
+        P(SP, TP),
+        P(SP, TP),
+        P(SP, TP),
+        P(TP),
+        P(SP, TP),
         P(),
-        P("tp", None),
+        P(TP, None),
         P(),
-        P(SP, "tp"),
-        P(SP, "tp"),
-        P("tp", SP),
+        P(SP, TP),
+        P(SP, TP),
+        P(TP, SP),
     )
     return jax.shard_map(local, mesh=finer, in_specs=placed, out_specs=P(SP, None), check_vma=False)

time: 230 us -> 221 us (0.961)
  waiting for transfers between devices: 68.6 us -> 12.6 us
  blocking collectives: 108 us -> 135 us
  starting transfers between devices: 14.1 us -> 36.3 us
  between operations: 13.6 us -> 0.41 us
  Pallas kernels: 0 us -> 10.8 us
  local copies, waits for them, and re-layouts: 3.11 us -> 12.4 us
  matrix products: 18.4 us -> 9.83 us
    all_gather x0 -> x3, blocking collectives: none -> 83.9 us  [the longest x1 45.6 us: local(): along_z = lax.all_gather(packed, 'z', axis=0, tiled=True)]
    all_to_all x3 -> x0, blocking collectives: 64 us -> none  [the longest x2 36.8 us: copy_for_each(): return lax.all_to_all(copies, axis, split_axis=0, concat_axis=0, tiled=True)]
    all_gather x1 -> x0, waiting for transfers between devices: 53.7 us -> none  [gather_turned(): filled = lax.all_gather(both, axis, axis=0, tiled=True)]
    ppermute x0 -> x6, starting transfers between devices: none -> 21.4 us  [shifted(): lax.ppermute(value, axis, [(k, (k + step) % size) for k in range(size)])]
    pallas_call x0 -> x1, Pallas kernels: none -> 10.8 us  [ffn(): pl.pallas_call(ffn_kernel, out_shape=jax.ShapeDtypeStruct((256, 2048), jn...]
    dot_general x3 -> x1, matrix products: 12 us -> 3.91 us  [local(): projected = jnp.dot(gated_all, out_full, preferred_element_type=jnp.float32)]
    slice x0 -> x6, local copies, waits for them, and re-layouts: none -> 7.66 us  [the longest x1 2.36 us: local(): low = shifted(down1[:256], 'y', 1)]
    all_gather x2, blocking collectives: 43.5 us -> 50.7 us  [gathered_once(): both, at, found = (lax.all_gather(jnp.concatenate(lines), axis), 0, {})]
  transfers between devices with their start and end apart: 2 -> 8, of which waited for: 2 -> 3; matrix products, arithmetic and copies ran while one was open for 5% -> 9% of each run, Pallas kernels for 0% -> 0%
where the time goes in v1:
time: 221 us
  blocking collectives  135 us (61%)
  starting transfers between devices  36.3 us (16%)
  waiting for transfers between devices  12.6 us (6%)
  local copies, waits for them, and re-layouts  12.4 us (6%)
  Pallas kernels  10.8 us (5%)
  matrix products  9.83 us (4%)
  other arithmetic  3.38 us (2%)
    all_gather x2, blocking collectives, gathered_once(): both, at, found = (lax.all_gather(jnp.concatenate(lines), axis), 0, {})  50.7 us
    all_gather x1, blocking collectives, local(): along_z = lax.all_gather(packed, 'z', axis=0, tiled=True)  45.6 us
    all_gather x1, blocking collectives, local(): gated_all = lax.all_gather(gated, TP)  28.3 us
    ppermute x6, starting transfers between devices, shifted(): lax.ppermute(value, axis, [(k, (k + step) % size) for k in range(size)])  21.4 us
    all_to_all x1, starting transfers between devices, local(): lax.all_to_all(out_copies, TP, split_axis=0, concat_axis=0, tiled=True)  11.5 us
    pallas_call x1, Pallas kernels, ffn(): pl.pallas_call(ffn_kernel, out_shape=jax.ShapeDtypeStruct((256, 2048), jn...  10.8 us
    all_gather x1, blocking collectives, local(): along_x = lax.all_gather(finished, 'x')  10 us
    all_to_all x1, waiting for transfers between devices, local(): arrived = lax.all_to_all(pair, 'x', split_axis=0, concat_axis=0, tiled=True)  9.36 us
  transfers between devices with their start and end apart: 8, of which 3 were waited for; matrix products, arithmetic and copies ran while one was open for 9% of the time, Pallas kernels for 0%

profile of v1, /device:TPU:1, one launch (start us, length us, event | category | flops | bytes accessed | tf_op | source)
XLA Modules:
  0.0 220.5 jit_solution(11003901253664081359)
XLA Ops:
  3.9 45.6 %all-gather.7 = f16[512,2176]{1,0:T(8,128)(2,1)S(1)} all-gather(f16[32,2176]{1,0:T(8,128)(2,1)S(1)} %multiply_convert_fusion.1), channel_id=1, replica_groups=mesh['z'=16,'y'=4,'x'=4,'c'=2] {'z'}, dimensions={0}, use_global_device_ids=true | all-gather | bytes 2367488 | tf_op jit(solution)/shard_map/all_gather | solution.py:186
  49.9 3.2 %collective-permute-start = (bf16[512,2176]{1,0:T(8,128)(2,1)S(1)}, bf16[512,2176]{1,0:T(8,128)(2,1)}, u32[]{:S(2)}, u32[]{:S(2)}) collective-permute-start(bf16[512,2176]{1,0:T(8,128)(2,1)S(1)} %multiply_convert_fusion.own_ref), channel_id=1, source_target_pairs={{0,8},{8,16},{16,24},{24,0},{1,9},{9,17},{17,25},{25,1},{2,10},{10... | collective-permute-start | bytes 6684680 | tf_op jit(solution)/shard_map/ppermute | solution.py:94
  53.1 3.4 %collective-permute-start.1 = (bf16[512,2176]{1,0:T(8,128)(2,1)S(1)}, bf16[512,2176]{1,0:T(8,128)(2,1)}, u32[]{:S(2)}, u32[]{:S(2)}) collective-permute-start(bf16[512,2176]{1,0:T(8,128)(2,1)S(1)} %multiply_convert_fusion.own_ref), channel_id=1, source_target_pairs={{0,24},{8,0},{16,8},{24,16},{1,25},{9,1},{17,9},{25,17},{2,26},{10... | collective-permute-start | bytes 6684680 | tf_op jit(solution)/shard_map/ppermute | solution.py:94
  56.5 2.5 %broadcast_in_dim.29 = bf16[8,128,2048]{2,1,0:T(8,128)(2,1)} broadcast(bf16[128,2048]{1,0:T(8,128)(2,1)S(1)} %copy-done.1), dimensions={1,2} | broadcast | bytes 4718592 | tf_op jit(solution)/shard_map/broadcast_in_dim | solution.py:188
  59.0 11.5 %all-to-all-start = ((bf16[8,128,2048]{2,1,0:T(8,128)(2,1)}), bf16[8,128,2048]{2,1,0:T(8,128)(2,1)}, u32[]{:S(2)}, u32[]{:S(2)}) async-start(bf16[8,128,2048]{2,1,0:T(8,128)(2,1)} %broadcast_in_dim.29), calls=%async_computation | async-start | bytes 8388608 | tf_op jit(solution)/shard_map/all_to_all | solution.py:189
  70.7 6.6 %while.17 = (s32[]{:T(128)}, f32[1,128,128]{2,1,0:T(8,128)S(1)}, f32[1,128]{1,0:T(1,128)S(1)}, f32[4,1,64,128]{3,2,1,0:T(8,128)S(1)}, bf16[4,1,64,128]{3,2,1,0:T...) while((s32[]{:T(128)}, f32[1,128,128]{2,1,0:T(8,128)S(1)}, ...), condition=%wide.region_2.3_spmd.clone, body=%wide.region_0.2_spmd.clone.sunk | while | flops 8499459 | bytes 949905 | solution.py:212
  75.8 0.9 fusion.126
  77.4 27.1 %all-gather.4 = bf16[4,129,128]{2,1,0:T(8,128)(2,1)S(1)} all-gather(bf16[1,129,128]{2,1,0:T(8,128)(2,1)S(1)} %maximum_bitcast_fusion), channel_id=2, replica_groups=mesh['z'=16,'y'=4,'x'=4,'c'=2] {'y'}, dimensions={0}, use_global_device_ids=true | all-gather | bytes 165120 | tf_op jit(solution)/shard_map/all_gather | solution.py:33
  104.7 23.5 %all-gather.5 = bf16[16,129,128]{2,1,0:T(8,128)(2,1)S(1)} all-gather(bf16[1,129,128]{2,1,0:T(8,128)(2,1)S(1)} %maximum_bitcast_fusion.1), channel_id=3, replica_groups=mesh['z'=16,'y'=4,'x'=4,'c'=2] {'z'}, dimensions={0}, use_global_device_ids=true | all-gather | bytes 561408 | tf_op jit(solution)/shard_map/all_gather | solution.py:33
  129.1 2.4 %slice.249 = bf16[256,2176]{1,0:T(8,128)(2,1)} slice(bf16[512,2176]{1,0:T(8,128)(2,1)} %collective-permute-done.down1_ref), slice={[0:256], [0:2176]} | slice | bytes 2228224 | tf_op jit(solution)/shard_map/slice | solution.py:218
  131.5 3.2 %collective-permute-start.2 = (bf16[256,2176]{1,0:T(8,128)(2,1)}, bf16[256,2176]{1,0:T(8,128)(2,1)S(1)}, u32[]{:S(2)}, u32[]{:S(2)}) collective-permute-start(bf16[256,2176]{1,0:T(8,128)(2,1)} %slice.249), channel_id=1, source_target_pairs={{0,8},{8,16},{16,24},{24,0},{1,9},{9,17},{17,25},{25,1},{2,10},{10... | collective-permute-start | bytes 3342344 | tf_op jit(solution)/shard_map/ppermute | solution.py:94
  134.7 2.3 %slice.250 = bf16[256,2176]{1,0:T(8,128)(2,1)} slice(bf16[512,2176]{1,0:T(8,128)(2,1)} %collective-permute-done.1.up1_ref), slice={[256:512], [0:2176]} | slice | bytes 2228224 | tf_op jit(solution)/shard_map/slice | solution.py:219
  137.0 3.3 %collective-permute-start.3 = (bf16[256,2176]{1,0:T(8,128)(2,1)}, bf16[256,2176]{1,0:T(8,128)(2,1)}, u32[]{:S(2)}, u32[]{:S(2)}) collective-permute-start(bf16[256,2176]{1,0:T(8,128)(2,1)} %slice.250), channel_id=1, source_target_pairs={{0,24},{8,0},{16,8},{24,16},{1,25},{9,1},{17,9},{25,17},{2,26},{10... | collective-permute-start | bytes 3342344 | tf_op jit(solution)/shard_map/ppermute | solution.py:94
  140.4 28.3 %all-gather.2 = bf16[2048,128]{1,0:T(8,128)(2,1)S(1)} all-gather(bf16[256,128]{1,0:T(8,128)(2,1)S(1)} %fusion.54), channel_id=4, replica_groups=mesh['z'=16,'y'=4,'x'=4,'c'=2] {'x','c'}, dimensions={0}, use_global_device_ids=true | all-gather | bytes 589824 | tf_op jit(solution)/shard_map/all_gather | solution.py:229
  168.7 3.9 %fusion.43 = (f32[256]{0:T(256)S(1)}, bf16[256,2048]{1,0:T(8,128)(2,1)S(1)}) fusion(bf16[256,8,128]{2,0,1:T(8,128)(2,1)S(1)} %bitcast.230, bf16[8,128,2048]{2,1,0:T(8,128)(2,1)} %all-to-all-done, bf16[256,2048]{1,0:T(8,128)(2,1)} %param.15), kind=kOutput, calls=%fused_computation.57 | convolution fusion | flops 1076887296 | bytes 6816768 | tf_op jit(solution)/shard_map/dot_general | solution.py:231
  172.9 10.8 %ffn.1 = bf16[256,2048]{1,0:T(8,128)(2,1)S(1)} custom-call(s32[1]{0:T(128)} %bitcast.41.y_ref, bf16[256,2048]{1,0:T(8,128)(2,1)S(1)} %fusion.45.rows_ref, bf16[512,2176]{1,0:T(8,128)(2,1)} %copy-done, bf16[512,2176]{1,0:T(8,128)(2,1)} %collective-permute-done.down1_ref, bf16[512,2176]{1,0:T(8,128)(2,1)} %collective-permute-done.1.up1_ref, ...), custom_call_target="tpu_custom_call" | custom-call | flops 2214592512 | bytes 11534336 | tf_op jit(solution)/shard_map/ffn/pallas_call | solution.py:142
  183.8 2.1 collective-permute-start.4
  185.9 1.7 collective-permute-done.4
  188.5 3.5 %all-to-all-start.1 = ((bf16[4,32,2048]{2,1,0:T(8,128)(2,1)}), bf16[4,32,2048]{2,1,0:T(8,128)(2,1)S(1)}, u32[]{:S(2)}, u32[]{:S(2)}) async-start(bf16[4,32,2048]{2,1,0:T(8,128)(2,1)} %fusion.47), calls=%async_computation.1 | async-start | bytes 1048576 | tf_op jit(solution)/shard_map/all_to_all | solution.py:248
  192.0 9.4 %all-to-all-done.1 = bf16[4,32,2048]{2,1,0:T(8,128)(2,1)S(1)} async-done(((bf16[4,32,2048]{2,1,0:T(8,128)(2,1)}), bf16[4,32,2048]{2,1,0:T(8,128)(2,1)S(1)}, u32[]{:S(2)}, u32[]{:S(2)}) %all-to-all-start.1) | async-done | bytes 524320 | tf_op jit(solution)/shard_map/all_to_all | solution.py:248
  201.5 10.0 %all-gather.3 = bf16[128,2048]{1,0:T(8,128)(2,1)S(1)} all-gather(bf16[32,2048]{1,0:T(8,128)(2,1)S(1)} %add_convert_fusion), channel_id=5, replica_groups=mesh['z'=16,'y'=4,'x'=4,'c'=2] {'x'}, dimensions={0}, use_global_device_ids=true | all-gather | bytes 655360 | tf_op jit(solution)/shard_map/all_gather | solution.py:253
  211.5 6.2 %collective-permute-start.5 = (bf16[4,32,2048]{2,1,0:T(8,128)(2,1)S(1)}, bf16[4,32,2048]{2,1,0:T(8,128)(2,1)S(1)}, u32[]{:S(2)}, u32[]{:S(2)}) collective-permute-start(bf16[4,32,2048]{2,1,0:T(8,128)(2,1)S(1)} %bitcast.225), channel_id=1, source_target_pairs={{0,1},{1,0},{2,3},{3,2},{4,5},{5,4},{6,7},{7,6},{8,9},{9,8},{10,11... | collective-permute-start | bytes 1572872 | tf_op jit(solution)/shard_map/ppermute | solution.py:94
  217.8 1.5 collective-permute-done.5
  219.5 1.0 copy.17
  (106 shorter events, 12.5 us)
Async XLA Ops:
  49.5 7.0 %copy-start.1 = (bf16[128,2048]{1,0:T(8,128)(2,1)S(1)}, bf16[128,2048]{1,0:T(8,128)(2,1)}, u32[]{:S(2)}) copy-start(bf16[128,2048]{1,0:T(8,128)(2,1)} %param.23) | copy-start | bytes 1572868
  49.9 9.1 %copy-start = (bf16[512,2176]{1,0:T(8,128)(2,1)}, bf16[512,2176]{1,0:T(8,128)(2,1)S(1)}, u32[]{:S(2)}) copy-start(bf16[512,2176]{1,0:T(8,128)(2,1)S(1)} %multiply_convert_fusion.own_ref) | copy-start | bytes 6684676
  49.9 78.8 %collective-permute-start = (bf16[512,2176]{1,0:T(8,128)(2,1)S(1)}, bf16[512,2176]{1,0:T(8,128)(2,1)}, u32[]{:S(2)}, u32[]{:S(2)}) collective-permute-start(bf16[512,2176]{1,0:T(8,128)(2,1)S(1)} %multiply_convert_fusion.own_ref), channel_id=1, source_target_pairs={{0,8},{8,16},{16,24},{24,0},{1,9},{9,17},{17,25},{25,1},{2,10},{10... | collective-permute-start | bytes 6684680 | tf_op jit(solution)/shard_map/ppermute | solution.py:94
  53.1 75.6 %collective-permute-start.1 = (bf16[512,2176]{1,0:T(8,128)(2,1)S(1)}, bf16[512,2176]{1,0:T(8,128)(2,1)}, u32[]{:S(2)}, u32[]{:S(2)}) collective-permute-start(bf16[512,2176]{1,0:T(8,128)(2,1)S(1)} %multiply_convert_fusion.own_ref), channel_id=1, source_target_pairs={{0,24},{8,0},{16,8},{24,16},{1,25},{9,1},{17,9},{25,17},{2,26},{10... | collective-permute-start | bytes 6684680 | tf_op jit(solution)/shard_map/ppermute | solution.py:94
  59.0 11.5 %copy-start.4 = (bf16[256,128]{1,0:T(8,128)(2,1)S(1)}, bf16[256,128]{1,0:T(8,128)(2,1)}, u32[]{:S(2)}) copy-start(bf16[256,128]{1,0:T(8,128)(2,1)} %param.16) | copy-start | bytes 196612
  59.0 11.5 %copy-start.3 = (f32[256,128]{1,0:T(8,128)S(1)}, f32[256,128]{1,0:T(8,128)}, u32[]{:S(2)}) copy-start(f32[256,128]{1,0:T(8,128)} %param.21) | copy-start | bytes 393220
  59.0 11.6 %copy-start.5 = (bf16[256,128]{1,0:T(8,128)(2,1)S(1)}, bf16[256,128]{1,0:T(8,128)(2,1)}, u32[]{:S(2)}) copy-start(bf16[256,128]{1,0:T(8,128)(2,1)} %param.17) | copy-start | bytes 196612
  59.0 11.6 %copy-start.9 = (f32[128]{0:T(128)S(1)}, f32[128]{0:T(128)}, u32[]{:S(2)}) copy-start(f32[128]{0:T(128)} %param.20) | copy-start | bytes 1540
  59.0 11.7 %copy-start.2 = (bf16[256,128]{1,0:T(8,128)(2,1)S(1)}, bf16[256,128]{1,0:T(8,128)(2,1)}, u32[]{:S(2)}) copy-start(bf16[256,128]{1,0:T(8,128)(2,1)} %param.18) | copy-start | bytes 196612
  59.0 109.6 %all-to-all-start = ((bf16[8,128,2048]{2,1,0:T(8,128)(2,1)}), bf16[8,128,2048]{2,1,0:T(8,128)(2,1)}, u32[]{:S(2)}, u32[]{:S(2)}) async-start(bf16[8,128,2048]{2,1,0:T(8,128)(2,1)} %broadcast_in_dim.29), calls=%async_computation | async-start | bytes 8388608 | tf_op jit(solution)/shard_map/all_to_all | solution.py:189
  129.1 11.2 %copy-start.6 = (bf16[256,128]{1,0:T(8,128)(2,1)S(1)}, bf16[256,128]{1,0:T(8,128)(2,1)}, u32[]{:S(2)}) copy-start(bf16[256,128]{1,0:T(8,128)(2,1)} %param.19) | copy-start | bytes 196612
  129.1 11.2 %copy-start.8 = (f32[128]{0:T(128)S(1)}, f32[128]{0:T(128)}, u32[]{:S(2)}) copy-start(f32[128]{0:T(128)} %param.22) | copy-start | bytes 1540
  131.5 41.5 %collective-permute-start.2 = (bf16[256,2176]{1,0:T(8,128)(2,1)}, bf16[256,2176]{1,0:T(8,128)(2,1)S(1)}, u32[]{:S(2)}, u32[]{:S(2)}) collective-permute-start(bf16[256,2176]{1,0:T(8,128)(2,1)} %slice.249), channel_id=1, source_target_pairs={{0,8},{8,16},{16,24},{24,0},{1,9},{9,17},{17,25},{25,1},{2,10},{10... | collective-permute-start | bytes 3342344 | tf_op jit(solution)/shard_map/ppermute | solution.py:94
  137.0 35.9 %collective-permute-start.3 = (bf16[256,2176]{1,0:T(8,128)(2,1)}, bf16[256,2176]{1,0:T(8,128)(2,1)}, u32[]{:S(2)}, u32[]{:S(2)}) collective-permute-start(bf16[256,2176]{1,0:T(8,128)(2,1)} %slice.250), channel_id=1, source_target_pairs={{0,24},{8,0},{16,8},{24,16},{1,25},{9,1},{17,9},{25,17},{2,26},{10... | collective-permute-start | bytes 3342344 | tf_op jit(solution)/shard_map/ppermute | solution.py:94
  168.7 3.9 %copy-start.7 = (f32[2048]{0:T(1024)S(1)}, f32[2048]{0:T(1024)}, u32[]{:S(2)}) copy-start(f32[2048]{0:T(1024)} %param.24) | copy-start | bytes 24580
  183.8 3.8 %collective-permute-start.4 = (bf16[4,32,2048]{2,1,0:T(8,128)(2,1)S(1)}, bf16[4,32,2048]{2,1,0:T(8,128)(2,1)S(1)}, u32[]{:S(2)}, u32[]{:S(2)}) collective-permute-start(bf16[4,32,2048]{2,1,0:T(8,128)(2,1)S(1)} %dynamic-slice_bitcast_fusion.2), channel_id=1, source_target_pairs={{0,1},{1,0},{2,3},{3,2},{4,5},{5,4},{6,7},{7,6},{8,9},{9,8},{10,11... | collective-permute-start | bytes 1572872 | tf_op jit(solution)/shard_map/ppermute | solution.py:94
  188.5 12.8 %all-to-all-start.1 = ((bf16[4,32,2048]{2,1,0:T(8,128)(2,1)}), bf16[4,32,2048]{2,1,0:T(8,128)(2,1)S(1)}, u32[]{:S(2)}, u32[]{:S(2)}) async-start(bf16[4,32,2048]{2,1,0:T(8,128)(2,1)} %fusion.47), calls=%async_computation.1 | async-start | bytes 1048576 | tf_op jit(solution)/shard_map/all_to_all | solution.py:248
  211.5 7.8 %collective-permute-start.5 = (bf16[4,32,2048]{2,1,0:T(8,128)(2,1)S(1)}, bf16[4,32,2048]{2,1,0:T(8,128)(2,1)S(1)}, u32[]{:S(2)}, u32[]{:S(2)}) collective-permute-start(bf16[4,32,2048]{2,1,0:T(8,128)(2,1)S(1)} %bitcast.225), channel_id=1, source_target_pairs={{0,1},{1,0},{2,3},{3,2},{4,5},{5,4},{6,7},{7,6},{8,9},{9,8},{10,11... | collective-permute-start | bytes 1572872 | tf_op jit(solution)/shard_map/ppermute | solution.py:94

commit v2 on v1

v2 whole, which is shorter than its diff:
```python
import jax
import jax.numpy as jnp
from jax import lax
from jax.experimental import pallas as pl
from jax.experimental.pallas import tpu as pltpu
from jax.sharding import Mesh
from jax.sharding import PartitionSpec as P

HD = 128
BLOCK = 64
SP = ("z", "y")
TP = ("x", "c")
SCALE = 2.0**18
STATE_SCALE = 2.0**10
NN = (((1,), (0,)), ((), ()))
NT = (((1,), (1,)), ((), ()))
TN = (((0,), (0,)), ((), ()))


eps = 1e-06


def shifted(value, axis, step):
    size = lax.axis_size(axis)
    return lax.ppermute(value, axis, [(k, (k + step) % size) for k in range(size)])


def whole(space=pltpu.VMEM):
    return pl.BlockSpec(memory_space=space)


def dot(left, right, dims=NN):
    return lax.dot_general(
        left.astype(jnp.bfloat16),
        right.astype(jnp.bfloat16),
        dims,
        preferred_element_type=jnp.float32,
    )


def scan_kernel(q_ref, f_ref, v_ref, margin_ref, extra_ref, out_ref, scaled_ref, lines_ref):
    queries = q_ref[...].astype(jnp.float32)
    inflow = margin_ref[...] * jax.nn.sigmoid(-f_ref[...].astype(jnp.float32))
    keep_log = jnp.log1p(-inflow) + extra_ref[...]
    row = lax.broadcasted_iota(jnp.int32, (256, 256), 0)
    column = lax.broadcasted_iota(jnp.int32, (256, 256), 1)
    lower = (column <= row).astype(jnp.float32)
    total = jnp.dot(
        lower, keep_log, precision=lax.Precision.HIGHEST, preferred_element_type=jnp.float32
    )
    scaled_ref[...] = (queries * jnp.exp(total)).astype(jnp.bfloat16)
    causal = lax.broadcasted_iota(jnp.int32, (BLOCK, BLOCK), 1) <= lax.broadcasted_iota(
        jnp.int32, (BLOCK, BLOCK), 0
    )
    state = None
    ended = jnp.zeros((1, HD), jnp.float32)
    for k in range(256 // BLOCK):
        rows = slice(k * BLOCK, (k + 1) * BLOCK)
        inside, sums = queries[rows], total[rows]
        middle, end = sums[BLOCK // 2 - 1 : BLOCK // 2], sums[BLOCK - 1 :]
        values = v_ref[rows]
        scores = dot(inside * jnp.exp(sums - middle), inflow[rows] * jnp.exp(middle - sums), NT)
        result = dot(jnp.where(causal, scores, 0.0), values)
        added = dot(values, inflow[rows] * jnp.exp(end - sums), TN)
        if state is not None:
            result = result + dot(inside * jnp.exp(sums - ended), state, NT)
            added = added + jnp.exp(end - ended) * state
        out_ref[rows, :] = result
        state, ended = added, end
    packed = state.astype(jnp.bfloat16)
    for k in range(8):
        lines_ref[:, k * 128 : (k + 1) * 128] = packed[k * 16 : (k + 1) * 16]
    lines_ref[:, 1024:1152] = jnp.broadcast_to(ended, (16, HD)).astype(jnp.bfloat16)
    lines_ref[:, 1152:1280] = jnp.zeros((16, HD), jnp.bfloat16)


def scanned(queries, logits, values, margin, extra):
    return pl.pallas_call(
        scan_kernel,
        out_shape=(
            jax.ShapeDtypeStruct((256, HD), jnp.float32),
            jax.ShapeDtypeStruct((256, HD), jnp.bfloat16),
            jax.ShapeDtypeStruct((16, 1280), jnp.bfloat16),
        ),
        in_specs=[whole()] * 5,
        out_specs=(whole(),) * 3,
        cost_estimate=pl.CostEstimate(
            flops=4_000_000_000, bytes_accessed=500_000, transcendentals=300_000
        ),
        name="scan",
    )(queries, logits, values, margin, extra)


def y_kernel(y_ref, pieces_ref, total_ref, here_ref):
    y = y_ref[0]
    total_sum = here_sum = jnp.zeros((1, HD), jnp.float32)
    total = here = jnp.zeros((HD, HD), jnp.float32)
    for k in range(4):
        here = jnp.where(k == y, total, here)
        here_sum = jnp.where(k == y, total_sum, here_sum)
        state = jnp.concatenate(
            [pieces_ref[k, 32:48, j * 128 : (j + 1) * 128] for j in range(8)], axis=0
        ).astype(jnp.float32)
        one = pieces_ref[k, 32:48, 1024:1152].astype(jnp.float32)[:1]
        total = jnp.exp(one) * total + state
        total_sum = total_sum + one
    here_ref[:HD, :] = here
    here_ref[HD:, :] = jnp.broadcast_to(here_sum, (8, HD))
    lines = jnp.concatenate(
        [total * STATE_SCALE, jnp.broadcast_to(total_sum, (40, HD))], axis=0
    )
    for j in range(7):
        total_ref[:, j * 128 : (j + 1) * 128] = lines[j * 24 : (j + 1) * 24]


def joined_over_y(y, pieces):
    return pl.pallas_call(
        y_kernel,
        out_shape=(
            jax.ShapeDtypeStruct((24, 896), jnp.float32),
            jax.ShapeDtypeStruct((136, HD), jnp.float32),
        ),
        in_specs=[whole(pltpu.SMEM), whole()],
        out_specs=(whole(), whole()),
        cost_estimate=pl.CostEstimate(
            flops=1_000_000_000, bytes_accessed=700_000, transcendentals=1000
        ),
        name="join",
    )(y, pieces)


def mix_kernel(z_ref, lines_ref, here_ref, out_ref, scaled_ref, logits_ref, gain_ref, gated_ref):
    z = z_ref[0]
    before = jnp.zeros((HD, HD), jnp.float32)
    for k in range(15):
        lines = jnp.concatenate(
            [lines_ref[k, :, j * 128 : (j + 1) * 128] for j in range(7)], axis=0
        )
        joined = jnp.exp(lines[HD : HD + 1]) * before + lines[:HD]
        before = jnp.where(k < z, joined, before)
    here = here_ref[...]
    state = jnp.exp(here[HD : HD + 1]) * (before * (1.0 / STATE_SCALE)) + here[:HD]
    mixed = out_ref[...] + dot(scaled_ref[...], state, NT)
    normed = mixed * lax.rsqrt(jnp.mean(mixed * mixed, axis=-1, keepdims=True) + eps)
    logits = logits_ref[...].astype(jnp.float32)
    gated_ref[...] = (normed * gain_ref[...] * (logits * jax.nn.sigmoid(logits))).astype(
        jnp.bfloat16
    )


def mixed_rows(z, lines, here, out, scaled, logits, gain):
    return pl.pallas_call(
        mix_kernel,
        out_shape=jax.ShapeDtypeStruct((256, HD), jnp.bfloat16),
        in_specs=[whole(pltpu.SMEM)] + [whole()] * 6,
        out_specs=whole(),
        cost_estimate=pl.CostEstimate(
            flops=2_000_000_000, bytes_accessed=2_000_000, transcendentals=100_000
        ),
        name="mix",
    )(z, lines, here, out, scaled, logits, gain)


def ffn_kernel(
    y_ref,
    rows_ref,
    wide_ref,
    own_ref,
    down1_ref,
    up1_ref,
    low_ref,
    high_ref,
    out_ref,
    columns,
    weights,
    hidden,
    column_sems,
    piece_sems,
):
    y = y_ref[0]
    places = [lax.rem(y + k, 4) for k in range(4)]
    column_copies = [
        pltpu.make_async_copy(
            wide_ref.at[:, pl.ds(n * 128, 128)], columns.at[n], column_sems.at[n]
        )
        for n in range(10)
    ]
    piece_copies = [
        pltpu.make_async_copy(ref, weights.at[pl.ds(start, size), places[k]], piece_sems.at[n])
        for n, (ref, k, start, size) in enumerate(
            (
                (own_ref, 0, 0, 16),
                (up1_ref, 1, 0, 16),
                (down1_ref, 3, 0, 16),
                (low_ref, 2, 0, 8),
                (high_ref, 2, 8, 8),
            )
        )
    ]
    for n in range(5):
        column_copies[n].start()
        column_copies[n + 5].start()
    for copy in piece_copies:
        copy.start()
    rows = rows_ref[...]

    for n in range(5):
        column_copies[n].wait()
        gate = jnp.dot(rows, columns[n], preferred_element_type=jnp.float32)
        column_copies[n + 5].wait()
        up = jnp.dot(rows, columns[n + 5], preferred_element_type=jnp.float32)
        hidden[:, n * 128 : (n + 1) * 128] = (gate * jax.nn.sigmoid(gate) * up).astype(
            jnp.bfloat16
        )
    for copy in piece_copies:
        copy.wait()
    last = weights[:, :, :, :128].reshape(2048, 128)
    both = jnp.dot(rows, last, preferred_element_type=jnp.float32)
    gate, up = both[:, :64], both[:, 64:]
    hidden[:, 640:704] = (gate * jax.nn.sigmoid(gate) * up).astype(jnp.bfloat16)
    inner = hidden[:, :704]

    @pl.loop(0, 8)
    def _(n):
        at = pl.multiple_of(n * 256, 256)
        part = lax.dot_general(
            inner,
            weights[pl.ds(n * 2, 2), :, :, 128:832].reshape(256, 704),
            NT,
            preferred_element_type=jnp.float32,
        )
        out_ref[:, pl.ds(at, 256)] = part.astype(jnp.bfloat16)


def ffn(y, rows, wide, *pieces):
    pieces = [piece.reshape(-1, 32, 896) for piece in pieces]
    return pl.pallas_call(
        ffn_kernel,
        out_shape=jax.ShapeDtypeStruct((256, 2048), jnp.bfloat16),
        in_specs=[whole(pltpu.SMEM), whole()] + [whole(pltpu.HBM)] * 6,
        out_specs=whole(),
        scratch_shapes=[
            pltpu.VMEM((10, 2048, 128), jnp.bfloat16),
            pltpu.VMEM((16, 4, 32, 896), jnp.bfloat16),
            pltpu.VMEM((256, 768), jnp.bfloat16),
            pltpu.SemaphoreType.DMA((10,)),
            pltpu.SemaphoreType.DMA((5,)),
        ],
        compiler_params=pltpu.CompilerParams(vmem_limit_bytes=32 * 2**20),
        cost_estimate=pl.CostEstimate(
            flops=2 * 256 * 2048 * 2112, bytes_accessed=11 * 2**20, transcendentals=256 * 704
        ),
        name="ffn",
    )(y, rows, wide, *pieces)


def local(
    residual,
    queries,
    forget_gate_logits,
    projected_values,
    output_gate_logits,
    lower_bound_margin,
    extra_forget_logs,
    per_head_norm_gain,
    output_weight,
    feedforward_norm_gain,
    gate_weight,
    up_weight,
    down_weight,
):
    y = lax.axis_index("y").reshape(1)
    z = lax.axis_index("z").reshape(1)
    with jax.named_scope("outgather"):
        out_copies = jnp.broadcast_to(output_weight, (8, *output_weight.shape))
        out_full = lax.all_to_all(out_copies, TP, split_axis=0, concat_axis=0, tiled=True)
        out_full = out_full.reshape(1024, 2048)
    by_y = jnp.concatenate([gate_weight[:, :640], up_weight[:, :640]], axis=1)
    by_z = jnp.concatenate(
        [gate_weight[:, 640:], up_weight[:, 640:], down_weight.T, jnp.zeros((32, 64), jnp.bfloat16)],
        axis=1,
    )
    by_z = (by_z.astype(jnp.float32) * SCALE).astype(jnp.float16)
    out_rows, scaled, lines = scanned(
        queries,
        forget_gate_logits,
        projected_values,
        lower_bound_margin.reshape(1, HD),
        extra_forget_logs,
    )
    with jax.named_scope("ygather"):
        along_y = lax.all_gather(jnp.concatenate([by_y, lines], axis=0), "y")
    with jax.named_scope("widegather"):
        wide = lax.all_gather(along_y[:, :32].reshape(128, 1280), "z", axis=0, tiled=True)
    total, here = joined_over_y(y, along_y)
    with jax.named_scope("zgather"):
        along_z = lax.all_gather(
            jnp.concatenate([by_z, total.astype(jnp.float16)], axis=0), "z"
        )
    own = (along_z[:, :32].astype(jnp.float32) * (1.0 / SCALE)).astype(jnp.bfloat16)
    own = own.reshape(512, 896)
    down1 = shifted(own, "y", 1)
    up1 = shifted(own, "y", -1)
    gated = mixed_rows(
        z,
        along_z[:, 32:].astype(jnp.float32),
        here,
        out_rows,
        scaled,
        output_gate_logits,
        per_head_norm_gain.reshape(1, HD),
    )
    with jax.named_scope("gatedgather"):
        gated_all = lax.all_gather(gated, TP)
    gated_all, down1, up1 = lax.optimization_barrier((gated_all, down1, up1))
    low = shifted(down1[:256], "y", 1)
    high = shifted(up1[256:], "y", -1)
    gated_all = gated_all.transpose(1, 0, 2).reshape(256, 1024)
    projected = jnp.dot(gated_all, out_full, preferred_element_type=jnp.float32)
    after_mixer = (residual.astype(jnp.float32) + projected).astype(jnp.bfloat16)
    widened = after_mixer.astype(jnp.float32)
    normed = (
        widened
        * lax.rsqrt(jnp.mean(widened * widened, axis=-1, keepdims=True) + eps)
        * feedforward_norm_gain
    ).astype(jnp.bfloat16)
    part = ffn(y, normed, wide, own, down1, up1, low, high)

    core = lax.axis_index("c")
    part = part.reshape(4, 2, 32, 2048)
    theirs = lax.dynamic_index_in_dim(part, 1 - core, 1, keepdims=False)
    mine = lax.dynamic_index_in_dim(part, core, 1, keepdims=False)
    swapped = shifted(theirs, "c", 1)
    pair = (mine.astype(jnp.float32) + swapped.astype(jnp.float32)).astype(jnp.bfloat16)
    place = lax.axis_index(TP) * 32
    own_rows = lax.dynamic_slice_in_dim(after_mixer, place, 32, 0)
    pair, own_rows = lax.optimization_barrier((pair, own_rows))
    arrived = lax.all_to_all(pair, "x", split_axis=0, concat_axis=0, tiled=True)
    ffn_sum = arrived.astype(jnp.float32).sum(axis=0)
    finished = (own_rows.astype(jnp.float32) + 0.5 * ffn_sum).astype(jnp.bfloat16)
    along_x = lax.all_gather(finished, "x")
    others = shifted(along_x, "c", 1)
    first = jnp.where(core == 0, along_x, others)
    second = jnp.where(core == 0, others, along_x)
    return jnp.stack([first, second], axis=1).reshape(256, 2048)


def solution(mesh):
    finer = Mesh(mesh.devices.reshape(16, 4, 4, 2), ("z", "y", "x", "c"))
    placed = (
        P(SP, None),
        P(SP, TP),
        P(SP, TP),
        P(SP, TP),
        P(SP, TP),
        P(TP),
        P(SP, TP),
        P(),
        P(TP, None),
        P(),
        P(SP, TP),
        P(SP, TP),
        P(TP, SP),
    )
    return jax.shard_map(local, mesh=finer, in_specs=placed, out_specs=P(SP, None), check_vma=False)
```

time: 221 us -> 202 us (0.914)
  blocking collectives: 135 us -> 105 us
  between operations: 0.41 us -> 13.6 us
  matrix products: 9.83 us -> 4.05 us
  waiting for transfers between devices: 12.6 us -> 7.41 us
  Pallas kernels: 10.8 us -> 15.8 us
    all_gather x3 -> x2, blocking collectives: 96.3 us -> 63.6 us  [the longest x1 52.4 us: local(): lax.all_gather(jnp.concatenate([by_z, total.astype(jnp.float16)], axis=0)...]
    all_to_all x0 -> x1, blocking collectives: none -> 11.4 us  [local(): arrived = lax.all_to_all(pair, 'x', split_axis=0, concat_axis=0, tiled=True)]
    all_to_all x1 -> x0, waiting for transfers between devices: 9.36 us -> none  [local(): arrived = lax.all_to_all(pair, 'x', split_axis=0, concat_axis=0, tiled=True)]
    all_gather x1, blocking collectives: 28.3 us -> 19.2 us  [local(): gated_all = lax.all_gather(gated, TP)]
    pallas_call x0 -> x3, Pallas kernels: none -> 7.18 us  [the longest x1 2.96 us: scanned(): pl.pallas_call(scan_kernel, out_shape=(jax.ShapeDtypeStruct((256, HD), jn...]
    dot_general x17 -> x0, matrix products: 5.92 us -> none  [the longest x4 3.76 us: block_update(): scores = jnp.einsum('htk,htsk,hsk->hts', queries, weights, state_increment)]
    unnamed x20 -> x22, local copies, waits for them, and re-layouts: 0.04 us -> 5.86 us
    ppermute x6, waiting for transfers between devices: 3.24 us -> 7.39 us  [shifted(): lax.ppermute(value, axis, [(k, (k + step) % size) for k in range(size)])]
  transfers between devices with their start and end apart: 8 -> 8, of which waited for: 3 -> 4; matrix products, arithmetic and copies ran while one was open for 9% -> 7% of each run, Pallas kernels for 0% -> 2%
where the time goes in v2:
time: 202 us; the launch traced here: 201 us
  blocking collectives  105 us (52%)
  starting transfers between devices  36.7 us (18%)
  Pallas kernels  15.8 us (8%)
  between operations  13.6 us (7%)
  local copies, waits for them, and re-layouts  13.1 us (6%)
  waiting for transfers between devices  7.41 us (4%)
  other arithmetic  5.04 us (2%)
  matrix products  4.05 us (2%)
    all_gather x1, blocking collectives, local(): lax.all_gather(jnp.concatenate([by_z, total.astype(jnp.float16)], axis=0)...  52.4 us
    ppermute x6, starting transfers between devices, shifted(): lax.ppermute(value, axis, [(k, (k + step) % size) for k in range(size)])  23.9 us
    all_gather x1, blocking collectives, local(): gated_all = lax.all_gather(gated, TP)  19.2 us
    all_to_all x1, starting transfers between devices, local(): lax.all_to_all(out_copies, TP, split_axis=0, concat_axis=0, tiled=True)  12.8 us
    all_to_all x1, blocking collectives, local(): arrived = lax.all_to_all(pair, 'x', split_axis=0, concat_axis=0, tiled=True)  11.4 us
    all_gather x1, blocking collectives, local(): along_y = lax.all_gather(jnp.concatenate([by_y, lines], axis=0), 'y')  11.2 us
    all_gather x1, blocking collectives, local(): along_x = lax.all_gather(finished, 'x')  11.1 us
    pallas_call x1, Pallas kernels, ffn(): pl.pallas_call(ffn_kernel, out_shape=jax.ShapeDtypeStruct((256, 2048), jn...  8.65 us
  transfers between devices with their start and end apart: 8, of which 4 were waited for; matrix products, arithmetic and copies ran while one was open for 7% of the time, Pallas kernels for 2%

profile of v2, /device:TPU:1, one launch (start us, length us, event | category | flops | bytes accessed | tf_op | source)
XLA Modules:
  0.0 201.1 jit_solution(18323270598187676234)
XLA Ops:
  6.5 3.0 %scan.1 = (f32[256,128]{1,0:T(8,128)}, bf16[256,128]{1,0:T(8,128)(2,1)}, bf16[16,1280]{1,0:T(8,128)(2,1)}) custom-call(bf16[256,128]{1,0:T(8,128)(2,1)} %q_ref.1, bf16[256,128]{1,0:T(8,128)(2,1)} %f_ref.1, bf16[256,128]{1,0:T(8,128)(2,1)} %v_ref.1, f32[1,128]{1,0:T(1,128)} %bitcast.54, f32[256,128]{1,0:T(8,128)} %extra_ref.1), custom_call_target="tpu_custom_call" | custom-call | flops 4000000000 | bytes 500000 | tf_op jit(solution)/shard_map/scan/pallas_call | solution.py:78
  10.4 11.2 %all-gather = bf16[192,1280]{1,0:T(8,128)(2,1)S(1)} all-gather(bf16[48,1280]{1,0:T(8,128)(2,1)S(1)} %pad_maximum_fusion.1), channel_id=2, replica_groups=mesh['z'=16,'y'=4,'x'=4,'c'=2] {'y'}, dimensions={0}, use_global_device_ids=true | all-gather | bytes 614400 | tf_op jit(solution)/shard_map/ygather/all_gather | solution.py:292
  22.4 2.6 %broadcast_in_dim.9 = bf16[8,128,2048]{2,1,0:T(8,128)(2,1)} broadcast(bf16[128,2048]{1,0:T(8,128)(2,1)S(1)} %copy-done.8), dimensions={1,2} | broadcast | bytes 4718592 | tf_op jit(solution)/shard_map/outgather/broadcast_in_dim | solution.py:275
  25.0 12.8 %all-to-all-start = ((bf16[8,128,2048]{2,1,0:T(8,128)(2,1)}), bf16[8,128,2048]{2,1,0:T(8,128)(2,1)}, u32[]{:S(2)}, u32[]{:S(2)}) async-start(bf16[8,128,2048]{2,1,0:T(8,128)(2,1)} %broadcast_in_dim.9), calls=%async_computation | async-start | bytes 8388608 | tf_op jit(solution)/shard_map/outgather/all_to_all | solution.py:276
  37.9 1.8 join.1
  40.7 52.4 %all-gather.8 = f16[896,896]{1,0:T(8,128)(2,1)S(1)} all-gather(f16[56,896]{1,0:T(8,128)(2,1)S(1)} %pad_maximum_fusion.2), channel_id=3, replica_groups=mesh['z'=16,'y'=4,'x'=4,'c'=2] {'z'}, dimensions={0}, use_global_device_ids=true | all-gather | bytes 1705984 | tf_op jit(solution)/shard_map/zgather/all_gather | solution.py:297
  94.3 4.4 %collective-permute-start = (bf16[512,896]{1,0:T(8,128)(2,1)S(1)}, bf16[512,896]{1,0:T(8,128)(2,1)S(1)}, u32[]{:S(2)}, u32[]{:S(2)}) collective-permute-start(bf16[512,896]{1,0:T(8,128)(2,1)S(1)} %bitcast.40), channel_id=1, source_target_pairs={{0,8},{8,16},{16,24},{24,0},{1,9},{9,17},{17,25},{25,1},{2,10},{10... | collective-permute-start | bytes 2752520 | tf_op jit(solution)/shard_map/ppermute | solution.py:25
  98.7 3.8 %collective-permute-start.1 = (bf16[512,896]{1,0:T(8,128)(2,1)S(1)}, bf16[512,896]{1,0:T(8,128)(2,1)S(1)}, u32[]{:S(2)}, u32[]{:S(2)}) collective-permute-start(bf16[512,896]{1,0:T(8,128)(2,1)S(1)} %bitcast.41), channel_id=1, source_target_pairs={{0,24},{8,0},{16,8},{24,16},{1,25},{9,1},{17,9},{25,17},{2,26},{10... | collective-permute-start | bytes 2752520 | tf_op jit(solution)/shard_map/ppermute | solution.py:25
  102.6 2.3 %slice_convert_fusion.lines_ref = f32[16,24,896]{2,1,0:T(8,128)} fusion(f16[16,56,896]{2,1,0:T(8,128)(2,1)} %bitcast.46), kind=kLoop, calls=%fused_computation.13 | loop fusion | flops 344064 | bytes 2064384 | tf_op jit(solution)/shard_map/convert_element_type | solution.py:306
  104.9 2.5 %mix.1 = bf16[256,128]{1,0:T(8,128)(2,1)} custom-call(s32[1]{0:T(128)} %bitcast.1.z_ref, f32[16,24,896]{2,1,0:T(8,128)} %slice_convert_fusion.lines_ref, f32[136,128]{1,0:T(8,128)} %get-tuple-element.17.here_ref, f32[256,128]{1,0:T(8,128)} %get-tuple-element.18.out_ref, bf16[256,128]{1,0:T(8,128)(2,1)} %get-tuple-element.19.scaled_ref, ...), custom_call_target="tpu_custom_call" | custom-call | flops 2000000000 | bytes 2000000 | tf_op jit(solution)/shard_map/mix/pallas_call | solution.py:152
  107.3 19.2 %all-gather.2 = bf16[2048,128]{1,0:T(8,128)(2,1)} all-gather(bf16[256,128]{1,0:T(8,128)(2,1)} %mix.1), channel_id=4, replica_groups=mesh['z'=16,'y'=4,'x'=4,'c'=2] {'x','c'}, dimensions={0}, use_global_device_ids=true | all-gather | bytes 589824 | tf_op jit(solution)/shard_map/gatedgather/all_gather | solution.py:314
  127.4 1.9 collective-permute-start.2
  130.1 4.7 %collective-permute-start.3 = (bf16[256,896]{1,0:T(8,128)(2,1)}, bf16[256,896]{1,0:T(8,128)(2,1)}, u32[]{:S(2)}, u32[]{:S(2)}) collective-permute-start(bf16[256,896]{1,0:T(8,128)(2,1)} %slice.35), channel_id=1, source_target_pairs={{0,24},{8,0},{16,8},{24,16},{1,25},{9,1},{17,9},{25,17},{2,26},{10... | collective-permute-start | bytes 1376264 | tf_op jit(solution)/shard_map/ppermute | solution.py:25
  134.9 4.0 %fusion.2 = (f32[256]{0:T(256)S(1)}, bf16[256,2048]{1,0:T(8,128)(2,1)S(1)}) fusion(bf16[8,128,2048]{2,1,0:T(8,128)(2,1)} %all-to-all-done, bf16[8,256,128]{2,1,0:T(8,128)(2,1)} %bitcast.52, bf16[256,2048]{1,0:T(8,128)(2,1)} %param.13), kind=kOutput, calls=%fused_computation.5 | convolution fusion | flops 1076887296 | bytes 6816768 | tf_op jit(solution)/shard_map/dot_general | solution.py:319
  139.3 3.4 %collective-permute-done.2 = bf16[256,896]{1,0:T(8,128)(2,1)S(1)} collective-permute-done((bf16[256,896]{1,0:T(8,128)(2,1)}, bf16[256,896]{1,0:T(8,128)(2,1)S(1)}, u32[]{:S(2)}, u32[]{:S(2)}) %collective-permute-start.2) | collective-permute-done | bytes 458784 | tf_op jit(solution)/shard_map/ppermute | solution.py:25
  142.6 1.9 collective-permute-done.3
  144.6 2.5 %copy-done = bf16[2048,1280]{1,0:T(8,128)(2,1)S(1)} copy-done((bf16[2048,1280]{1,0:T(8,128)(2,1)S(1)}, bf16[2048,1280]{1,0:T(8,128)(2,1)}, u32[]{:S(2)}) %copy-start) | copy-done | bytes 5242904
  147.1 1.2 copy-done.2
  149.4 8.6 %ffn.1 = bf16[256,2048]{1,0:T(8,128)(2,1)S(1)} custom-call(s32[1]{0:T(128)} %bitcast.y_ref, bf16[256,2048]{1,0:T(8,128)(2,1)S(1)} %fusion.4.rows_ref, bf16[2048,1280]{1,0:T(8,128)(2,1)S(1)} %copy-done, bf16[16,32,896]{2,1,0:T(8,128)(2,1)S(1)} %multiply_convert_fusion.own_ref, bf16[16,32,896]{2,1,0:T(8,128)(2,1)S(1)} %bitcast.42, ...), custom_call_target="tpu_custom_call" | custom-call | flops 2214592512 | bytes 11534336 | tf_op jit(solution)/shard_map/ffn/pallas_call | solution.py:237
  158.1 3.2 %collective-permute-start.4 = (bf16[4,32,2048]{2,1,0:T(8,128)(2,1)S(1)}, bf16[4,32,2048]{2,1,0:T(8,128)(2,1)S(1)}, u32[]{:S(2)}, u32[]{:S(2)}) collective-permute-start(bf16[4,32,2048]{2,1,0:T(8,128)(2,1)S(1)} %dynamic-slice_bitcast_fusion), channel_id=1, source_target_pairs={{0,1},{1,0},{2,3},{3,2},{4,5},{5,4},{6,7},{7,6},{8,9},{9,8},{10,11... | collective-permute-start | bytes 1572872 | tf_op jit(solution)/shard_map/ppermute | solution.py:25
  163.0 11.4 %all_to_all.10 = bf16[4,32,2048]{2,1,0:T(8,128)(2,1)S(1)} all-to-all(bf16[4,32,2048]{2,1,0:T(8,128)(2,1)S(1)} %fusion.5), channel_id=1, replica_groups=mesh['z'=16,'y'=4,'x'=4,'c'=2] {'x'}, dimensions={0} | all-to-all | bytes 1048576 | tf_op jit(solution)/shard_map/all_to_all | solution.py:338
  174.5 11.1 %all-gather.3 = bf16[128,2048]{1,0:T(8,128)(2,1)S(1)} all-gather(bf16[32,2048]{1,0:T(8,128)(2,1)S(1)} %add_convert_fusion), channel_id=5, replica_groups=mesh['z'=16,'y'=4,'x'=4,'c'=2] {'x'}, dimensions={0}, use_global_device_ids=true | all-gather | bytes 655360 | tf_op jit(solution)/shard_map/all_gather | solution.py:341
  185.6 5.8 %collective-permute-start.5 = (bf16[4,32,2048]{2,1,0:T(8,128)(2,1)S(1)}, bf16[4,32,2048]{2,1,0:T(8,128)(2,1)S(1)}, u32[]{:S(2)}, u32[]{:S(2)}) collective-permute-start(bf16[4,32,2048]{2,1,0:T(8,128)(2,1)S(1)} %bitcast.47), channel_id=1, source_target_pairs={{0,1},{1,0},{2,3},{3,2},{4,5},{5,4},{6,7},{7,6},{8,9},{9,8},{10,11... | collective-permute-start | bytes 1572872 | tf_op jit(solution)/shard_map/ppermute | solution.py:25
  191.5 1.5 collective-permute-done.5
  (55 shorter events, 10.2 us)
Async XLA Ops:
  6.5 138.0 %all-gather.7.cloned.1.call-start = ((), (), s32[]{:S(2)}) async-start(), calls=%async_computation.2 | async-start | bytes 5570560 | tf_op jit(solution)/shard_map/widegather/all_gather | solution.py:294
  6.5 3.0 %slice-start = ((bf16[32,704]{1,0:T(8,128)(2,1)}), bf16[32,640]{1,0:T(8,128)(2,1)S(1)}, s32[]{:S(2)}) async-start(bf16[32,704]{1,0:T(8,128)(2,1)} %param.24), calls=%async_computation.3 | async-start | bytes 81920 | tf_op jit(solution)/shard_map/slice | solution.py:278
  6.5 3.0 %slice-start.2 = ((bf16[32,704]{1,0:T(8,128)(2,1)}), bf16[32,640]{1,0:T(8,128)(2,1)S(1)}, s32[]{:S(2)}) async-start(bf16[32,704]{1,0:T(8,128)(2,1)} %param.23), calls=%async_computation.5 | async-start | bytes 81920 | tf_op jit(solution)/shard_map/slice | solution.py:278
  9.5 12.9 %copy-start.8 = (bf16[128,2048]{1,0:T(8,128)(2,1)S(1)}, bf16[128,2048]{1,0:T(8,128)(2,1)}, u32[]{:S(2)}) copy-start(bf16[128,2048]{1,0:T(8,128)(2,1)} %param.21) | copy-start | bytes 1572868
  21.5 3.5 %copy-start.6 = (bf16[192,1280]{1,0:T(8,128)(2,1)}, bf16[192,1280]{1,0:T(8,128)(2,1)S(1)}, u32[]{:S(2)}) copy-start(bf16[192,1280]{1,0:T(8,128)(2,1)S(1)} %all-gather) | copy-start | bytes 1474564
  25.0 109.8 %all-to-all-start = ((bf16[8,128,2048]{2,1,0:T(8,128)(2,1)}), bf16[8,128,2048]{2,1,0:T(8,128)(2,1)}, u32[]{:S(2)}, u32[]{:S(2)}) async-start(bf16[8,128,2048]{2,1,0:T(8,128)(2,1)} %broadcast_in_dim.9), calls=%async_computation | async-start | bytes 8388608 | tf_op jit(solution)/shard_map/outgather/all_to_all | solution.py:276
  37.9 2.8 %slice-start.1 = ((bf16[32,704]{1,0:T(8,128)(2,1)}), bf16[32,64]{1,0:T(8,128)(2,1)S(1)}, s32[]{:S(2)}) async-start(bf16[32,704]{1,0:T(8,128)(2,1)} %param.24), calls=%async_computation.4 | async-start | bytes 16384 | tf_op jit(solution)/shard_map/slice | solution.py:280
  37.9 2.8 %slice-start.3 = ((bf16[32,704]{1,0:T(8,128)(2,1)}), bf16[32,64]{1,0:T(8,128)(2,1)S(1)}, s32[]{:S(2)}) async-start(bf16[32,704]{1,0:T(8,128)(2,1)} %param.23), calls=%async_computation.6 | async-start | bytes 16384 | tf_op jit(solution)/shard_map/slice | solution.py:280
  37.9 2.8 %copy-start.9 = (bf16[704,32]{0,1:T(8,128)(2,1)S(1)}, bf16[704,32]{0,1:T(8,128)(2,1)}, u32[]{:S(2)}) copy-start(bf16[704,32]{0,1:T(8,128)(2,1)} %param.25) | copy-start | bytes 135172
  93.1 1.2 copy-start.5
  94.3 32.2 %collective-permute-start = (bf16[512,896]{1,0:T(8,128)(2,1)S(1)}, bf16[512,896]{1,0:T(8,128)(2,1)S(1)}, u32[]{:S(2)}, u32[]{:S(2)}) collective-permute-start(bf16[512,896]{1,0:T(8,128)(2,1)S(1)} %bitcast.40), channel_id=1, source_target_pairs={{0,8},{8,16},{16,24},{24,0},{1,9},{9,17},{17,25},{25,1},{2,10},{10... | collective-permute-start | bytes 2752520 | tf_op jit(solution)/shard_map/ppermute | solution.py:25
  98.7 27.8 %collective-permute-start.1 = (bf16[512,896]{1,0:T(8,128)(2,1)S(1)}, bf16[512,896]{1,0:T(8,128)(2,1)S(1)}, u32[]{:S(2)}, u32[]{:S(2)}) collective-permute-start(bf16[512,896]{1,0:T(8,128)(2,1)S(1)} %bitcast.41), channel_id=1, source_target_pairs={{0,24},{8,0},{16,8},{24,16},{1,25},{9,1},{17,9},{25,17},{2,26},{10... | collective-permute-start | bytes 2752520 | tf_op jit(solution)/shard_map/ppermute | solution.py:25
  126.5 12.4 %copy-start.1 = (bf16[512,896]{1,0:T(8,128)(2,1)}, bf16[512,896]{1,0:T(8,128)(2,1)S(1)}, u32[]{:S(2)}) copy-start(bf16[512,896]{1,0:T(8,128)(2,1)S(1)} %collective-permute-done) | copy-start | bytes 2752516
  126.5 12.4 %copy-start.3 = (bf16[512,896]{1,0:T(8,128)(2,1)}, bf16[512,896]{1,0:T(8,128)(2,1)S(1)}, u32[]{:S(2)}) copy-start(bf16[512,896]{1,0:T(8,128)(2,1)S(1)} %collective-permute-done.1) | copy-start | bytes 2752516
  127.4 15.2 %collective-permute-start.2 = (bf16[256,896]{1,0:T(8,128)(2,1)}, bf16[256,896]{1,0:T(8,128)(2,1)S(1)}, u32[]{:S(2)}, u32[]{:S(2)}) collective-permute-start(bf16[256,896]{1,0:T(8,128)(2,1)} %slice.34), channel_id=1, source_target_pairs={{0,8},{8,16},{16,24},{24,0},{1,9},{9,17},{17,25},{25,1},{2,10},{10... | collective-permute-start | bytes 1376264 | tf_op jit(solution)/shard_map/ppermute | solution.py:25
  130.1 8.8 %copy-start.10 = (f32[2048]{0:T(1024)S(1)}, f32[2048]{0:T(1024)}, u32[]{:S(2)}) copy-start(f32[2048]{0:T(1024)} %param.22) | copy-start | bytes 24580
  130.1 14.4 %collective-permute-start.3 = (bf16[256,896]{1,0:T(8,128)(2,1)}, bf16[256,896]{1,0:T(8,128)(2,1)}, u32[]{:S(2)}, u32[]{:S(2)}) collective-permute-start(bf16[256,896]{1,0:T(8,128)(2,1)} %slice.35), channel_id=1, source_target_pairs={{0,24},{8,0},{16,8},{24,16},{1,25},{9,1},{17,9},{25,17},{2,26},{10... | collective-permute-start | bytes 1376264 | tf_op jit(solution)/shard_map/ppermute | solution.py:25
  138.9 3.7 %copy-start.7 = (bf16[256,2048]{1,0:T(8,128)(2,1)}, bf16[256,2048]{1,0:T(8,128)(2,1)S(1)}, u32[]{:S(2)}) copy-start(bf16[256,2048]{1,0:T(8,128)(2,1)S(1)} %get-tuple-element.28) | copy-start | bytes 3145732
  144.6 2.5 %copy-start = (bf16[2048,1280]{1,0:T(8,128)(2,1)S(1)}, bf16[2048,1280]{1,0:T(8,128)(2,1)}, u32[]{:S(2)}) copy-start(bf16[2048,1280]{1,0:T(8,128)(2,1)} %all-gather.7.cloned.1.call-done.wide_ref) | copy-start | bytes 15728644
  147.1 1.2 copy-start.2
  148.2 1.2 copy-start.4
  158.1 4.7 %collective-permute-start.4 = (bf16[4,32,2048]{2,1,0:T(8,128)(2,1)S(1)}, bf16[4,32,2048]{2,1,0:T(8,128)(2,1)S(1)}, u32[]{:S(2)}, u32[]{:S(2)}) collective-permute-start(bf16[4,32,2048]{2,1,0:T(8,128)(2,1)S(1)} %dynamic-slice_bitcast_fusion), channel_id=1, source_target_pairs={{0,1},{1,0},{2,3},{3,2},{4,5},{5,4},{6,7},{7,6},{8,9},{9,8},{10,11... | collective-permute-start | bytes 1572872 | tf_op jit(solution)/shard_map/ppermute | solution.py:25
  185.6 7.3 %collective-permute-start.5 = (bf16[4,32,2048]{2,1,0:T(8,128)(2,1)S(1)}, bf16[4,32,2048]{2,1,0:T(8,128)(2,1)S(1)}, u32[]{:S(2)}, u32[]{:S(2)}) collective-permute-start(bf16[4,32,2048]{2,1,0:T(8,128)(2,1)S(1)} %bitcast.47), channel_id=1, source_target_pairs={{0,1},{1,0},{2,3},{3,2},{4,5},{5,4},{6,7},{7,6},{8,9},{9,8},{10,11... | collective-permute-start | bytes 1572872 | tf_op jit(solution)/shard_map/ppermute | solution.py:25
Sparse Core Ops, SparseCore 0:
  22.5 96.8 all-gather.6

commit v3 on v2

--- a/solution.py
+++ b/solution.py
@@ -10,8 +10,6 @@
 BLOCK = 64
 SP = ("z", "y")
 TP = ("x", "c")
-SCALE = 2.0**18
-STATE_SCALE = 2.0**10
 NN = (((1,), (0,)), ((), ()))
 NT = (((1,), (1,)), ((), ()))
 TN = (((0,), (0,)), ((), ()))
@@ -36,6 +34,11 @@
         dims,
         preferred_element_type=jnp.float32,
     )
+
+
+def halves(value):
+    high = value.astype(jnp.bfloat16)
+    return high, (value - high.astype(jnp.float32)).astype(jnp.bfloat16)
 
 
 def scan_kernel(q_ref, f_ref, v_ref, margin_ref, extra_ref, out_ref, scaled_ref, lines_ref):
@@ -70,8 +73,9 @@
     packed = state.astype(jnp.bfloat16)
     for k in range(8):
         lines_ref[:, k * 128 : (k + 1) * 128] = packed[k * 16 : (k + 1) * 16]
-    lines_ref[:, 1024:1152] = jnp.broadcast_to(ended, (16, HD)).astype(jnp.bfloat16)
-    lines_ref[:, 1152:1280] = jnp.zeros((16, HD), jnp.bfloat16)
+    high, low = halves(jnp.broadcast_to(ended, (16, HD)))
+    lines_ref[:, 1024:1152] = high
+    lines_ref[:, 1152:1280] = low
 
 
 def scanned(queries, logits, values, margin, extra):
@@ -99,25 +103,28 @@
         here = jnp.where(k == y, total, here)
         here_sum = jnp.where(k == y, total_sum, here_sum)
         state = jnp.concatenate(
-            [pieces_ref[k, 32:48, j * 128 : (j + 1) * 128] for j in range(8)], axis=0
+            [pieces_ref[k, :, j * 128 : (j + 1) * 128] for j in range(8)], axis=0
         ).astype(jnp.float32)
-        one = pieces_ref[k, 32:48, 1024:1152].astype(jnp.float32)[:1]
+        one = pieces_ref[k, :, 1024:1152].astype(jnp.float32)[:1]
+        one = one + pieces_ref[k, :, 1152:1280].astype(jnp.float32)[:1]
         total = jnp.exp(one) * total + state
         total_sum = total_sum + one
     here_ref[:HD, :] = here
     here_ref[HD:, :] = jnp.broadcast_to(here_sum, (8, HD))
-    lines = jnp.concatenate(
-        [total * STATE_SCALE, jnp.broadcast_to(total_sum, (40, HD))], axis=0
-    )
-    for j in range(7):
-        total_ref[:, j * 128 : (j + 1) * 128] = lines[j * 24 : (j + 1) * 24]
+    packed = total.astype(jnp.bfloat16)
+    high, low = halves(jnp.broadcast_to(total_sum, (16, HD)))
+    total_ref[:, :128] = packed[:48]
+    total_ref[:, 128:256] = packed[48:96]
+    total_ref[:32, 256:] = packed[96:]
+    row = lax.broadcasted_iota(jnp.int32, (16, HD), 0)
+    total_ref[32:, 256:] = jnp.where(row < 8, high, low)
 
 
 def joined_over_y(y, pieces):
     return pl.pallas_call(
         y_kernel,
         out_shape=(
-            jax.ShapeDtypeStruct((24, 896), jnp.float32),
+            jax.ShapeDtypeStruct((48, 384), jnp.bfloat16),
             jax.ShapeDtypeStruct((136, HD), jnp.float32),
         ),
         in_specs=[whole(pltpu.SMEM), whole()],
@@ -134,12 +141,13 @@
     before = jnp.zeros((HD, HD), jnp.float32)
     for k in range(15):
         lines = jnp.concatenate(
-            [lines_ref[k, :, j * 128 : (j + 1) * 128] for j in range(7)], axis=0
-        )
-        joined = jnp.exp(lines[HD : HD + 1]) * before + lines[:HD]
+            [lines_ref[k, 32:, j * 128 : (j + 1) * 128] for j in range(3)], axis=0
+        ).astype(jnp.float32)
+        one = lines[HD : HD + 1] + lines[HD + 8 : HD + 9]
+        joined = jnp.exp(one) * before + lines[:HD]
         before = jnp.where(k < z, joined, before)
     here = here_ref[...]
-    state = jnp.exp(here[HD : HD + 1]) * (before * (1.0 / STATE_SCALE)) + here[:HD]
+    state = jnp.exp(here[HD : HD + 1]) * before + here[:HD]
     mixed = out_ref[...] + dot(scaled_ref[...], state, NT)
     normed = mixed * lax.rsqrt(jnp.mean(mixed * mixed, axis=-1, keepdims=True) + eps)
     logits = logits_ref[...].astype(jnp.float32)
@@ -172,6 +180,7 @@
     high_ref,
     out_ref,
     columns,
+    rest,
     weights,
     hidden,
     column_sems,
@@ -181,10 +190,11 @@
     places = [lax.rem(y + k, 4) for k in range(4)]
     column_copies = [
         pltpu.make_async_copy(
-            wide_ref.at[:, pl.ds(n * 128, 128)], columns.at[n], column_sems.at[n]
+            wide_ref.at[:, pl.ds(n * 256, 256)], columns.at[n], column_sems.at[n]
         )
-        for n in range(10)
+        for n in range(5)
     ]
+    rest_copy = pltpu.make_async_copy(wide_ref.at[:, pl.ds(1280, 512)], rest, column_sems.at[5])
     piece_copies = [
         pltpu.make_async_copy(ref, weights.at[pl.ds(start, size), places[k]], piece_sems.at[n])
         for n, (ref, k, start, size) in enumerate(
@@ -197,35 +207,39 @@
             )
         )
     ]
-    for n in range(5):
-        column_copies[n].start()
-        column_copies[n + 5].start()
+    for copy in column_copies:
+        copy.start()
+    rest_copy.start()
     for copy in piece_copies:
         copy.start()
     rows = rows_ref[...]
 
     for n in range(5):
         column_copies[n].wait()
-        gate = jnp.dot(rows, columns[n], preferred_element_type=jnp.float32)
-        column_copies[n + 5].wait()
-        up = jnp.dot(rows, columns[n + 5], preferred_element_type=jnp.float32)
+        both = jnp.dot(rows, columns[n], preferred_element_type=jnp.float32)
+        gate, up = both[:, :128], both[:, 128:]
         hidden[:, n * 128 : (n + 1) * 128] = (gate * jax.nn.sigmoid(gate) * up).astype(
             jnp.bfloat16
         )
+    rest_copy.wait()
+    both = jnp.dot(rows, rest[:, :128], preferred_element_type=jnp.float32)
+    gate, up = both[:, :64], both[:, 64:]
+    hidden[:, 640:704] = (gate * jax.nn.sigmoid(gate) * up).astype(jnp.bfloat16)
     for copy in piece_copies:
         copy.wait()
-    last = weights[:, :, :, :128].reshape(2048, 128)
-    both = jnp.dot(rows, last, preferred_element_type=jnp.float32)
-    gate, up = both[:, :64], both[:, 64:]
-    hidden[:, 640:704] = (gate * jax.nn.sigmoid(gate) * up).astype(jnp.bfloat16)
-    inner = hidden[:, :704]
+    first, second = hidden[:, :384], hidden[:, 384:704]
 
     @pl.loop(0, 8)
     def _(n):
         at = pl.multiple_of(n * 256, 256)
         part = lax.dot_general(
-            inner,
-            weights[pl.ds(n * 2, 2), :, :, 128:832].reshape(256, 704),
+            first,
+            weights[pl.ds(n * 2, 2)].reshape(256, 384),
+            NT,
+            preferred_element_type=jnp.float32,
+        ) + lax.dot_general(
+            second,
+            rest[pl.ds(at, 256), 128:448],
             NT,
             preferred_element_type=jnp.float32,
         )
@@ -233,20 +247,21 @@
 
 
 def ffn(y, rows, wide, *pieces):
-    pieces = [piece.reshape(-1, 32, 896) for piece in pieces]
+    pieces = [piece.reshape(-1, 32, 384) for piece in pieces]
     return pl.pallas_call(
         ffn_kernel,
         out_shape=jax.ShapeDtypeStruct((256, 2048), jnp.bfloat16),
         in_specs=[whole(pltpu.SMEM), whole()] + [whole(pltpu.HBM)] * 6,
         out_specs=whole(),
         scratch_shapes=[
-            pltpu.VMEM((10, 2048, 128), jnp.bfloat16),
-            pltpu.VMEM((16, 4, 32, 896), jnp.bfloat16),
+            pltpu.VMEM((5, 2048, 256), jnp.bfloat16),
+            pltpu.VMEM((2048, 512), jnp.bfloat16),
+            pltpu.VMEM((16, 4, 32, 384), jnp.bfloat16),
             pltpu.VMEM((256, 768), jnp.bfloat16),
-            pltpu.SemaphoreType.DMA((10,)),
+            pltpu.SemaphoreType.DMA((6,)),
             pltpu.SemaphoreType.DMA((5,)),
         ],
-        compiler_params=pltpu.CompilerParams(vmem_limit_bytes=32 * 2**20),
+        compiler_params=pltpu.CompilerParams(vmem_limit_bytes=60 * 2**20),
         cost_estimate=pl.CostEstimate(
             flops=2 * 256 * 2048 * 2112, bytes_accessed=11 * 2**20, transcendentals=256 * 704
         ),
@@ -275,12 +290,23 @@
         out_copies = jnp.broadcast_to(output_weight, (8, *output_weight.shape))
         out_full = lax.all_to_all(out_copies, TP, split_axis=0, concat_axis=0, tiled=True)
         out_full = out_full.reshape(1024, 2048)
-    by_y = jnp.concatenate([gate_weight[:, :640], up_weight[:, :640]], axis=1)
-    by_z = jnp.concatenate(
-        [gate_weight[:, 640:], up_weight[:, 640:], down_weight.T, jnp.zeros((32, 64), jnp.bfloat16)],
+    turned = down_weight.T
+    blocks = [part[:, n * 128 : (n + 1) * 128] for n in range(5) for part in (gate_weight, up_weight)]
+    by_y = jnp.concatenate(
+        [
+            *blocks,
+            gate_weight[:, 640:],
+            up_weight[:, 640:],
+            turned[:, 384:],
+            jnp.zeros((32, 64), jnp.bfloat16),
+        ],
         axis=1,
     )
-    by_z = (by_z.astype(jnp.float32) * SCALE).astype(jnp.float16)
+    with jax.named_scope("wideygather"):
+        along_y = lax.all_gather(by_y, "y", axis=0, tiled=True)
+    with jax.named_scope("widegather"):
+        wide = lax.all_gather(along_y, "z", axis=0, tiled=True)
+    extra_forget_logs, along_y = lax.optimization_barrier((extra_forget_logs, along_y))
     out_rows, scaled, lines = scanned(
         queries,
         forget_gate_logits,
@@ -289,21 +315,16 @@
         extra_forget_logs,
     )
     with jax.named_scope("ygather"):
-        along_y = lax.all_gather(jnp.concatenate([by_y, lines], axis=0), "y")
-    with jax.named_scope("widegather"):
-        wide = lax.all_gather(along_y[:, :32].reshape(128, 1280), "z", axis=0, tiled=True)
-    total, here = joined_over_y(y, along_y)
+        states = lax.all_gather(lines, "y")
+    total, here = joined_over_y(y, states)
     with jax.named_scope("zgather"):
-        along_z = lax.all_gather(
-            jnp.concatenate([by_z, total.astype(jnp.float16)], axis=0), "z"
-        )
-    own = (along_z[:, :32].astype(jnp.float32) * (1.0 / SCALE)).astype(jnp.bfloat16)
-    own = own.reshape(512, 896)
+        along_z = lax.all_gather(jnp.concatenate([turned[:, :384], total], axis=0), "z")
+    own = along_z[:, :32].reshape(512, 384)
     down1 = shifted(own, "y", 1)
     up1 = shifted(own, "y", -1)
     gated = mixed_rows(
         z,
-        along_z[:, 32:].astype(jnp.float32),
+        along_z,
         here,
         out_rows,
         scaled,

time: 202 us -> 200 us (0.990)
  blocking collectives: 105 us -> 113 us
  waiting for transfers between devices: 7.41 us -> 3.04 us
  local copies, waits for them, and re-layouts: 13.1 us -> 9.66 us
  starting transfers between devices: 36.7 us -> 34.1 us
    all_gather x2 -> x3, blocking collectives: 63.6 us -> 69.1 us  [the longest x1 45.8 us: local(): lax.all_gather(jnp.concatenate([turned[:, :384], total], axis=0), 'z')]
    unnamed x22 -> x16, local copies, waits for them, and re-layouts: 5.86 us -> 0.75 us
    ppermute x6, waiting for transfers between devices: 7.39 us -> 3 us  [shifted(): lax.ppermute(value, axis, [(k, (k + step) % size) for k in range(size)])]
    convert_element_type x4 -> x0, other arithmetic: 3.43 us -> none  [the longest x1 2.29 us: local(): along_z[:, 32:].astype(jnp.float32)]
    ppermute x6, starting transfers between devices: 23.9 us -> 21.4 us  [shifted(): lax.ppermute(value, axis, [(k, (k + step) % size) for k in range(size)])]
    all_gather x1, blocking collectives: 19.2 us -> 21.3 us  [local(): gated_all = lax.all_gather(gated, TP)]
  transfers between devices with their start and end apart: 8 -> 8, of which waited for: 4 -> 2; matrix products, arithmetic and copies ran while one was open for 7% -> 5% of each run, Pallas kernels for 2% -> 3%
where the time goes in v3:
time: 200 us; the launch traced here: 198 us
  blocking collectives  113 us (56%)
  starting transfers between devices  34.1 us (17%)
  Pallas kernels  17.2 us (9%)
  between operations  13.6 us (7%)
  local copies, waits for them, and re-layouts  9.66 us (5%)
  matrix products  3.89 us (2%)
  other arithmetic  3.52 us (2%)
  waiting for transfers between devices  3.04 us (2%)
    all_gather x1, blocking collectives, local(): lax.all_gather(jnp.concatenate([turned[:, :384], total], axis=0), 'z')  45.8 us
    ppermute x6, starting transfers between devices, shifted(): lax.ppermute(value, axis, [(k, (k + step) % size) for k in range(size)])  21.4 us
    all_gather x1, blocking collectives, local(): gated_all = lax.all_gather(gated, TP)  21.3 us
    all_to_all x1, starting transfers between devices, local(): lax.all_to_all(out_copies, TP, split_axis=0, concat_axis=0, tiled=True)  12.7 us
    all_gather x1, blocking collectives, local(): along_y = lax.all_gather(by_y, 'y', axis=0, tiled=True)  12.3 us
    all_to_all x1, blocking collectives, local(): arrived = lax.all_to_all(pair, 'x', split_axis=0, concat_axis=0, tiled=True)  11.8 us
    all_gather x1, blocking collectives, local(): along_x = lax.all_gather(finished, 'x')  11.1 us
    all_gather x1, blocking collectives, local(): states = lax.all_gather(lines, 'y')  11 us
  transfers between devices with their start and end apart: 8, of which 2 were waited for; matrix products, arithmetic and copies ran while one was open for 5% of the time, Pallas kernels for 3%

profile of v3, /device:TPU:1, one launch (start us, length us, event | category | flops | bytes accessed | tf_op | source)
XLA Modules:
  0.0 198.4 jit_solution(11655880349782265173)
XLA Ops:
  9.6 12.3 %all_gather.30 = bf16[128,1792]{1,0:T(8,128)(2,1)} all-gather(bf16[32,1792]{1,0:T(8,128)(2,1)S(1)} %concatenate.6), channel_id=1, replica_groups=mesh['z'=16,'y'=4,'x'=4,'c'=2] {'y'}, dimensions={0}, use_global_device_ids=true | all-gather | bytes 573440 | tf_op jit(solution)/shard_map/wideygather/all_gather | solution.py:306
  21.9 3.6 %broadcast_in_dim.9 = bf16[8,128,2048]{2,1,0:T(8,128)(2,1)} broadcast(bf16[128,2048]{1,0:T(8,128)(2,1)} %param.21), dimensions={1,2} | broadcast | bytes 4718592 | tf_op jit(solution)/shard_map/outgather/broadcast_in_dim | solution.py:290
  25.5 12.7 %all-to-all-start = ((bf16[8,128,2048]{2,1,0:T(8,128)(2,1)}), bf16[8,128,2048]{2,1,0:T(8,128)(2,1)}, u32[]{:S(2)}, u32[]{:S(2)}) async-start(bf16[8,128,2048]{2,1,0:T(8,128)(2,1)} %broadcast_in_dim.9), calls=%async_computation | async-start | bytes 8388608 | tf_op jit(solution)/shard_map/outgather/all_to_all | solution.py:291
  38.2 3.0 %scan.1 = (f32[256,128]{1,0:T(8,128)}, bf16[256,128]{1,0:T(8,128)(2,1)}, bf16[16,1280]{1,0:T(8,128)(2,1)}) custom-call(bf16[256,128]{1,0:T(8,128)(2,1)} %q_ref.1, bf16[256,128]{1,0:T(8,128)(2,1)} %f_ref.1, bf16[256,128]{1,0:T(8,128)(2,1)} %v_ref.1, f32[1,128]{1,0:T(1,128)} %bitcast.53, f32[256,128]{1,0:T(8,128)} %extra_ref), custom_call_target="tpu_custom_call" | custom-call | flops 4000000000 | bytes 500000 | tf_op jit(solution)/shard_map/scan/pallas_call | solution.py:82
  41.2 11.0 %all-gather = bf16[64,1280]{1,0:T(8,128)(2,1)} all-gather(bf16[16,1280]{1,0:T(8,128)(2,1)} %get-tuple-element.17), channel_id=2, replica_groups=mesh['z'=16,'y'=4,'x'=4,'c'=2] {'y'}, dimensions={0}, use_global_device_ids=true | all-gather | bytes 204800 | tf_op jit(solution)/shard_map/ygather/all_gather | solution.py:318
  52.2 1.6 join.1
  54.5 45.8 %all-gather.1 = bf16[1280,384]{1,0:T(8,128)(2,1)S(1)} all-gather(bf16[80,384]{1,0:T(8,128)(2,1)S(1)} %pad_maximum_fusion.1), channel_id=3, replica_groups=mesh['z'=16,'y'=4,'x'=4,'c'=2] {'z'}, dimensions={0}, use_global_device_ids=true | all-gather | bytes 1044480 | tf_op jit(solution)/shard_map/zgather/all_gather | solution.py:321
  100.4 2.3 %collective-permute-start = (bf16[512,384]{1,0:T(8,128)(2,1)S(1)}, bf16[512,384]{1,0:T(8,128)(2,1)S(1)}, u32[]{:S(2)}, u32[]{:S(2)}) collective-permute-start(bf16[512,384]{1,0:T(8,128)(2,1)S(1)} %bitcast.43), channel_id=1, source_target_pairs={{0,8},{8,16},{16,24},{24,0},{1,9},{9,17},{17,25},{25,1},{2,10},{10... | collective-permute-start | bytes 1179656 | tf_op jit(solution)/shard_map/ppermute | solution.py:23
  102.7 4.2 %collective-permute-start.1 = (bf16[512,384]{1,0:T(8,128)(2,1)S(1)}, bf16[512,384]{1,0:T(8,128)(2,1)S(1)}, u32[]{:S(2)}, u32[]{:S(2)}) collective-permute-start(bf16[512,384]{1,0:T(8,128)(2,1)S(1)} %bitcast.44), channel_id=1, source_target_pairs={{0,24},{8,0},{16,8},{24,16},{1,25},{9,1},{17,9},{25,17},{2,26},{10... | collective-permute-start | bytes 1179656 | tf_op jit(solution)/shard_map/ppermute | solution.py:23
  107.0 2.3 %mix.1 = bf16[256,128]{1,0:T(8,128)(2,1)} custom-call(s32[1]{0:T(128)} %bitcast.1.z_ref, bf16[16,80,384]{2,1,0:T(8,128)(2,1)} %bitcast.42, f32[136,128]{1,0:T(8,128)} %get-tuple-element.19.here_ref, f32[256,128]{1,0:T(8,128)} %get-tuple-element.20.out_ref, bf16[256,128]{1,0:T(8,128)(2,1)} %get-tuple-element.21.scaled_ref, bf16[256,128]{1,0:T(8,128)(2,1)} %logits_ref.1, ...), custom_call_target="tpu_custom_call" | custom-call | flops 2000000000 | bytes 2000000 | tf_op jit(solution)/shard_map/mix/pallas_call | solution.py:160
  109.3 21.3 %all-gather.2 = bf16[2048,128]{1,0:T(8,128)(2,1)S(1)} all-gather(bf16[256,128]{1,0:T(8,128)(2,1)} %mix.1), channel_id=4, replica_groups=mesh['z'=16,'y'=4,'x'=4,'c'=2] {'x','c'}, dimensions={0}, use_global_device_ids=true | all-gather | bytes 589824 | tf_op jit(solution)/shard_map/gatedgather/all_gather | solution.py:335
  130.7 1.9 collective-permute-start.2
  132.7 4.6 %collective-permute-start.3 = (bf16[256,384]{1,0:T(8,128)(2,1)S(1)}, bf16[256,384]{1,0:T(8,128)(2,1)S(1)}, u32[]{:S(2)}, u32[]{:S(2)}) collective-permute-start(bf16[256,384]{1,0:T(8,128)(2,1)S(1)} %slice.67), channel_id=1, source_target_pairs={{0,24},{8,0},{16,8},{24,16},{1,25},{9,1},{17,9},{25,17},{2,26},{10... | collective-permute-start | bytes 589832 | tf_op jit(solution)/shard_map/ppermute | solution.py:23
  137.3 3.9 %fusion.2 = (f32[256]{0:T(256)S(1)}, bf16[256,2048]{1,0:T(8,128)(2,1)S(1)}) fusion(bf16[8,128,2048]{2,1,0:T(8,128)(2,1)} %all-to-all-done, bf16[8,256,128]{2,1,0:T(8,128)(2,1)S(1)} %bitcast.47, bf16[256,2048]{1,0:T(8,128)(2,1)} %param.13), kind=kOutput, calls=%fused_computation.5 | convolution fusion | flops 1076887296 | bytes 6816768 | tf_op jit(solution)/shard_map/dot_general | solution.py:340
  141.2 1.3 fusion.4.rows_ref
  143.2 10.3 %ffn.1 = bf16[256,2048]{1,0:T(8,128)(2,1)} custom-call(s32[1]{0:T(128)} %bitcast.y_ref, bf16[256,2048]{1,0:T(8,128)(2,1)} %fusion.4.rows_ref, bf16[2048,1792]{1,0:T(8,128)(2,1)} %all-gather.6.cloned.1.call-done.wide_ref, bf16[16,32,384]{2,1,0:T(8,128)(2,1)} %copy-done.1, bf16[16,32,384]{2,1,0:T(8,128)(2,1)} %bitcast.45, bf16[16,32,384]{2,1,0:T(8,128)(2,1)} %bitcast.46, ...), custom_call_target="tpu_custom_call" | custom-call | flops 2214592512 | bytes 11534336 | tf_op jit(solution)/shard_map/ffn/pallas_call | solution.py:251
  153.6 1.1 dynamic-slice_bitcast_fusion
  154.7 2.6 %collective-permute-start.4 = (bf16[4,32,2048]{2,1,0:T(8,128)(2,1)S(1)}, bf16[4,32,2048]{2,1,0:T(8,128)(2,1)S(1)}, u32[]{:S(2)}, u32[]{:S(2)}) collective-permute-start(bf16[4,32,2048]{2,1,0:T(8,128)(2,1)S(1)} %dynamic-slice_bitcast_fusion), channel_id=1, source_target_pairs={{0,1},{1,0},{2,3},{3,2},{4,5},{5,4},{6,7},{7,6},{8,9},{9,8},{10,11... | collective-permute-start | bytes 1572872 | tf_op jit(solution)/shard_map/ppermute | solution.py:23
  157.3 1.5 collective-permute-done.4
  158.8 1.2 fusion.5
  160.0 11.8 %all_to_all.10 = bf16[4,32,2048]{2,1,0:T(8,128)(2,1)S(1)} all-to-all(bf16[4,32,2048]{2,1,0:T(8,128)(2,1)S(1)} %fusion.5), channel_id=1, replica_groups=mesh['z'=16,'y'=4,'x'=4,'c'=2] {'x'}, dimensions={0} | all-to-all | bytes 1048576 | tf_op jit(solution)/shard_map/all_to_all | solution.py:359
  171.9 11.1 %all-gather.3 = bf16[128,2048]{1,0:T(8,128)(2,1)S(1)} all-gather(bf16[32,2048]{1,0:T(8,128)(2,1)S(1)} %add_convert_fusion), channel_id=5, replica_groups=mesh['z'=16,'y'=4,'x'=4,'c'=2] {'x'}, dimensions={0}, use_global_device_ids=true | all-gather | bytes 655360 | tf_op jit(solution)/shard_map/all_gather | solution.py:362
  183.0 5.8 %collective-permute-start.5 = (bf16[4,32,2048]{2,1,0:T(8,128)(2,1)S(1)}, bf16[4,32,2048]{2,1,0:T(8,128)(2,1)S(1)}, u32[]{:S(2)}, u32[]{:S(2)}) collective-permute-start(bf16[4,32,2048]{2,1,0:T(8,128)(2,1)S(1)} %bitcast.39), channel_id=1, source_target_pairs={{0,1},{1,0},{2,3},{3,2},{4,5},{5,4},{6,7},{7,6},{8,9},{9,8},{10,11... | collective-permute-start | bytes 1572872 | tf_op jit(solution)/shard_map/ppermute | solution.py:23
  188.9 1.5 collective-permute-done.5
  (42 shorter events, 6.1 us)
Async XLA Ops:
  6.5 136.0 %all-gather.6.cloned.1.call-start = ((), (), s32[]{:S(2)}) async-start(), calls=%async_computation.2 | async-start | bytes 7798784 | tf_op jit(solution)/shard_map/widegather/all_gather | solution.py:308
  25.5 12.7 %copy-start.6 = (bf16[704,32]{0,1:T(8,128)(2,1)S(1)}, bf16[704,32]{0,1:T(8,128)(2,1)}, u32[]{:S(2)}) copy-start(bf16[704,32]{0,1:T(8,128)(2,1)} %param.25) | copy-start | bytes 135172
  25.5 111.7 %all-to-all-start = ((bf16[8,128,2048]{2,1,0:T(8,128)(2,1)}), bf16[8,128,2048]{2,1,0:T(8,128)(2,1)}, u32[]{:S(2)}, u32[]{:S(2)}) async-start(bf16[8,128,2048]{2,1,0:T(8,128)(2,1)} %broadcast_in_dim.9), calls=%async_computation | async-start | bytes 8388608 | tf_op jit(solution)/shard_map/outgather/all_to_all | solution.py:291
  100.4 6.6 %copy-start = (bf16[1280,384]{1,0:T(8,128)(2,1)}, bf16[1280,384]{1,0:T(8,128)(2,1)S(1)}, u32[]{:S(2)}) copy-start(bf16[1280,384]{1,0:T(8,128)(2,1)S(1)} %all-gather.1) | copy-start | bytes 2949124
  100.4 8.9 %copy-start.1 = (bf16[16,32,384]{2,1,0:T(8,128)(2,1)}, bf16[16,32,384]{2,1,0:T(8,128)(2,1)S(1)}, u32[]{:S(2)}) copy-start(bf16[16,32,384]{2,1,0:T(8,128)(2,1)S(1)} %slice.70.own_ref) | copy-start | bytes 1179652
  100.4 30.2 %collective-permute-start = (bf16[512,384]{1,0:T(8,128)(2,1)S(1)}, bf16[512,384]{1,0:T(8,128)(2,1)S(1)}, u32[]{:S(2)}, u32[]{:S(2)}) collective-permute-start(bf16[512,384]{1,0:T(8,128)(2,1)S(1)} %bitcast.43), channel_id=1, source_target_pairs={{0,8},{8,16},{16,24},{24,0},{1,9},{9,17},{17,25},{25,1},{2,10},{10... | collective-permute-start | bytes 1179656 | tf_op jit(solution)/shard_map/ppermute | solution.py:23
  102.7 27.9 %collective-permute-start.1 = (bf16[512,384]{1,0:T(8,128)(2,1)S(1)}, bf16[512,384]{1,0:T(8,128)(2,1)S(1)}, u32[]{:S(2)}, u32[]{:S(2)}) collective-permute-start(bf16[512,384]{1,0:T(8,128)(2,1)S(1)} %bitcast.44), channel_id=1, source_target_pairs={{0,24},{8,0},{16,8},{24,16},{1,25},{9,1},{17,9},{25,17},{2,26},{10... | collective-permute-start | bytes 1179656 | tf_op jit(solution)/shard_map/ppermute | solution.py:23
  130.7 10.5 %copy-start.2 = (bf16[512,384]{1,0:T(8,128)(2,1)}, bf16[512,384]{1,0:T(8,128)(2,1)S(1)}, u32[]{:S(2)}) copy-start(bf16[512,384]{1,0:T(8,128)(2,1)S(1)} %collective-permute-done) | copy-start | bytes 1179652
  130.7 10.5 %copy-start.3 = (bf16[512,384]{1,0:T(8,128)(2,1)}, bf16[512,384]{1,0:T(8,128)(2,1)S(1)}, u32[]{:S(2)}) copy-start(bf16[512,384]{1,0:T(8,128)(2,1)S(1)} %collective-permute-done.1) | copy-start | bytes 1179652
  130.7 11.8 %collective-permute-start.2 = (bf16[256,384]{1,0:T(8,128)(2,1)S(1)}, bf16[256,384]{1,0:T(8,128)(2,1)S(1)}, u32[]{:S(2)}, u32[]{:S(2)}) collective-permute-start(bf16[256,384]{1,0:T(8,128)(2,1)S(1)} %slice.66), channel_id=1, source_target_pairs={{0,8},{8,16},{16,24},{24,0},{1,9},{9,17},{17,25},{25,1},{2,10},{10... | collective-permute-start | bytes 589832 | tf_op jit(solution)/shard_map/ppermute | solution.py:23
  132.7 8.5 %copy-start.7 = (f32[2048]{0:T(1024)S(1)}, f32[2048]{0:T(1024)}, u32[]{:S(2)}) copy-start(f32[2048]{0:T(1024)} %param.22) | copy-start | bytes 24580
  132.7 9.8 %collective-permute-start.3 = (bf16[256,384]{1,0:T(8,128)(2,1)S(1)}, bf16[256,384]{1,0:T(8,128)(2,1)S(1)}, u32[]{:S(2)}, u32[]{:S(2)}) collective-permute-start(bf16[256,384]{1,0:T(8,128)(2,1)S(1)} %slice.67), channel_id=1, source_target_pairs={{0,24},{8,0},{16,8},{24,16},{1,25},{9,1},{17,9},{25,17},{2,26},{10... | collective-permute-start | bytes 589832 | tf_op jit(solution)/shard_map/ppermute | solution.py:23
  142.5 0.7 copy-start.4
  142.5 0.8 copy-start.5
  154.7 4.2 %collective-permute-start.4 = (bf16[4,32,2048]{2,1,0:T(8,128)(2,1)S(1)}, bf16[4,32,2048]{2,1,0:T(8,128)(2,1)S(1)}, u32[]{:S(2)}, u32[]{:S(2)}) collective-permute-start(bf16[4,32,2048]{2,1,0:T(8,128)(2,1)S(1)} %dynamic-slice_bitcast_fusion), channel_id=1, source_target_pairs={{0,1},{1,0},{2,3},{3,2},{4,5},{5,4},{6,7},{7,6},{8,9},{9,8},{10,11... | collective-permute-start | bytes 1572872 | tf_op jit(solution)/shard_map/ppermute | solution.py:23
  183.0 7.3 %collective-permute-start.5 = (bf16[4,32,2048]{2,1,0:T(8,128)(2,1)S(1)}, bf16[4,32,2048]{2,1,0:T(8,128)(2,1)S(1)}, u32[]{:S(2)}, u32[]{:S(2)}) collective-permute-start(bf16[4,32,2048]{2,1,0:T(8,128)(2,1)S(1)} %bitcast.39), channel_id=1, source_target_pairs={{0,1},{1,0},{2,3},{3,2},{4,5},{5,4},{6,7},{7,6},{8,9},{9,8},{10,11... | collective-permute-start | bytes 1572872 | tf_op jit(solution)/shard_map/ppermute | solution.py:23
Sparse Core Ops, SparseCore 0:
  22.1 112.4 all-gather.5

commit v4 on v3

v4 whole, which is shorter than its diff:
```python
import jax
import jax.numpy as jnp
from jax import lax
from jax.experimental import pallas as pl
from jax.experimental.pallas import tpu as pltpu
from jax.sharding import Mesh
from jax.sharding import PartitionSpec as P

HD = 128
BLOCK = 64
SP = ("z", "y")
TP = ("x", "c")
SCALE = 2.0**18
STATE_SCALE = 2.0**10
NN = (((1,), (0,)), ((), ()))
NT = (((1,), (1,)), ((), ()))
TN = (((0,), (0,)), ((), ()))


eps = 1e-06


def shifted(value, axis, step):
    size = lax.axis_size(axis)
    return lax.ppermute(value, axis, [(k, (k + step) % size) for k in range(size)])


def whole(space=pltpu.VMEM):
    return pl.BlockSpec(memory_space=space)


def dot(left, right, dims=NN):
    return lax.dot_general(
        left.astype(jnp.bfloat16),
        right.astype(jnp.bfloat16),
        dims,
        preferred_element_type=jnp.float32,
    )


def halves(value):
    high = value.astype(jnp.bfloat16)
    return high, (value - high.astype(jnp.float32)).astype(jnp.bfloat16)


def scan_kernel(
    q_ref,
    f_ref,
    v_ref,
    margin_ref,
    extra_ref,
    gate_ref,
    up_ref,
    turned_ref,
    out_ref,
    scaled_ref,
    packed_ref,
):
    queries = q_ref[...].astype(jnp.float32)
    inflow = margin_ref[...] * jax.nn.sigmoid(-f_ref[...].astype(jnp.float32))
    keep_log = jnp.log1p(-inflow) + extra_ref[...]
    row = lax.broadcasted_iota(jnp.int32, (256, 256), 0)
    column = lax.broadcasted_iota(jnp.int32, (256, 256), 1)
    lower = (column <= row).astype(jnp.float32)
    total = jnp.dot(
        lower, keep_log, precision=lax.Precision.HIGHEST, preferred_element_type=jnp.float32
    )
    scaled_ref[...] = (queries * jnp.exp(total)).astype(jnp.bfloat16)
    causal = lax.broadcasted_iota(jnp.int32, (BLOCK, BLOCK), 1) <= lax.broadcasted_iota(
        jnp.int32, (BLOCK, BLOCK), 0
    )
    state = None
    ended = jnp.zeros((1, HD), jnp.float32)
    for k in range(256 // BLOCK):
        rows = slice(k * BLOCK, (k + 1) * BLOCK)
        inside, sums = queries[rows], total[rows]
        middle, end = sums[BLOCK // 2 - 1 : BLOCK // 2], sums[BLOCK - 1 :]
        values = v_ref[rows]
        scores = dot(inside * jnp.exp(sums - middle), inflow[rows] * jnp.exp(middle - sums), NT)
        result = dot(jnp.where(causal, scores, 0.0), values)
        added = dot(values, inflow[rows] * jnp.exp(end - sums), TN)
        if state is not None:
            result = result + dot(inside * jnp.exp(sums - ended), state, NT)
            added = added + jnp.exp(end - ended) * state
        out_ref[rows, :] = result
        state, ended = added, end
    packed = state.astype(jnp.bfloat16)
    for k in range(8):
        packed_ref[32:, k * 128 : (k + 1) * 128] = packed[k * 16 : (k + 1) * 16]
    high, low = halves(jnp.broadcast_to(ended, (16, HD)))
    packed_ref[32:, 1024:1152] = high
    packed_ref[32:, 1152:1280] = low
    packed_ref[32:, 1280:] = jnp.zeros((16, 256), jnp.bfloat16)
    for k in range(5):
        packed_ref[:32, k * 256 : k * 256 + 128] = gate_ref[:, k * 128 : (k + 1) * 128]
        packed_ref[:32, k * 256 + 128 : (k + 1) * 256] = up_ref[:, k * 128 : (k + 1) * 128]
    packed_ref[:32, 1280:1408] = jnp.concatenate([gate_ref[:, 640:], up_ref[:, 640:]], axis=1)
    packed_ref[:32, 1408:] = jnp.concatenate(
        [turned_ref[:, 640:], jnp.zeros((32, 64), jnp.bfloat16)], axis=1
    )


def scanned(*operands):
    return pl.pallas_call(
        scan_kernel,
        out_shape=(
            jax.ShapeDtypeStruct((256, HD), jnp.float32),
            jax.ShapeDtypeStruct((256, HD), jnp.bfloat16),
            jax.ShapeDtypeStruct((48, 1536), jnp.bfloat16),
        ),
        in_specs=[whole()] * 8,
        out_specs=(whole(),) * 3,
        cost_estimate=pl.CostEstimate(
            flops=4_000_000_000, bytes_accessed=500_000, transcendentals=300_000
        ),
        name="scan",
    )(*operands)


def y_kernel(y_ref, pieces_ref, turned_ref, total_ref, here_ref):
    y = y_ref[0]
    total_sum = here_sum = jnp.zeros((1, HD), jnp.float32)
    total = here = jnp.zeros((HD, HD), jnp.float32)
    for k in range(4):
        here = jnp.where(k == y, total, here)
        here_sum = jnp.where(k == y, total_sum, here_sum)
        state = jnp.concatenate(
            [pieces_ref[k, 32:, j * 128 : (j + 1) * 128] for j in range(8)], axis=0
        ).astype(jnp.float32)
        one = pieces_ref[k, 32:, 1024:1152].astype(jnp.float32)[:1]
        one = one + pieces_ref[k, 32:, 1152:1280].astype(jnp.float32)[:1]
        total = jnp.exp(one) * total + state
        total_sum = total_sum + one
    here_ref[:HD, :] = here
    here_ref[HD:, :] = jnp.broadcast_to(here_sum, (8, HD))
    total_ref[:32, :] = turned_ref[:, :640].astype(jnp.float32) * SCALE
    for k in range(4):
        total_ref[32:, k * 128 : (k + 1) * 128] = total[k * 32 : (k + 1) * 32] * STATE_SCALE
    total_ref[32:, 512:] = jnp.broadcast_to(total_sum, (32, HD))


def joined_over_y(y, pieces, turned):
    return pl.pallas_call(
        y_kernel,
        out_shape=(
            jax.ShapeDtypeStruct((64, 640), jnp.float32),
            jax.ShapeDtypeStruct((136, HD), jnp.float32),
        ),
        in_specs=[whole(pltpu.SMEM), whole(), whole()],
        out_specs=(whole(), whole()),
        cost_estimate=pl.CostEstimate(
            flops=1_000_000_000, bytes_accessed=700_000, transcendentals=1000
        ),
        name="join",
    )(y, pieces, turned)


def mix_kernel(z_ref, lines_ref, here_ref, out_ref, scaled_ref, logits_ref, gain_ref, gated_ref):
    z = z_ref[0]
    before = jnp.zeros((HD, HD), jnp.float32)
    for k in range(15):
        state = jnp.concatenate(
            [lines_ref[k, :, j * 128 : (j + 1) * 128] for j in range(4)], axis=0
        )
        joined = jnp.exp(lines_ref[k, :1, 512:]) * before + state
        before = jnp.where(k < z, joined, before)
    here = here_ref[...]
    state = jnp.exp(here[HD : HD + 1]) * (before * (1.0 / STATE_SCALE)) + here[:HD]
    mixed = out_ref[...] + dot(scaled_ref[...], state, NT)
    normed = mixed * lax.rsqrt(jnp.mean(mixed * mixed, axis=-1, keepdims=True) + eps)
    logits = logits_ref[...].astype(jnp.float32)
    gated_ref[...] = (normed * gain_ref[...] * (logits * jax.nn.sigmoid(logits))).astype(
        jnp.bfloat16
    )


def mixed_rows(z, lines, here, out, scaled, logits, gain):
    return pl.pallas_call(
        mix_kernel,
        out_shape=jax.ShapeDtypeStruct((256, HD), jnp.bfloat16),
        in_specs=[whole(pltpu.SMEM)] + [whole()] * 6,
        out_specs=whole(),
        cost_estimate=pl.CostEstimate(
            flops=2_000_000_000, bytes_accessed=2_000_000, transcendentals=100_000
        ),
        name="mix",
    )(z, lines, here, out, scaled, logits, gain)


def ffn_kernel(
    place_ref,
    rows_ref,
    wide_ref,
    own_ref,
    down1_ref,
    up1_ref,
    far_ref,
    mine_ref,
    theirs_ref,
    columns,
    rest,
    weights,
    hidden,
    column_sems,
    piece_sems,
):
    y, core = place_ref[0], place_ref[1]
    places = [lax.rem(y + k, 4) for k in range(4)]
    column_copies = [
        pltpu.make_async_copy(
            wide_ref.at[:, pl.ds(n * 256, 256)], columns.at[n], column_sems.at[n]
        )
        for n in range(5)
    ]
    rest_copy = pltpu.make_async_copy(wide_ref.at[:, pl.ds(1280, 256)], rest, column_sems.at[5])
    piece_copies = [
        pltpu.make_async_copy(ref, weights.at[:, places[k]], piece_sems.at[n])
        for n, (ref, k) in enumerate(
            (
                (own_ref, 0),
                (up1_ref, 1),
                (far_ref, 2),
                (down1_ref, 3),
            )
        )
    ]
    for copy in column_copies:
        copy.start()
    rest_copy.start()
    for copy in piece_copies:
        copy.start()
    rows = rows_ref[...]

    for n in range(5):
        column_copies[n].wait()
        both = jnp.dot(rows, columns[n], preferred_element_type=jnp.float32)
        gate, up = both[:, :128], both[:, 128:]
        hidden[:, n * 128 : (n + 1) * 128] = (gate * jax.nn.sigmoid(gate) * up).astype(
            jnp.bfloat16
        )
    rest_copy.wait()
    both = jnp.dot(rows, rest[:, :128], preferred_element_type=jnp.float32)
    gate, up = both[:, :64], both[:, 64:]
    hidden[:, 640:704] = (gate * jax.nn.sigmoid(gate) * up).astype(jnp.bfloat16)
    for copy in piece_copies:
        copy.wait()
    first, second = hidden[:, :640], hidden[:, 640:704]

    @pl.loop(0, 8)
    def _(n):
        at = pl.multiple_of(n * 256, 256)
        part = lax.dot_general(
            first,
            weights[pl.ds(n * 2, 2)].reshape(256, 640),
            NT,
            preferred_element_type=jnp.float32,
        ) + lax.dot_general(
            second,
            rest[pl.ds(at, 256), 128:192],
            NT,
            preferred_element_type=jnp.float32,
        )
        part = part.astype(jnp.bfloat16).reshape(4, 2, 32, 256)
        mine_ref[:, :, pl.ds(at, 256)] = jnp.where(core == 0, part[:, 0], part[:, 1])
        theirs_ref[:, :, pl.ds(at, 256)] = jnp.where(core == 0, part[:, 1], part[:, 0])


def ffn(place, rows, wide, *pieces):
    pieces = [piece.reshape(16, 32, 640) for piece in pieces]
    half = jax.ShapeDtypeStruct((4, 32, 2048), jnp.bfloat16)
    return pl.pallas_call(
        ffn_kernel,
        out_shape=(half, half),
        in_specs=[whole(pltpu.SMEM), whole()] + [whole(pltpu.HBM)] * 5,
        out_specs=(whole(), whole()),
        scratch_shapes=[
            pltpu.VMEM((5, 2048, 256), jnp.bfloat16),
            pltpu.VMEM((2048, 256), jnp.bfloat16),
            pltpu.VMEM((16, 4, 32, 640), jnp.bfloat16),
            pltpu.VMEM((256, 768), jnp.bfloat16),
            pltpu.SemaphoreType.DMA((6,)),
            pltpu.SemaphoreType.DMA((4,)),
        ],
        compiler_params=pltpu.CompilerParams(vmem_limit_bytes=60 * 2**20),
        cost_estimate=pl.CostEstimate(
            flops=2 * 256 * 2048 * 2112, bytes_accessed=11 * 2**20, transcendentals=256 * 704
        ),
        name="ffn",
    )(place, rows, wide, *pieces)


def local(
    residual,
    queries,
    forget_gate_logits,
    projected_values,
    output_gate_logits,
    lower_bound_margin,
    extra_forget_logs,
    per_head_norm_gain,
    output_weight,
    feedforward_norm_gain,
    gate_weight,
    up_weight,
    down_weight,
):
    y = lax.axis_index("y").reshape(1)
    z = lax.axis_index("z").reshape(1)
    core = lax.axis_index("c")
    turned = down_weight.T
    out_rows, scaled, packed = scanned(
        queries,
        forget_gate_logits,
        projected_values,
        lower_bound_margin.reshape(1, HD),
        extra_forget_logs,
        gate_weight,
        up_weight,
        turned,
    )
    with jax.named_scope("ygather"):
        along_y = lax.all_gather(packed, "y")
    with jax.named_scope("widegather"):
        wide = lax.all_gather(along_y[:, :32].reshape(128, 1536), "z", axis=0, tiled=True)
    with jax.named_scope("outgather"):
        out_copies = jnp.broadcast_to(output_weight, (4, *output_weight.shape))
        out_mine = lax.all_to_all(out_copies, "x", split_axis=0, concat_axis=0, tiled=True)
    total, here = joined_over_y(y, along_y, turned)
    with jax.named_scope("zgather"):
        along_z = lax.all_gather(total.astype(jnp.float16), "z")
    own = (along_z[:, :32].astype(jnp.float32) * (1.0 / SCALE)).astype(jnp.bfloat16)
    own = own.reshape(512, 640)
    down1 = shifted(own, "y", 1)
    up1 = shifted(own, "y", -1)
    far = shifted(own, "y", 2)
    lines = along_z[:, 32:].astype(jnp.float32)
    lines, out_mine = lax.optimization_barrier((lines, out_mine))
    out_other = shifted(out_mine, "c", 1)
    gated = mixed_rows(
        z,
        lines,
        here,
        out_rows,
        scaled,
        output_gate_logits,
        per_head_norm_gain.reshape(1, HD),
    )
    with jax.named_scope("gatedgather"):
        gated_all = lax.all_gather(gated, TP)
    gated_all = gated_all.reshape(4, 2, 256, HD)
    projected = 0.0
    for which, weight in ((core, out_mine), (1 - core, out_other)):
        heads = lax.dynamic_index_in_dim(gated_all, which, 1, keepdims=False)
        projected = projected + jnp.dot(
            heads.transpose(1, 0, 2).reshape(256, 512),
            weight.reshape(512, 2048),
            preferred_element_type=jnp.float32,
        )
    after_mixer = (residual.astype(jnp.float32) + projected).astype(jnp.bfloat16)
    widened = after_mixer.astype(jnp.float32)
    normed = (
        widened
        * lax.rsqrt(jnp.mean(widened * widened, axis=-1, keepdims=True) + eps)
        * feedforward_norm_gain
    ).astype(jnp.bfloat16)
    places = jnp.stack([lax.axis_index("y"), core])
    mine, theirs = ffn(places, normed, wide, own, down1, up1, far)
    swapped = shifted(theirs, "c", 1)
    pair = (mine.astype(jnp.float32) + swapped.astype(jnp.float32)).astype(jnp.bfloat16)
    place = lax.axis_index(TP) * 32
    own_rows = lax.dynamic_slice_in_dim(after_mixer, place, 32, 0)
    pair, own_rows = lax.optimization_barrier((pair, own_rows))
    arrived = lax.all_to_all(pair, "x", split_axis=0, concat_axis=0, tiled=True)
    ffn_sum = arrived.astype(jnp.float32).sum(axis=0)
    finished = (own_rows.astype(jnp.float32) + 0.5 * ffn_sum).astype(jnp.bfloat16)
    along_x = lax.all_gather(finished, "x")
    others = shifted(along_x, "c", 1)
    first = jnp.where(core == 0, along_x, others)
    second = jnp.where(core == 0, others, along_x)
    return jnp.stack([first, second], axis=1).reshape(256, 2048)


def solution(mesh):
    finer = Mesh(mesh.devices.reshape(16, 4, 4, 2), ("z", "y", "x", "c"))
    placed = (
        P(SP, None),
        P(SP, TP),
        P(SP, TP),
        P(SP, TP),
        P(SP, TP),
        P(TP),
        P(SP, TP),
        P(),
        P(TP, None),
        P(),
        P(SP, TP),
        P(SP, TP),
        P(TP, SP),
    )
    return jax.shard_map(local, mesh=finer, in_specs=placed, out_specs=P(SP, None), check_vma=False)
```

time: 200 us -> 189 us (0.945)
  blocking collectives: 113 us -> 103 us
  local copies, waits for them, and re-layouts: 9.66 us -> 4.14 us
  other arithmetic: 3.52 us -> 6.51 us
    ppermute x6, starting transfers between devices: 21.4 us -> 30.1 us  [shifted(): lax.ppermute(value, axis, [(k, (k + step) % size) for k in range(size)])]
    all_to_all x1, starting transfers between devices: 12.7 us -> 5.4 us  [local(): lax.all_to_all(out_copies, 'x', split_axis=0, concat_axis=0, tiled=True)]
    all_gather x3 -> x2, blocking collectives: 69.1 us -> 62.1 us  [the longest x1 50.4 us: local(): along_z = lax.all_gather(total.astype(jnp.float16), 'z')]
    all_gather x1, blocking collectives: 21.3 us -> 16.2 us  [local(): gated_all = lax.all_gather(gated, TP)]
    convert_element_type x0 -> x3, other arithmetic: none -> 3.11 us  [the longest x1 1.23 us: local(): lines = along_z[:, 32:].astype(jnp.float32)]
    slice x8 -> x1, local copies, waits for them, and re-layouts: 3.07 us -> 0.82 us  [local(): along_y[:, :32].reshape(128, 1536)]
  transfers between devices with their start and end apart: 8 -> 8, of which waited for: 2 -> 3; matrix products, arithmetic and copies ran while one was open for 5% -> 5% of each run, Pallas kernels for 3% -> 2%
where the time goes in v4:
time: 189 us; the launch traced here: 188 us
  blocking collectives  103 us (54%)
  starting transfers between devices  35.5 us (19%)
  Pallas kernels  17.6 us (9%)
  between operations  13.6 us (7%)
  other arithmetic  6.51 us (3%)
  local copies, waits for them, and re-layouts  4.14 us (2%)
  waiting for transfers between devices  4.12 us (2%)
  matrix products  3.27 us (2%)
    all_gather x1, blocking collectives, local(): along_z = lax.all_gather(total.astype(jnp.float16), 'z')  50.4 us
    ppermute x6, starting transfers between devices, shifted(): lax.ppermute(value, axis, [(k, (k + step) % size) for k in range(size)])  30.1 us
    all_gather x1, blocking collectives, local(): gated_all = lax.all_gather(gated, TP)  16.2 us
    all_to_all x1, blocking collectives, local(): arrived = lax.all_to_all(pair, 'x', split_axis=0, concat_axis=0, tiled=True)  13.7 us
    all_gather x1, blocking collectives, local(): along_y = lax.all_gather(packed, 'y')  11.7 us
    all_gather x1, blocking collectives, local(): along_x = lax.all_gather(finished, 'x')  11.1 us
    pallas_call x1, Pallas kernels, ffn(): pl.pallas_call(ffn_kernel, out_shape=(half, half), in_specs=[whole(pltpu....  10.4 us
    all_to_all x1, starting transfers between devices, local(): lax.all_to_all(out_copies, 'x', split_axis=0, concat_axis=0, tiled=True)  5.4 us
  transfers between devices with their start and end apart: 8, of which 3 were waited for; matrix products, arithmetic and copies ran while one was open for 5% of the time, Pallas kernels for 2%

profile of v4, /device:TPU:1, one launch (start us, length us, event | category | flops | bytes accessed | tf_op | source)
XLA Modules:
  0.0 187.8 jit_solution(17083772113627719176)
XLA Ops:
  6.5 3.0 %scan.1 = (f32[256,128]{1,0:T(8,128)}, bf16[256,128]{1,0:T(8,128)(2,1)}, bf16[48,1536]{1,0:T(8,128)(2,1)}) custom-call(bf16[256,128]{1,0:T(8,128)(2,1)} %q_ref.1, bf16[256,128]{1,0:T(8,128)(2,1)} %f_ref.1, bf16[256,128]{1,0:T(8,128)(2,1)} %v_ref.1, f32[1,128]{1,0:T(1,128)} %bitcast.57, f32[256,128]{1,0:T(8,128)} %extra_ref.1, bf16[32,704]{1,0:T(8,128)(2,1)} %gate_ref.1, ...), custom_call_target="tpu_custom_call" | custom-call | flops 4000000000 | bytes 500000 | tf_op jit(solution)/shard_map/scan/pallas_call | solution.py:104
  9.6 11.7 %all-gather = bf16[192,1536]{1,0:T(8,128)(2,1)S(1)} all-gather(bf16[48,1536]{1,0:T(8,128)(2,1)} %get-tuple-element.16), channel_id=2, replica_groups=mesh['z'=16,'y'=4,'x'=4,'c'=2] {'y'}, dimensions={0}, use_global_device_ids=true | all-gather | bytes 737280 | tf_op jit(solution)/shard_map/ygather/all_gather | solution.py:322
  22.1 1.6 broadcast_in_dim.2
  23.7 5.4 %all-to-all-start = ((bf16[4,128,2048]{2,1,0:T(8,128)(2,1)}), bf16[4,128,2048]{2,1,0:T(8,128)(2,1)S(1)}, u32[]{:S(2)}, u32[]{:S(2)}) async-start(bf16[4,128,2048]{2,1,0:T(8,128)(2,1)} %broadcast_in_dim.2), calls=%async_computation | async-start | bytes 4194304 | tf_op jit(solution)/shard_map/outgather/all_to_all | solution.py:327
  29.1 1.8 join.1
  31.9 50.4 %all-gather.8 = f16[1024,640]{1,0:T(8,128)(2,1)S(1)} all-gather(f16[64,640]{1,0:T(8,128)(2,1)S(1)} %convert_element_type.43), channel_id=3, replica_groups=mesh['z'=16,'y'=4,'x'=4,'c'=2] {'z'}, dimensions={0}, use_global_device_ids=true | all-gather | bytes 1392640 | tf_op jit(solution)/shard_map/zgather/all_gather | solution.py:330
  82.2 1.2 slice_convert_fusion.lines_ref
  83.5 11.2 %collective-permute-start = (bf16[4,128,2048]{2,1,0:T(8,128)(2,1)S(1)}, bf16[4,128,2048]{2,1,0:T(8,128)(2,1)}, u32[]{:S(2)}, u32[]{:S(2)}) collective-permute-start(bf16[4,128,2048]{2,1,0:T(8,128)(2,1)S(1)} %all-to-all-done), channel_id=1, source_target_pairs={{0,1},{1,0},{2,3},{3,2},{4,5},{5,4},{6,7},{7,6},{8,9},{9,8},{10,11... | collective-permute-start | bytes 6291464 | tf_op jit(solution)/shard_map/ppermute | solution.py:25
  95.6 2.4 %collective-permute-start.1 = (bf16[512,640]{1,0:T(8,128)(2,1)}, bf16[512,640]{1,0:T(8,128)(2,1)S(1)}, u32[]{:S(2)}, u32[]{:S(2)}) collective-permute-start(bf16[512,640]{1,0:T(8,128)(2,1)} %bitcast.16), channel_id=1, source_target_pairs={{0,8},{8,16},{16,24},{24,0},{1,9},{9,17},{17,25},{25,1},{2,10},{10... | collective-permute-start | bytes 1966088 | tf_op jit(solution)/shard_map/ppermute | solution.py:25
  98.1 4.1 %collective-permute-start.2 = (bf16[512,640]{1,0:T(8,128)(2,1)}, bf16[512,640]{1,0:T(8,128)(2,1)S(1)}, u32[]{:S(2)}, u32[]{:S(2)}) collective-permute-start(bf16[512,640]{1,0:T(8,128)(2,1)} %bitcast.16), channel_id=1, source_target_pairs={{0,24},{8,0},{16,8},{24,16},{1,25},{9,1},{17,9},{25,17},{2,26},{10... | collective-permute-start | bytes 1966088 | tf_op jit(solution)/shard_map/ppermute | solution.py:25
  102.1 3.1 %collective-permute-start.3 = (bf16[512,640]{1,0:T(8,128)(2,1)}, bf16[512,640]{1,0:T(8,128)(2,1)}, u32[]{:S(2)}, u32[]{:S(2)}) collective-permute-start(bf16[512,640]{1,0:T(8,128)(2,1)} %bitcast.16), channel_id=1, source_target_pairs={{0,16},{8,24},{16,0},{24,8},{1,17},{9,25},{17,1},{25,9},{2,18},{10... | collective-permute-start | bytes 1966088 | tf_op jit(solution)/shard_map/ppermute | solution.py:25
  105.9 2.4 %mix.1 = bf16[256,128]{1,0:T(8,128)(2,1)} custom-call(s32[1]{0:T(128)} %bitcast.2.z_ref, f32[16,32,640]{2,1,0:T(8,128)} %slice_convert_fusion.lines_ref, f32[136,128]{1,0:T(8,128)} %get-tuple-element.19.here_ref, f32[256,128]{1,0:T(8,128)} %get-tuple-element.20.out_ref, bf16[256,128]{1,0:T(8,128)(2,1)} %get-tuple-element.21.scaled_ref, ...), custom_call_target="tpu_custom_call" | custom-call | flops 2000000000 | bytes 2000000 | tf_op jit(solution)/shard_map/mix/pallas_call | solution.py:178
  108.3 16.2 %all-gather.2 = bf16[2048,128]{1,0:T(8,128)(2,1)S(1)} all-gather(bf16[256,128]{1,0:T(8,128)(2,1)} %mix.1), channel_id=4, replica_groups=mesh['z'=16,'y'=4,'x'=4,'c'=2] {'x','c'}, dimensions={0}, use_global_device_ids=true | all-gather | bytes 589824 | tf_op jit(solution)/shard_map/gatedgather/all_gather | solution.py:349
  125.8 2.5 %fusion.3 = (f32[256]{0:T(256)S(1)}, bf16[256,2048]{1,0:T(8,128)(2,1)S(1)}) fusion(f32[256,2048]{1,0:T(8,128)S(1)} %convolution_bitcast_fusion.1, bf16[4,128,2048]{2,1,0:T(8,128)(2,1)} %collective-permute-done, bf16[4,2,256,128]{3,2,1,0:T(8,128)(2,1)S(1)} %bitcast.49, s32[]{:T(128)S(6)} %select_n.24, bf16[256,2048]{1,0:T(8,128)(2,1)S(1)} %copy-done.1), kind=kOutput, calls=%fused_computation.7 | convolution fusion | flops 540540672 | bytes 6554628 | tf_op jit(solution)/shard_map/dot_general | solution.py:354
  128.3 1.3 fusion.5.rows_ref
  130.7 10.4 %ffn.1 = (bf16[4,32,2048]{2,1,0:T(8,128)(2,1)}, bf16[4,32,2048]{2,1,0:T(8,128)(2,1)}) custom-call(s32[2]{0:T(128)} %pad_add_fusion.place_ref, bf16[256,2048]{1,0:T(8,128)(2,1)} %fusion.5.rows_ref, bf16[2048,1536]{1,0:T(8,128)(2,1)} %all-gather.7.cloned.1.call-done.wide_ref, bf16[16,32,640]{2,1,0:T(8,128)(2,1)} %multiply_convert_fusion.own_ref, ...), custom_call_target="tpu_custom_call" | custom-call | flops 2214592512 | bytes 11534336 | tf_op jit(solution)/shard_map/ffn/pallas_call | solution.py:271
  141.0 3.5 %collective-permute-start.4 = (bf16[4,32,2048]{2,1,0:T(8,128)(2,1)}, bf16[4,32,2048]{2,1,0:T(8,128)(2,1)S(1)}, u32[]{:S(2)}, u32[]{:S(2)}) collective-permute-start(bf16[4,32,2048]{2,1,0:T(8,128)(2,1)} %get-tuple-element.24), channel_id=1, source_target_pairs={{0,1},{1,0},{2,3},{3,2},{4,5},{5,4},{6,7},{7,6},{8,9},{9,8},{10,11... | collective-permute-start | bytes 1572872 | tf_op jit(solution)/shard_map/ppermute | solution.py:25
  144.6 1.7 collective-permute-done.4
  146.3 1.2 add_convert_fusion
  147.5 13.7 %all_to_all.10 = bf16[4,32,2048]{2,1,0:T(8,128)(2,1)S(1)} all-to-all(bf16[4,32,2048]{2,1,0:T(8,128)(2,1)S(1)} %add_convert_fusion), channel_id=1, replica_groups=mesh['z'=16,'y'=4,'x'=4,'c'=2] {'x'}, dimensions={0} | all-to-all | bytes 1048576 | tf_op jit(solution)/shard_map/all_to_all | solution.py:373
  161.3 11.1 %all-gather.3 = bf16[128,2048]{1,0:T(8,128)(2,1)S(1)} all-gather(bf16[32,2048]{1,0:T(8,128)(2,1)S(1)} %add_convert_fusion.1), channel_id=5, replica_groups=mesh['z'=16,'y'=4,'x'=4,'c'=2] {'x'}, dimensions={0}, use_global_device_ids=true | all-gather | bytes 655360 | tf_op jit(solution)/shard_map/all_gather | solution.py:376
  172.4 5.8 %collective-permute-start.5 = (bf16[4,32,2048]{2,1,0:T(8,128)(2,1)S(1)}, bf16[4,32,2048]{2,1,0:T(8,128)(2,1)S(1)}, u32[]{:S(2)}, u32[]{:S(2)}) collective-permute-start(bf16[4,32,2048]{2,1,0:T(8,128)(2,1)S(1)} %bitcast.46), channel_id=1, source_target_pairs={{0,1},{1,0},{2,3},{3,2},{4,5},{5,4},{6,7},{7,6},{8,9},{9,8},{10,11... | collective-permute-start | bytes 1572872 | tf_op jit(solution)/shard_map/ppermute | solution.py:25
  178.2 1.5 collective-permute-done.5
  179.9 1.0 copy.14
  (31 shorter events, 5.9 us)
Async XLA Ops:
  6.5 124.0 %all-gather.7.cloned.1.call-start = ((), (), s32[]{:S(2)}) async-start(), calls=%async_computation.2 | async-start | bytes 6684672 | tf_op jit(solution)/shard_map/widegather/all_gather | solution.py:324
  9.6 12.5 %copy-start.4 = (bf16[128,2048]{1,0:T(8,128)(2,1)S(1)}, bf16[128,2048]{1,0:T(8,128)(2,1)}, u32[]{:S(2)}) copy-start(bf16[128,2048]{1,0:T(8,128)(2,1)} %param.21) | copy-start | bytes 1572868
  21.3 2.5 %copy-start = (bf16[192,1536]{1,0:T(8,128)(2,1)}, bf16[192,1536]{1,0:T(8,128)(2,1)S(1)}, u32[]{:S(2)}) copy-start(bf16[192,1536]{1,0:T(8,128)(2,1)S(1)} %all-gather) | copy-start | bytes 1769476
  23.7 59.7 %all-to-all-start = ((bf16[4,128,2048]{2,1,0:T(8,128)(2,1)}), bf16[4,128,2048]{2,1,0:T(8,128)(2,1)S(1)}, u32[]{:S(2)}, u32[]{:S(2)}) async-start(bf16[4,128,2048]{2,1,0:T(8,128)(2,1)} %broadcast_in_dim.2), calls=%async_computation | async-start | bytes 4194304 | tf_op jit(solution)/shard_map/outgather/all_to_all | solution.py:327
  83.5 41.8 %collective-permute-start = (bf16[4,128,2048]{2,1,0:T(8,128)(2,1)S(1)}, bf16[4,128,2048]{2,1,0:T(8,128)(2,1)}, u32[]{:S(2)}, u32[]{:S(2)}) collective-permute-start(bf16[4,128,2048]{2,1,0:T(8,128)(2,1)S(1)} %all-to-all-done), channel_id=1, source_target_pairs={{0,1},{1,0},{2,3},{3,2},{4,5},{5,4},{6,7},{7,6},{8,9},{9,8},{10,11... | collective-permute-start | bytes 6291464 | tf_op jit(solution)/shard_map/ppermute | solution.py:25
  95.6 34.0 %collective-permute-start.1 = (bf16[512,640]{1,0:T(8,128)(2,1)}, bf16[512,640]{1,0:T(8,128)(2,1)S(1)}, u32[]{:S(2)}, u32[]{:S(2)}) collective-permute-start(bf16[512,640]{1,0:T(8,128)(2,1)} %bitcast.16), channel_id=1, source_target_pairs={{0,8},{8,16},{16,24},{24,0},{1,9},{9,17},{17,25},{25,1},{2,10},{10... | collective-permute-start | bytes 1966088 | tf_op jit(solution)/shard_map/ppermute | solution.py:25
  98.1 31.5 %collective-permute-start.2 = (bf16[512,640]{1,0:T(8,128)(2,1)}, bf16[512,640]{1,0:T(8,128)(2,1)S(1)}, u32[]{:S(2)}, u32[]{:S(2)}) collective-permute-start(bf16[512,640]{1,0:T(8,128)(2,1)} %bitcast.16), channel_id=1, source_target_pairs={{0,24},{8,0},{16,8},{24,16},{1,25},{9,1},{17,9},{25,17},{2,26},{10... | collective-permute-start | bytes 1966088 | tf_op jit(solution)/shard_map/ppermute | solution.py:25
  102.1 28.4 %collective-permute-start.3 = (bf16[512,640]{1,0:T(8,128)(2,1)}, bf16[512,640]{1,0:T(8,128)(2,1)}, u32[]{:S(2)}, u32[]{:S(2)}) collective-permute-start(bf16[512,640]{1,0:T(8,128)(2,1)} %bitcast.16), channel_id=1, source_target_pairs={{0,16},{8,24},{16,0},{24,8},{1,17},{9,25},{17,1},{25,9},{2,18},{10... | collective-permute-start | bytes 1966088 | tf_op jit(solution)/shard_map/ppermute | solution.py:25
  124.5 1.2 copy-start.1
  125.3 3.1 %copy-start.5 = (f32[2048]{0:T(1024)S(1)}, f32[2048]{0:T(1024)}, u32[]{:S(2)}) copy-start(f32[2048]{0:T(1024)} %param.22) | copy-start | bytes 24580
  129.6 0.9 copy-start.2
  129.6 1.0 copy-start.3
  141.0 5.3 %collective-permute-start.4 = (bf16[4,32,2048]{2,1,0:T(8,128)(2,1)}, bf16[4,32,2048]{2,1,0:T(8,128)(2,1)S(1)}, u32[]{:S(2)}, u32[]{:S(2)}) collective-permute-start(bf16[4,32,2048]{2,1,0:T(8,128)(2,1)} %get-tuple-element.24), channel_id=1, source_target_pairs={{0,1},{1,0},{2,3},{3,2},{4,5},{5,4},{6,7},{7,6},{8,9},{9,8},{10,11... | collective-permute-start | bytes 1572872 | tf_op jit(solution)/shard_map/ppermute | solution.py:25
  172.4 7.3 %collective-permute-start.5 = (bf16[4,32,2048]{2,1,0:T(8,128)(2,1)S(1)}, bf16[4,32,2048]{2,1,0:T(8,128)(2,1)S(1)}, u32[]{:S(2)}, u32[]{:S(2)}) collective-permute-start(bf16[4,32,2048]{2,1,0:T(8,128)(2,1)S(1)} %bitcast.46), channel_id=1, source_target_pairs={{0,1},{1,0},{2,3},{3,2},{4,5},{5,4},{6,7},{7,6},{8,9},{9,8},{10,11... | collective-permute-start | bytes 1572872 | tf_op jit(solution)/shard_map/ppermute | solution.py:25
Sparse Core Ops, SparseCore 0:
  22.2 103.2 all-gather.6

commit v5 on v4

--- a/solution.py
+++ b/solution.py
@@ -5,6 +5,7 @@
 from jax.experimental.pallas import tpu as pltpu
 from jax.sharding import Mesh
 from jax.sharding import PartitionSpec as P
+
 
 HD = 128
 BLOCK = 64
@@ -188,7 +189,8 @@
 
 
 def ffn_kernel(
-    place_ref,
+    y_ref,
+    core_ref,
     rows_ref,
     wide_ref,
     own_ref,
@@ -197,22 +199,21 @@
     far_ref,
     mine_ref,
     theirs_ref,
-    columns,
-    rest,
+    bands,
+    half,
     weights,
     hidden,
-    column_sems,
+    band_sems,
     piece_sems,
 ):
-    y, core = place_ref[0], place_ref[1]
+    y, core = y_ref[0], core_ref[0]
     places = [lax.rem(y + k, 4) for k in range(4)]
-    column_copies = [
+    band_copies = [
         pltpu.make_async_copy(
-            wide_ref.at[:, pl.ds(n * 256, 256)], columns.at[n], column_sems.at[n]
-        )
-        for n in range(5)
+            wide_ref.at[pl.ds(n * 1024, 1024)], bands.at[pl.ds(n * 1024, 1024)], band_sems.at[n]
+        )
+        for n in range(2)
     ]
-    rest_copy = pltpu.make_async_copy(wide_ref.at[:, pl.ds(1280, 256)], rest, column_sems.at[5])
     piece_copies = [
         pltpu.make_async_copy(ref, weights.at[:, places[k]], piece_sems.at[n])
         for n, (ref, k) in enumerate(
@@ -224,24 +225,26 @@
             )
         )
     ]
-    for copy in column_copies:
+    for copy in band_copies:
         copy.start()
-    rest_copy.start()
     for copy in piece_copies:
         copy.start()
-    rows = rows_ref[...]
-
-    for n in range(5):
-        column_copies[n].wait()
-        both = jnp.dot(rows, columns[n], preferred_element_type=jnp.float32)
-        gate, up = both[:, :128], both[:, 128:]
-        hidden[:, n * 128 : (n + 1) * 128] = (gate * jax.nn.sigmoid(gate) * up).astype(
+    spans = [slice(n * 256, min(n * 256 + 256, 1408)) for n in range(6)]
+    rows = rows_ref[:, :1024]
+    band_copies[0].wait()
+    for span in spans:
+        half[:, span] = jnp.dot(rows, bands[:1024, span], preferred_element_type=jnp.float32)
+    rows = rows_ref[:, 1024:]
+    band_copies[1].wait()
+    for n, span in enumerate(spans):
+        both = half[:, span] + jnp.dot(
+            rows, bands[1024:, span], preferred_element_type=jnp.float32
+        )
+        width = both.shape[1] // 2
+        gate, up = both[:, :width], both[:, width:]
+        hidden[:, n * 128 : n * 128 + width] = (gate * jax.nn.sigmoid(gate) * up).astype(
             jnp.bfloat16
         )
-    rest_copy.wait()
-    both = jnp.dot(rows, rest[:, :128], preferred_element_type=jnp.float32)
-    gate, up = both[:, :64], both[:, 64:]
-    hidden[:, 640:704] = (gate * jax.nn.sigmoid(gate) * up).astype(jnp.bfloat16)
     for copy in piece_copies:
         copy.wait()
     first, second = hidden[:, :640], hidden[:, 640:704]
@@ -256,7 +259,7 @@
             preferred_element_type=jnp.float32,
         ) + lax.dot_general(
             second,
-            rest[pl.ds(at, 256), 128:192],
+            bands[pl.ds(at, 256), 1408:1472],
             NT,
             preferred_element_type=jnp.float32,
         )
@@ -265,20 +268,20 @@
         theirs_ref[:, :, pl.ds(at, 256)] = jnp.where(core == 0, part[:, 1], part[:, 0])
 
 
-def ffn(place, rows, wide, *pieces):
+def ffn(y, core, rows, wide, *pieces):
     pieces = [piece.reshape(16, 32, 640) for piece in pieces]
     half = jax.ShapeDtypeStruct((4, 32, 2048), jnp.bfloat16)
     return pl.pallas_call(
         ffn_kernel,
         out_shape=(half, half),
-        in_specs=[whole(pltpu.SMEM), whole()] + [whole(pltpu.HBM)] * 5,
+        in_specs=[whole(pltpu.SMEM)] * 2 + [whole()] + [whole(pltpu.HBM)] * 5,
         out_specs=(whole(), whole()),
         scratch_shapes=[
-            pltpu.VMEM((5, 2048, 256), jnp.bfloat16),
-            pltpu.VMEM((2048, 256), jnp.bfloat16),
+            pltpu.VMEM((2048, 1536), jnp.bfloat16),
+            pltpu.VMEM((256, 1408), jnp.float32),
             pltpu.VMEM((16, 4, 32, 640), jnp.bfloat16),
             pltpu.VMEM((256, 768), jnp.bfloat16),
-            pltpu.SemaphoreType.DMA((6,)),
+            pltpu.SemaphoreType.DMA((2,)),
             pltpu.SemaphoreType.DMA((4,)),
         ],
         compiler_params=pltpu.CompilerParams(vmem_limit_bytes=60 * 2**20),
@@ -286,7 +289,7 @@
             flops=2 * 256 * 2048 * 2112, bytes_accessed=11 * 2**20, transcendentals=256 * 704
         ),
         name="ffn",
-    )(place, rows, wide, *pieces)
+    )(y, core, rows, wide, *pieces)
 
 
 def local(
@@ -318,23 +321,19 @@
         up_weight,
         turned,
     )
-    with jax.named_scope("ygather"):
-        along_y = lax.all_gather(packed, "y")
-    with jax.named_scope("widegather"):
-        wide = lax.all_gather(along_y[:, :32].reshape(128, 1536), "z", axis=0, tiled=True)
-    with jax.named_scope("outgather"):
-        out_copies = jnp.broadcast_to(output_weight, (4, *output_weight.shape))
-        out_mine = lax.all_to_all(out_copies, "x", split_axis=0, concat_axis=0, tiled=True)
+    along_y = lax.all_gather(packed, "y")
+    wide = lax.all_gather(along_y[:, :32].reshape(128, 1536), "z", axis=0, tiled=True)
+    out_copies = jnp.broadcast_to(output_weight, (4, *output_weight.shape))
+    out_mine = lax.all_to_all(out_copies, "x", split_axis=0, concat_axis=0, tiled=True)
     total, here = joined_over_y(y, along_y, turned)
-    with jax.named_scope("zgather"):
-        along_z = lax.all_gather(total.astype(jnp.float16), "z")
+    along_z = lax.all_gather(total.astype(jnp.float16), "z")
     own = (along_z[:, :32].astype(jnp.float32) * (1.0 / SCALE)).astype(jnp.bfloat16)
     own = own.reshape(512, 640)
     down1 = shifted(own, "y", 1)
     up1 = shifted(own, "y", -1)
     far = shifted(own, "y", 2)
     lines = along_z[:, 32:].astype(jnp.float32)
-    lines, out_mine = lax.optimization_barrier((lines, out_mine))
+    lines, out_mine, own = lax.optimization_barrier((lines, out_mine, own))
     out_other = shifted(out_mine, "c", 1)
     gated = mixed_rows(
         z,
@@ -345,14 +344,14 @@
         output_gate_logits,
         per_head_norm_gain.reshape(1, HD),
     )
-    with jax.named_scope("gatedgather"):
-        gated_all = lax.all_gather(gated, TP)
-    gated_all = gated_all.reshape(4, 2, 256, HD)
+    heads = lax.all_to_all(
+        jnp.broadcast_to(gated, (4, 256, HD)), "x", split_axis=0, concat_axis=0, tiled=True
+    )
+    heads_other = shifted(heads, "c", 1)
     projected = 0.0
-    for which, weight in ((core, out_mine), (1 - core, out_other)):
-        heads = lax.dynamic_index_in_dim(gated_all, which, 1, keepdims=False)
+    for part, weight in ((heads, out_mine), (heads_other, out_other)):
         projected = projected + jnp.dot(
-            heads.transpose(1, 0, 2).reshape(256, 512),
+            part.transpose(1, 0, 2).reshape(256, 512),
             weight.reshape(512, 2048),
             preferred_element_type=jnp.float32,
         )
@@ -363,8 +362,7 @@
         * lax.rsqrt(jnp.mean(widened * widened, axis=-1, keepdims=True) + eps)
         * feedforward_norm_gain
     ).astype(jnp.bfloat16)
-    places = jnp.stack([lax.axis_index("y"), core])
-    mine, theirs = ffn(places, normed, wide, own, down1, up1, far)
+    mine, theirs = ffn(y, core.reshape(1), normed, wide, own, down1, up1, far)
     swapped = shifted(theirs, "c", 1)
     pair = (mine.astype(jnp.float32) + swapped.astype(jnp.float32)).astype(jnp.bfloat16)
     place = lax.axis_index(TP) * 32
@@ -397,4 +395,6 @@
         P(SP, TP),
         P(TP, SP),
     )
-    return jax.shard_map(local, mesh=finer, in_specs=placed, out_specs=P(SP, None), check_vma=False)
+    return jax.shard_map(
+        local, mesh=finer, in_specs=placed, out_specs=P(SP, None), check_vma=False
+    )

time: 189 us -> 203 us (1.074)
  waiting for transfers between devices: 4.12 us -> 23.2 us
  blocking collectives: 103 us -> 94.3 us
  starting transfers between devices: 35.5 us -> 40.3 us
    ppermute x6 -> x7, waiting for transfers between devices: 4.1 us -> 23.2 us  [shifted(): lax.ppermute(value, axis, [(k, (k + step) % size) for k in range(size)])]
    all_gather x1 -> x0, blocking collectives: 16.2 us -> none  [local(): gated_all = lax.all_gather(gated, TP)]
    all_to_all x0 -> x1, blocking collectives: none -> 10.4 us  [local(): lax.all_to_all(jnp.broadcast_to(gated, (4, 256, HD)), 'x', split_axis=0,...]
    ppermute x6 -> x7, starting transfers between devices: 30.1 us -> 34.9 us  [shifted(): lax.ppermute(value, axis, [(k, (k + step) % size) for k in range(size)])]
    all_to_all x1, blocking collectives: 13.7 us -> 11.6 us  [local(): arrived = lax.all_to_all(pair, 'x', split_axis=0, concat_axis=0, tiled=True)]
  transfers between devices with their start and end apart: 8 -> 9, of which waited for: 3 -> 5; matrix products, arithmetic and copies ran while one was open for 5% -> 5% of each run, Pallas kernels for 2% -> 2%
where the time goes in v5:
time: 203 us; the launch traced here: 201 us
  blocking collectives  94.3 us (46%)
  starting transfers between devices  40.3 us (20%)
  waiting for transfers between devices  23.2 us (11%)
  Pallas kernels  16.6 us (8%)
  between operations  13.6 us (7%)
  other arithmetic  5.1 us (3%)
  local copies, waits for them, and re-layouts  4.87 us (2%)
  matrix products  3.23 us (2%)
    all_gather x1, blocking collectives, local(): along_z = lax.all_gather(total.astype(jnp.float16), 'z')  50.4 us
    ppermute x7, starting transfers between devices, shifted(): lax.ppermute(value, axis, [(k, (k + step) % size) for k in range(size)])  34.9 us
    ppermute x7, waiting for transfers between devices, shifted(): lax.ppermute(value, axis, [(k, (k + step) % size) for k in range(size)])  23.2 us
    all_gather x1, blocking collectives, local(): along_y = lax.all_gather(packed, 'y')  11.7 us
    all_to_all x1, blocking collectives, local(): arrived = lax.all_to_all(pair, 'x', split_axis=0, concat_axis=0, tiled=True)  11.6 us
    all_to_all x1, blocking collectives, local(): lax.all_to_all(jnp.broadcast_to(gated, (4, 256, HD)), 'x', split_axis=0,...  10.4 us
    all_gather x1, blocking collectives, local(): along_x = lax.all_gather(finished, 'x')  10.2 us
    pallas_call x1, Pallas kernels, ffn(): pl.pallas_call(ffn_kernel, out_shape=(half, half), in_specs=[whole(pltpu....  9.31 us
  transfers between devices with their start and end apart: 9, of which 5 were waited for; matrix products, arithmetic and copies ran while one was open for 5% of the time, Pallas kernels for 2%

profile of v5, /device:TPU:1, one launch (start us, length us, event | category | flops | bytes accessed | tf_op | source)
XLA Modules:
  0.0 201.3 jit_solution(15992545800776799368)
XLA Ops:
  6.5 3.0 %scan.1 = (f32[256,128]{1,0:T(8,128)}, bf16[256,128]{1,0:T(8,128)(2,1)}, bf16[48,1536]{1,0:T(8,128)(2,1)}) custom-call(bf16[256,128]{1,0:T(8,128)(2,1)} %q_ref.1, bf16[256,128]{1,0:T(8,128)(2,1)} %f_ref.1, bf16[256,128]{1,0:T(8,128)(2,1)} %v_ref.1, f32[1,128]{1,0:T(1,128)} %bitcast.52, f32[256,128]{1,0:T(8,128)} %extra_ref.1, bf16[32,704]{1,0:T(8,128)(2,1)} %gate_ref.1, ...), custom_call_target="tpu_custom_call" | custom-call | flops 4000000000 | bytes 500000 | tf_op jit(solution)/shard_map/scan/pallas_call | solution.py:105
  9.6 11.7 %all-gather = bf16[192,1536]{1,0:T(8,128)(2,1)S(1)} all-gather(bf16[48,1536]{1,0:T(8,128)(2,1)} %get-tuple-element.17), channel_id=2, replica_groups=mesh['z'=16,'y'=4,'x'=4,'c'=2] {'y'}, dimensions={0}, use_global_device_ids=true | all-gather | bytes 737280 | tf_op jit(solution)/shard_map/all_gather | solution.py:324
  22.1 1.6 broadcast_in_dim.8
  23.7 5.4 %all-to-all-start = ((bf16[4,128,2048]{2,1,0:T(8,128)(2,1)}), bf16[4,128,2048]{2,1,0:T(8,128)(2,1)S(1)}, u32[]{:S(2)}, u32[]{:S(2)}) async-start(bf16[4,128,2048]{2,1,0:T(8,128)(2,1)} %broadcast_in_dim.8), calls=%async_computation | async-start | bytes 4194304 | tf_op jit(solution)/shard_map/all_to_all | solution.py:327
  29.1 1.8 join.1
  31.9 50.4 %all-gather.7 = f16[1024,640]{1,0:T(8,128)(2,1)S(1)} all-gather(f16[64,640]{1,0:T(8,128)(2,1)S(1)} %convert_element_type.43), channel_id=3, replica_groups=mesh['z'=16,'y'=4,'x'=4,'c'=2] {'z'}, dimensions={0}, use_global_device_ids=true | all-gather | bytes 1392640 | tf_op jit(solution)/shard_map/all_gather | solution.py:329
  83.7 11.1 %collective-permute-start.1 = (bf16[4,128,2048]{2,1,0:T(8,128)(2,1)S(1)}, bf16[4,128,2048]{2,1,0:T(8,128)(2,1)}, u32[]{:S(2)}, u32[]{:S(2)}) collective-permute-start(bf16[4,128,2048]{2,1,0:T(8,128)(2,1)S(1)} %all-to-all-done), channel_id=1, source_target_pairs={{0,1},{1,0},{2,3},{3,2},{4,5},{5,4},{6,7},{7,6},{8,9},{9,8},{10,11... | collective-permute-start | bytes 6291464 | tf_op jit(solution)/shard_map/ppermute | solution.py:26
  94.8 2.4 %mix.1 = bf16[256,128]{1,0:T(8,128)(2,1)} custom-call(s32[1]{0:T(128)} %bitcast.2.z_ref, f32[16,32,640]{2,1,0:T(8,128)} %slice_convert_fusion.lines_ref, f32[136,128]{1,0:T(8,128)} %get-tuple-element.20.here_ref, f32[256,128]{1,0:T(8,128)} %get-tuple-element.21.out_ref, bf16[256,128]{1,0:T(8,128)(2,1)} %get-tuple-element.22.scaled_ref, ...), custom_call_target="tpu_custom_call" | custom-call | flops 2000000000 | bytes 2000000 | tf_op jit(solution)/shard_map/mix/pallas_call | solution.py:179
  98.1 10.4 %all_to_all.15 = bf16[4,256,128]{2,1,0:T(8,128)(2,1)S(1)} all-to-all(bf16[4,256,128]{2,1,0:T(8,128)(2,1)S(1)} %broadcast_in_dim.9), channel_id=1, replica_groups=mesh['z'=16,'y'=4,'x'=4,'c'=2] {'x'}, dimensions={0} | all-to-all | bytes 524288 | tf_op jit(solution)/shard_map/all_to_all | solution.py:347
  108.5 3.0 %collective-permute-start = (bf16[4,256,128]{2,1,0:T(8,128)(2,1)S(1)}, bf16[4,256,128]{2,1,0:T(8,128)(2,1)S(1)}, u32[]{:S(2)}, u32[]{:S(2)}) collective-permute-start(bf16[4,256,128]{2,1,0:T(8,128)(2,1)S(1)} %all_to_all.15), channel_id=1, source_target_pairs={{0,1},{1,0},{2,3},{3,2},{4,5},{5,4},{6,7},{7,6},{8,9},{9,8},{10,11... | collective-permute-start | bytes 786440 | tf_op jit(solution)/shard_map/ppermute | solution.py:26
  111.6 6.0 %collective-permute-start.2 = (bf16[512,640]{1,0:T(8,128)(2,1)S(1)}, bf16[512,640]{1,0:T(8,128)(2,1)}, u32[]{:S(2)}, u32[]{:S(2)}) collective-permute-start(bf16[512,640]{1,0:T(8,128)(2,1)S(1)} %bitcast.42), channel_id=1, source_target_pairs={{0,8},{8,16},{16,24},{24,0},{1,9},{9,17},{17,25},{25,1},{2,10},{10... | collective-permute-start | bytes 1966088 | tf_op jit(solution)/shard_map/ppermute | solution.py:26
  117.6 2.6 %collective-permute-start.3 = (bf16[512,640]{1,0:T(8,128)(2,1)S(1)}, bf16[512,640]{1,0:T(8,128)(2,1)}, u32[]{:S(2)}, u32[]{:S(2)}) collective-permute-start(bf16[512,640]{1,0:T(8,128)(2,1)S(1)} %bitcast.43), channel_id=1, source_target_pairs={{0,24},{8,0},{16,8},{24,16},{1,25},{9,1},{17,9},{25,17},{2,26},{10... | collective-permute-start | bytes 1966088 | tf_op jit(solution)/shard_map/ppermute | solution.py:26
  120.2 3.1 %collective-permute-start.4 = (bf16[512,640]{1,0:T(8,128)(2,1)S(1)}, bf16[512,640]{1,0:T(8,128)(2,1)}, u32[]{:S(2)}, u32[]{:S(2)}) collective-permute-start(bf16[512,640]{1,0:T(8,128)(2,1)S(1)} %bitcast.44), channel_id=1, source_target_pairs={{0,16},{8,24},{16,0},{24,8},{1,17},{9,25},{17,1},{25,9},{2,18},{10... | collective-permute-start | bytes 1966088 | tf_op jit(solution)/shard_map/ppermute | solution.py:26
  124.6 2.5 %fusion.3 = (f32[256]{0:T(256)S(1)}, bf16[256,2048]{1,0:T(8,128)(2,1)S(1)}) fusion(f32[256,2048]{1,0:T(8,128)S(1)} %convolution_bitcast_fusion.1, bf16[4,128,2048]{2,1,0:T(8,128)(2,1)} %collective-permute-done.1, bf16[4,256,128]{2,1,0:T(8,128)(2,1)S(1)} %collective-permute-done, bf16[256,2048]{1,0:T(8,128)(2,1)S(1)} %copy-done.2), kind=kOutput, calls=%fused_computation.7 | convolution fusion | flops 540540672 | bytes 6554624 | tf_op jit(solution)/shard_map/dot_general | solution.py:353
  128.4 5.1 %collective-permute-done.2 = bf16[512,640]{1,0:T(8,128)(2,1)} collective-permute-done((bf16[512,640]{1,0:T(8,128)(2,1)S(1)}, bf16[512,640]{1,0:T(8,128)(2,1)}, u32[]{:S(2)}, u32[]{:S(2)}) %collective-permute-start.2) | collective-permute-done | bytes 655392 | tf_op jit(solution)/shard_map/ppermute | solution.py:26
  133.5 2.1 %collective-permute-done.3 = bf16[512,640]{1,0:T(8,128)(2,1)} collective-permute-done((bf16[512,640]{1,0:T(8,128)(2,1)S(1)}, bf16[512,640]{1,0:T(8,128)(2,1)}, u32[]{:S(2)}, u32[]{:S(2)}) %collective-permute-start.3) | collective-permute-done | bytes 655392 | tf_op jit(solution)/shard_map/ppermute | solution.py:26
  135.6 12.8 %collective-permute-done.4 = bf16[512,640]{1,0:T(8,128)(2,1)} collective-permute-done((bf16[512,640]{1,0:T(8,128)(2,1)S(1)}, bf16[512,640]{1,0:T(8,128)(2,1)}, u32[]{:S(2)}, u32[]{:S(2)}) %collective-permute-start.4) | collective-permute-done | bytes 655392 | tf_op jit(solution)/shard_map/ppermute | solution.py:26
  148.4 9.3 %ffn.1 = (bf16[4,32,2048]{2,1,0:T(8,128)(2,1)}, bf16[4,32,2048]{2,1,0:T(8,128)(2,1)}) custom-call(s32[1]{0:T(128)} %bitcast.y_ref, s32[1]{0:T(128)} %bitcast.1.core_ref, bf16[256,2048]{1,0:T(8,128)(2,1)} %fusion.5.rows_ref, bf16[2048,1536]{1,0:T(8,128)(2,1)} %all-gather.6.cloned.1.call-done.wide_ref, bf16[16,32,640]{2,1,0:T(8,128)(2,1)} %copy-done, ...), custom_call_target="tpu_custom_call" | custom-call | flops 2214592512 | bytes 11534336 | tf_op jit(solution)/shard_map/ffn/pallas_call | solution.py:274
  157.7 2.8 %collective-permute-start.5 = (bf16[4,32,2048]{2,1,0:T(8,128)(2,1)}, bf16[4,32,2048]{2,1,0:T(8,128)(2,1)S(1)}, u32[]{:S(2)}, u32[]{:S(2)}) collective-permute-start(bf16[4,32,2048]{2,1,0:T(8,128)(2,1)} %get-tuple-element.26), channel_id=1, source_target_pairs={{0,1},{1,0},{2,3},{3,2},{4,5},{5,4},{6,7},{7,6},{8,9},{9,8},{10,11... | collective-permute-start | bytes 1572872 | tf_op jit(solution)/shard_map/ppermute | solution.py:26
  160.6 1.7 collective-permute-done.5
  163.4 11.6 %all_to_all.16 = bf16[4,32,2048]{2,1,0:T(8,128)(2,1)S(1)} all-to-all(bf16[4,32,2048]{2,1,0:T(8,128)(2,1)S(1)} %add_convert_fusion), channel_id=1, replica_groups=mesh['z'=16,'y'=4,'x'=4,'c'=2] {'x'}, dimensions={0} | all-to-all | bytes 1048576 | tf_op jit(solution)/shard_map/all_to_all | solution.py:371
  175.1 10.2 %all-gather.2 = bf16[128,2048]{1,0:T(8,128)(2,1)S(1)} all-gather(bf16[32,2048]{1,0:T(8,128)(2,1)S(1)} %add_convert_fusion.1), channel_id=4, replica_groups=mesh['z'=16,'y'=4,'x'=4,'c'=2] {'x'}, dimensions={0}, use_global_device_ids=true | all-gather | bytes 655360 | tf_op jit(solution)/shard_map/all_gather | solution.py:374
  185.4 6.3 %collective-permute-start.6 = (bf16[4,32,2048]{2,1,0:T(8,128)(2,1)S(1)}, bf16[4,32,2048]{2,1,0:T(8,128)(2,1)S(1)}, u32[]{:S(2)}, u32[]{:S(2)}) collective-permute-start(bf16[4,32,2048]{2,1,0:T(8,128)(2,1)S(1)} %bitcast.45), channel_id=1, source_target_pairs={{0,1},{1,0},{2,3},{3,2},{4,5},{5,4},{6,7},{7,6},{8,9},{9,8},{10,11... | collective-permute-start | bytes 1572872 | tf_op jit(solution)/shard_map/ppermute | solution.py:26
  191.7 1.5 collective-permute-done.6
  (31 shorter events, 9.1 us)
Async XLA Ops:
  6.5 141.9 %all-gather.6.cloned.1.call-start = ((), (), s32[]{:S(2)}) async-start(), calls=%async_computation.3 | async-start | bytes 6684672 | tf_op jit(solution)/shard_map/all_gather | solution.py:325
  9.6 12.5 %copy-start.3 = (bf16[128,2048]{1,0:T(8,128)(2,1)S(1)}, bf16[128,2048]{1,0:T(8,128)(2,1)}, u32[]{:S(2)}) copy-start(bf16[128,2048]{1,0:T(8,128)(2,1)} %param.21) | copy-start | bytes 1572868
  21.3 2.5 %copy-start.1 = (bf16[192,1536]{1,0:T(8,128)(2,1)}, bf16[192,1536]{1,0:T(8,128)(2,1)S(1)}, u32[]{:S(2)}) copy-start(bf16[192,1536]{1,0:T(8,128)(2,1)S(1)} %all-gather) | copy-start | bytes 1769476
  23.7 60.0 %all-to-all-start = ((bf16[4,128,2048]{2,1,0:T(8,128)(2,1)}), bf16[4,128,2048]{2,1,0:T(8,128)(2,1)S(1)}, u32[]{:S(2)}, u32[]{:S(2)}) async-start(bf16[4,128,2048]{2,1,0:T(8,128)(2,1)} %broadcast_in_dim.8), calls=%async_computation | async-start | bytes 4194304 | tf_op jit(solution)/shard_map/all_to_all | solution.py:327
  82.4 37.8 %copy-start = (bf16[16,32,640]{2,1,0:T(8,128)(2,1)}, bf16[16,32,640]{2,1,0:T(8,128)(2,1)S(1)}, u32[]{:S(2)}) copy-start(bf16[16,32,640]{2,1,0:T(8,128)(2,1)S(1)} %multiply_convert_fusion) | copy-start | bytes 1966084
  83.7 40.4 %collective-permute-start.1 = (bf16[4,128,2048]{2,1,0:T(8,128)(2,1)S(1)}, bf16[4,128,2048]{2,1,0:T(8,128)(2,1)}, u32[]{:S(2)}, u32[]{:S(2)}) collective-permute-start(bf16[4,128,2048]{2,1,0:T(8,128)(2,1)S(1)} %all-to-all-done), channel_id=1, source_target_pairs={{0,1},{1,0},{2,3},{3,2},{4,5},{5,4},{6,7},{7,6},{8,9},{9,8},{10,11... | collective-permute-start | bytes 6291464 | tf_op jit(solution)/shard_map/ppermute | solution.py:26
  108.5 15.5 %collective-permute-start = (bf16[4,256,128]{2,1,0:T(8,128)(2,1)S(1)}, bf16[4,256,128]{2,1,0:T(8,128)(2,1)S(1)}, u32[]{:S(2)}, u32[]{:S(2)}) collective-permute-start(bf16[4,256,128]{2,1,0:T(8,128)(2,1)S(1)} %all_to_all.15), channel_id=1, source_target_pairs={{0,1},{1,0},{2,3},{3,2},{4,5},{5,4},{6,7},{7,6},{8,9},{9,8},{10,11... | collective-permute-start | bytes 786440 | tf_op jit(solution)/shard_map/ppermute | solution.py:26
  111.6 21.9 %collective-permute-start.2 = (bf16[512,640]{1,0:T(8,128)(2,1)S(1)}, bf16[512,640]{1,0:T(8,128)(2,1)}, u32[]{:S(2)}, u32[]{:S(2)}) collective-permute-start(bf16[512,640]{1,0:T(8,128)(2,1)S(1)} %bitcast.42), channel_id=1, source_target_pairs={{0,8},{8,16},{16,24},{24,0},{1,9},{9,17},{17,25},{25,1},{2,10},{10... | collective-permute-start | bytes 1966088 | tf_op jit(solution)/shard_map/ppermute | solution.py:26
  117.6 18.0 %collective-permute-start.3 = (bf16[512,640]{1,0:T(8,128)(2,1)S(1)}, bf16[512,640]{1,0:T(8,128)(2,1)}, u32[]{:S(2)}, u32[]{:S(2)}) collective-permute-start(bf16[512,640]{1,0:T(8,128)(2,1)S(1)} %bitcast.43), channel_id=1, source_target_pairs={{0,24},{8,0},{16,8},{24,16},{1,25},{9,1},{17,9},{25,17},{2,26},{10... | collective-permute-start | bytes 1966088 | tf_op jit(solution)/shard_map/ppermute | solution.py:26
  120.2 28.2 %collective-permute-start.4 = (bf16[512,640]{1,0:T(8,128)(2,1)S(1)}, bf16[512,640]{1,0:T(8,128)(2,1)}, u32[]{:S(2)}, u32[]{:S(2)}) collective-permute-start(bf16[512,640]{1,0:T(8,128)(2,1)S(1)} %bitcast.44), channel_id=1, source_target_pairs={{0,16},{8,24},{16,0},{24,8},{1,17},{9,25},{17,1},{25,9},{2,18},{10... | collective-permute-start | bytes 1966088 | tf_op jit(solution)/shard_map/ppermute | solution.py:26
  123.3 1.2 copy-start.2
  124.1 3.0 %copy-start.4 = (f32[2048]{0:T(1024)S(1)}, f32[2048]{0:T(1024)}, u32[]{:S(2)}) copy-start(f32[2048]{0:T(1024)} %param.22) | copy-start | bytes 24580
  157.7 4.5 %collective-permute-start.5 = (bf16[4,32,2048]{2,1,0:T(8,128)(2,1)}, bf16[4,32,2048]{2,1,0:T(8,128)(2,1)S(1)}, u32[]{:S(2)}, u32[]{:S(2)}) collective-permute-start(bf16[4,32,2048]{2,1,0:T(8,128)(2,1)} %get-tuple-element.26), channel_id=1, source_target_pairs={{0,1},{1,0},{2,3},{3,2},{4,5},{5,4},{6,7},{7,6},{8,9},{9,8},{10,11... | collective-permute-start | bytes 1572872 | tf_op jit(solution)/shard_map/ppermute | solution.py:26
  185.4 7.8 %collective-permute-start.6 = (bf16[4,32,2048]{2,1,0:T(8,128)(2,1)S(1)}, bf16[4,32,2048]{2,1,0:T(8,128)(2,1)S(1)}, u32[]{:S(2)}, u32[]{:S(2)}) collective-permute-start(bf16[4,32,2048]{2,1,0:T(8,128)(2,1)S(1)} %bitcast.45), channel_id=1, source_target_pairs={{0,1},{1,0},{2,3},{3,2},{4,5},{5,4},{6,7},{7,6},{8,9},{9,8},{10,11... | collective-permute-start | bytes 1572872 | tf_op jit(solution)/shard_map/ppermute | solution.py:26
Sparse Core Ops, SparseCore 0:
  22.2 103.2 all-gather.5

commit v6 on v5

--- a/solution.py
+++ b/solution.py
@@ -170,9 +170,8 @@
     mixed = out_ref[...] + dot(scaled_ref[...], state, NT)
     normed = mixed * lax.rsqrt(jnp.mean(mixed * mixed, axis=-1, keepdims=True) + eps)
     logits = logits_ref[...].astype(jnp.float32)
-    gated_ref[...] = (normed * gain_ref[...] * (logits * jax.nn.sigmoid(logits))).astype(
-        jnp.bfloat16
-    )
+    gated = (normed * gain_ref[...] * (logits * jax.nn.sigmoid(logits))).astype(jnp.bfloat16)
+    gated_ref[...] = gated
 
 
 def mixed_rows(z, lines, here, out, scaled, logits, gain):
@@ -189,64 +188,31 @@
 
 
 def ffn_kernel(
-    y_ref,
     core_ref,
-    rows_ref,
-    wide_ref,
-    own_ref,
-    down1_ref,
-    up1_ref,
-    far_ref,
+    after_ref,
+    gain_ref,
+    bands,
+    pieces_ref,
     mine_ref,
     theirs_ref,
-    bands,
-    half,
-    weights,
+    normed,
     hidden,
-    band_sems,
-    piece_sems,
 ):
-    y, core = y_ref[0], core_ref[0]
-    places = [lax.rem(y + k, 4) for k in range(4)]
-    band_copies = [
-        pltpu.make_async_copy(
-            wide_ref.at[pl.ds(n * 1024, 1024)], bands.at[pl.ds(n * 1024, 1024)], band_sems.at[n]
-        )
-        for n in range(2)
-    ]
-    piece_copies = [
-        pltpu.make_async_copy(ref, weights.at[:, places[k]], piece_sems.at[n])
-        for n, (ref, k) in enumerate(
-            (
-                (own_ref, 0),
-                (up1_ref, 1),
-                (far_ref, 2),
-                (down1_ref, 3),
-            )
-        )
-    ]
-    for copy in band_copies:
-        copy.start()
-    for copy in piece_copies:
-        copy.start()
+    core = core_ref[0]
+    for k in range(8):
+        lines = slice(k * 32, (k + 1) * 32)
+        after = after_ref[lines].astype(jnp.float32)
+        scale = lax.rsqrt(jnp.mean(after * after, axis=-1, keepdims=True) + eps)
+        normed[lines] = (after * scale * gain_ref[...]).astype(jnp.bfloat16)
     spans = [slice(n * 256, min(n * 256 + 256, 1408)) for n in range(6)]
-    rows = rows_ref[:, :1024]
-    band_copies[0].wait()
-    for span in spans:
-        half[:, span] = jnp.dot(rows, bands[:1024, span], preferred_element_type=jnp.float32)
-    rows = rows_ref[:, 1024:]
-    band_copies[1].wait()
+    rows = normed[...]
     for n, span in enumerate(spans):
-        both = half[:, span] + jnp.dot(
-            rows, bands[1024:, span], preferred_element_type=jnp.float32
-        )
+        both = jnp.dot(rows, bands[:, span], preferred_element_type=jnp.float32)
         width = both.shape[1] // 2
         gate, up = both[:, :width], both[:, width:]
         hidden[:, n * 128 : n * 128 + width] = (gate * jax.nn.sigmoid(gate) * up).astype(
             jnp.bfloat16
         )
-    for copy in piece_copies:
-        copy.wait()
     first, second = hidden[:, :640], hidden[:, 640:704]
 
     @pl.loop(0, 8)
@@ -254,7 +220,9 @@
         at = pl.multiple_of(n * 256, 256)
         part = lax.dot_general(
             first,
-            weights[pl.ds(n * 2, 2)].reshape(256, 640),
+            jnp.concatenate(
+                [pieces_ref[k, n * 2 + j] for j in range(2) for k in range(4)], axis=0
+            ),
             NT,
             preferred_element_type=jnp.float32,
         ) + lax.dot_general(
@@ -268,28 +236,23 @@
         theirs_ref[:, :, pl.ds(at, 256)] = jnp.where(core == 0, part[:, 1], part[:, 0])
 
 
-def ffn(y, core, rows, wide, *pieces):
-    pieces = [piece.reshape(16, 32, 640) for piece in pieces]
+def ffn(core, after, gain, wide, pieces):
     half = jax.ShapeDtypeStruct((4, 32, 2048), jnp.bfloat16)
     return pl.pallas_call(
         ffn_kernel,
         out_shape=(half, half),
-        in_specs=[whole(pltpu.SMEM)] * 2 + [whole()] + [whole(pltpu.HBM)] * 5,
+        in_specs=[whole(pltpu.SMEM), whole(), whole(), whole(), whole()],
         out_specs=(whole(), whole()),
         scratch_shapes=[
-            pltpu.VMEM((2048, 1536), jnp.bfloat16),
-            pltpu.VMEM((256, 1408), jnp.float32),
-            pltpu.VMEM((16, 4, 32, 640), jnp.bfloat16),
+            pltpu.VMEM((256, 2048), jnp.bfloat16),
             pltpu.VMEM((256, 768), jnp.bfloat16),
-            pltpu.SemaphoreType.DMA((2,)),
-            pltpu.SemaphoreType.DMA((4,)),
         ],
-        compiler_params=pltpu.CompilerParams(vmem_limit_bytes=60 * 2**20),
+        compiler_params=pltpu.CompilerParams(vmem_limit_bytes=40 * 2**20),
         cost_estimate=pl.CostEstimate(
             flops=2 * 256 * 2048 * 2112, bytes_accessed=11 * 2**20, transcendentals=256 * 704
         ),
         name="ffn",
-    )(y, core, rows, wide, *pieces)
+    )(core, after, gain, wide, pieces)
 
 
 def local(
@@ -328,12 +291,10 @@
     total, here = joined_over_y(y, along_y, turned)
     along_z = lax.all_gather(total.astype(jnp.float16), "z")
     own = (along_z[:, :32].astype(jnp.float32) * (1.0 / SCALE)).astype(jnp.bfloat16)
-    own = own.reshape(512, 640)
-    down1 = shifted(own, "y", 1)
-    up1 = shifted(own, "y", -1)
-    far = shifted(own, "y", 2)
+    own = jnp.broadcast_to(own, (4, 16, 32, 640))
+    pieces = lax.all_to_all(own, "y", split_axis=0, concat_axis=0, tiled=True)
     lines = along_z[:, 32:].astype(jnp.float32)
-    lines, out_mine, own = lax.optimization_barrier((lines, out_mine, own))
+    lines, out_mine = lax.optimization_barrier((lines, out_mine))
     out_other = shifted(out_mine, "c", 1)
     gated = mixed_rows(
         z,
@@ -344,9 +305,7 @@
         output_gate_logits,
         per_head_norm_gain.reshape(1, HD),
     )
-    heads = lax.all_to_all(
-        jnp.broadcast_to(gated, (4, 256, HD)), "x", split_axis=0, concat_axis=0, tiled=True
-    )
+    heads = lax.all_gather(gated, "x")
     heads_other = shifted(heads, "c", 1)
     projected = 0.0
     for part, weight in ((heads, out_mine), (heads_other, out_other)):
@@ -356,13 +315,8 @@
             preferred_element_type=jnp.float32,
         )
     after_mixer = (residual.astype(jnp.float32) + projected).astype(jnp.bfloat16)
-    widened = after_mixer.astype(jnp.float32)
-    normed = (
-        widened
-        * lax.rsqrt(jnp.mean(widened * widened, axis=-1, keepdims=True) + eps)
-        * feedforward_norm_gain
-    ).astype(jnp.bfloat16)
-    mine, theirs = ffn(y, core.reshape(1), normed, wide, own, down1, up1, far)
+    gain = feedforward_norm_gain.reshape(1, 2048)
+    mine, theirs = ffn(core.reshape(1), after_mixer, gain, wide, pieces)
     swapped = shifted(theirs, "c", 1)
     pair = (mine.astype(jnp.float32) + swapped.astype(jnp.float32)).astype(jnp.bfloat16)
     place = lax.axis_index(TP) * 32

time: 203 us -> 189 us (0.931)
  waiting for transfers between devices: 23.2 us -> 10.1 us
  starting transfers between devices: 40.3 us -> 31.6 us
  blocking collectives: 94.3 us -> 102 us
  local copies, waits for them, and re-layouts: 4.87 us -> 10.2 us
  Pallas kernels: 16.6 us -> 12.8 us
  matrix products: 3.23 us -> 5.73 us
  other arithmetic: 5.1 us -> 2.64 us
    ppermute x7 -> x4, waiting for transfers between devices: 23.2 us -> 2.31 us  [shifted(): lax.ppermute(value, axis, [(k, (k + step) % size) for k in range(size)])]
    ppermute x7 -> x4, starting transfers between devices: 34.9 us -> 22.5 us  [shifted(): lax.ppermute(value, axis, [(k, (k + step) % size) for k in range(size)])]
    all_gather x0 -> x1, blocking collectives: none -> 12.1 us  [local(): heads = lax.all_gather(gated, 'x')]
    all_to_all x1 -> x0, blocking collectives: 10.4 us -> none  [local(): lax.all_to_all(jnp.broadcast_to(gated, (4, 256, HD)), 'x', split_axis=0,...]
    all_to_all x0 -> x1, waiting for transfers between devices: none -> 7.75 us  [local(): pieces = lax.all_to_all(own, 'y', split_axis=0, concat_axis=0, tiled=True)]
    pallas_call x1, Pallas kernels: 9.31 us -> 5.55 us  [ffn(): pl.pallas_call(ffn_kernel, out_shape=(half, half), in_specs=[whole(pltpu....]
    all_to_all x0 -> x1, starting transfers between devices: none -> 3.65 us  [local(): pieces = lax.all_to_all(own, 'y', split_axis=0, concat_axis=0, tiled=True)]
    unnamed x10 -> x12, local copies, waits for them, and re-layouts: 0.49 us -> 4.03 us
  transfers between devices with their start and end apart: 9 -> 7, of which waited for: 5 -> 3; matrix products, arithmetic and copies ran while one was open for 5% -> 7% of each run, Pallas kernels for 2% -> 2%
where the time goes in v6:
time: 189 us
  blocking collectives  102 us (54%)
  starting transfers between devices  31.6 us (17%)
  between operations  13.6 us (7%)
  Pallas kernels  12.8 us (7%)
  local copies, waits for them, and re-layouts  10.2 us (5%)
  waiting for transfers between devices  10.1 us (5%)
  matrix products  5.73 us (3%)
  other arithmetic  2.64 us (1%)
    all_gather x1, blocking collectives, local(): along_z = lax.all_gather(total.astype(jnp.float16), 'z')  53.5 us
    ppermute x4, starting transfers between devices, shifted(): lax.ppermute(value, axis, [(k, (k + step) % size) for k in range(size)])  22.5 us
    all_to_all x1, blocking collectives, local(): arrived = lax.all_to_all(pair, 'x', split_axis=0, concat_axis=0, tiled=True)  13.5 us
    all_gather x1, blocking collectives, local(): heads = lax.all_gather(gated, 'x')  12.1 us
    all_gather x1, blocking collectives, local(): along_y = lax.all_gather(packed, 'y')  11.7 us
    all_gather x1, blocking collectives, local(): along_x = lax.all_gather(finished, 'x')  11.1 us
    all_to_all x1, waiting for transfers between devices, local(): pieces = lax.all_to_all(own, 'y', split_axis=0, concat_axis=0, tiled=True)  7.75 us
    dot_general x2, matrix products, local(): jnp.dot(part.transpose(1, 0, 2).reshape(256, 512), weight.reshape(512, 20...  5.73 us
  transfers between devices with their start and end apart: 7, of which 3 were waited for; matrix products, arithmetic and copies ran while one was open for 7% of the time, Pallas kernels for 2%

profile of v6, /device:TPU:1, one launch (start us, length us, event | category | flops | bytes accessed | tf_op | source)
XLA Modules:
  0.0 188.6 jit_solution(2811194683305606242)
XLA Ops:
  6.5 3.0 %scan.1 = (f32[256,128]{1,0:T(8,128)}, bf16[256,128]{1,0:T(8,128)(2,1)}, bf16[48,1536]{1,0:T(8,128)(2,1)}) custom-call(bf16[256,128]{1,0:T(8,128)(2,1)} %q_ref.1, bf16[256,128]{1,0:T(8,128)(2,1)} %f_ref.1, bf16[256,128]{1,0:T(8,128)(2,1)} %v_ref.1, f32[1,128]{1,0:T(1,128)} %bitcast.47, f32[256,128]{1,0:T(8,128)} %extra_ref.1, bf16[32,704]{1,0:T(8,128)(2,1)} %gate_ref.1, ...), custom_call_target="tpu_custom_call" | custom-call | flops 4000000000 | bytes 500000 | tf_op jit(solution)/shard_map/scan/pallas_call | solution.py:105
  9.6 11.7 %all-gather = bf16[192,1536]{1,0:T(8,128)(2,1)S(1)} all-gather(bf16[48,1536]{1,0:T(8,128)(2,1)} %get-tuple-element.16), channel_id=2, replica_groups=mesh['z'=16,'y'=4,'x'=4,'c'=2] {'y'}, dimensions={0}, use_global_device_ids=true | all-gather | bytes 737280 | tf_op jit(solution)/shard_map/all_gather | solution.py:287
  22.1 1.6 broadcast_in_dim.6
  23.8 5.4 %all-to-all-start = ((bf16[4,128,2048]{2,1,0:T(8,128)(2,1)}), bf16[4,128,2048]{2,1,0:T(8,128)(2,1)}, u32[]{:S(2)}, u32[]{:S(2)}) async-start(bf16[4,128,2048]{2,1,0:T(8,128)(2,1)} %broadcast_in_dim.6), calls=%async_computation | async-start | bytes 4194304 | tf_op jit(solution)/shard_map/all_to_all | solution.py:290
  29.2 1.8 join.1
  31.9 53.5 %all-gather.8 = f16[1024,640]{1,0:T(8,128)(2,1)S(1)} all-gather(f16[64,640]{1,0:T(8,128)(2,1)S(1)} %convert_element_type.37), channel_id=3, replica_groups=mesh['z'=16,'y'=4,'x'=4,'c'=2] {'z'}, dimensions={0}, use_global_device_ids=true | all-gather | bytes 1392640 | tf_op jit(solution)/shard_map/all_gather | solution.py:292
  85.4 1.2 slice_convert_fusion.lines_ref
  86.5 10.1 %collective-permute-start.1 = (bf16[4,128,2048]{2,1,0:T(8,128)(2,1)}, bf16[4,128,2048]{2,1,0:T(8,128)(2,1)}, u32[]{:S(2)}, u32[]{:S(2)}) collective-permute-start(bf16[4,128,2048]{2,1,0:T(8,128)(2,1)} %all-to-all-done), channel_id=1, source_target_pairs={{0,1},{1,0},{2,3},{3,2},{4,5},{5,4},{6,7},{7,6},{8,9},{9,8},{10,11... | collective-permute-start | bytes 6291464 | tf_op jit(solution)/shard_map/ppermute | solution.py:26
  96.8 1.8 broadcast_in_dim.7
  98.6 3.7 %all-to-all-start.1 = ((bf16[4,16,32,640]{3,2,1,0:T(8,128)(2,1)}), bf16[4,16,32,640]{3,2,1,0:T(8,128)(2,1)S(1)}, u32[]{:S(2)}, u32[]{:S(2)}) async-start(bf16[4,16,32,640]{3,2,1,0:T(8,128)(2,1)} %broadcast_in_dim.7), calls=%async_computation.1 | async-start | bytes 5242880 | tf_op jit(solution)/shard_map/all_to_all | solution.py:295
  102.2 2.4 %mix.1 = bf16[256,128]{1,0:T(8,128)(2,1)} custom-call(s32[1]{0:T(128)} %bitcast.1.z_ref, f32[16,32,640]{2,1,0:T(8,128)} %slice_convert_fusion.lines_ref, f32[136,128]{1,0:T(8,128)} %get-tuple-element.19.here_ref, f32[256,128]{1,0:T(8,128)} %get-tuple-element.20.out_ref, bf16[256,128]{1,0:T(8,128)(2,1)} %get-tuple-element.21.scaled_ref, ...), custom_call_target="tpu_custom_call" | custom-call | flops 2000000000 | bytes 2000000 | tf_op jit(solution)/shard_map/mix/pallas_call | solution.py:178
  104.6 12.1 %all-gather.2 = bf16[1024,128]{1,0:T(8,128)(2,1)S(1)} all-gather(bf16[256,128]{1,0:T(8,128)(2,1)} %mix.1), channel_id=4, replica_groups=mesh['z'=16,'y'=4,'x'=4,'c'=2] {'x'}, dimensions={0}, use_global_device_ids=true | all-gather | bytes 327680 | tf_op jit(solution)/shard_map/all_gather | solution.py:308
  116.8 3.9 %collective-permute-start = (bf16[4,256,128]{2,1,0:T(8,128)(2,1)S(1)}, bf16[4,256,128]{2,1,0:T(8,128)(2,1)S(1)}, u32[]{:S(2)}, u32[]{:S(2)}) collective-permute-start(bf16[4,256,128]{2,1,0:T(8,128)(2,1)S(1)} %bitcast.43), channel_id=1, source_target_pairs={{0,1},{1,0},{2,3},{3,2},{4,5},{5,4},{6,7},{7,6},{8,9},{9,8},{10,11... | collective-permute-start | bytes 786440 | tf_op jit(solution)/shard_map/ppermute | solution.py:26
  120.7 2.4 %convolution_bitcast_fusion.1 = f32[256,2048]{1,0:T(8,128)S(1)} fusion(bf16[256,4,128]{2,0,1:T(8,128)(2,1)S(1)} %bitcast.44, bf16[4,128,2048]{2,1,0:T(8,128)(2,1)} %all-to-all-done), kind=kOutput, calls=%fused_computation.1 | convolution fusion | flops 536870912 | bytes 4456448 | tf_op jit(solution)/shard_map/dot_general | solution.py:312
  123.1 3.3 %fusion.2.after_ref = bf16[256,2048]{1,0:T(8,128)(2,1)} fusion(f32[256,2048]{1,0:T(8,128)S(1)} %convolution_bitcast_fusion.1, bf16[4,128,2048]{2,1,0:T(8,128)(2,1)} %collective-permute-done.1, bf16[256,2048]{1,0:T(8,128)(2,1)S(1)} %copy-done.4, bf16[4,256,128]{2,1,0:T(8,128)(2,1)S(1)} %collective-permute-done), kind=kOutput, calls=%fused_computation.4 | convolution fusion | flops 538968064 | bytes 6553600 | tf_op jit(solution)/shard_map/dot_general | solution.py:312
  126.5 7.8 %all-to-all-done.1.pieces_ref = bf16[4,16,32,640]{3,2,1,0:T(8,128)(2,1)S(1)} async-done(((bf16[4,16,32,640]{3,2,1,0:T(8,128)(2,1)}), bf16[4,16,32,640]{3,2,1,0:T(8,128)(2,1)S(1)}, u32[]{:S(2)}, u32[]{:S(2)}) %all-to-all-start.1) | async-done | bytes 2621472 | tf_op jit(solution)/shard_map/all_to_all | solution.py:295
  134.2 2.8 %copy-done = bf16[2048,1536]{1,0:T(8,128)(2,1)S(1)} copy-done((bf16[2048,1536]{1,0:T(8,128)(2,1)S(1)}, bf16[2048,1536]{1,0:T(8,128)(2,1)}, u32[]{:S(2)}) %copy-start) | copy-done | bytes 6291480
  137.0 1.2 copy-done.1
  138.2 5.5 %ffn.1 = (bf16[4,32,2048]{2,1,0:T(8,128)(2,1)S(1)}, bf16[4,32,2048]{2,1,0:T(8,128)(2,1)}) custom-call(s32[1]{0:T(128)} %bitcast.core_ref, bf16[256,2048]{1,0:T(8,128)(2,1)S(1)} %copy-done.1, f32[1,2048]{1,0:T(1,128)S(1)} %bitcast.35, bf16[2048,1536]{1,0:T(8,128)(2,1)S(1)} %copy-done, bf16[4,16,32,640]{3,2,1,0:T(8,128)(2,1)S(1)} %all-to-all-done.1.pieces_ref), custom_call_target="tpu_custom_call" | custom-call | flops 2214592512 | bytes 11534336 | tf_op jit(solution)/shard_map/ffn/pallas_call | solution.py:241
  143.8 2.8 %collective-permute-start.2 = (bf16[4,32,2048]{2,1,0:T(8,128)(2,1)}, bf16[4,32,2048]{2,1,0:T(8,128)(2,1)S(1)}, u32[]{:S(2)}, u32[]{:S(2)}) collective-permute-start(bf16[4,32,2048]{2,1,0:T(8,128)(2,1)} %get-tuple-element.24), channel_id=1, source_target_pairs={{0,1},{1,0},{2,3},{3,2},{4,5},{5,4},{6,7},{7,6},{8,9},{9,8},{10,11... | collective-permute-start | bytes 1572872 | tf_op jit(solution)/shard_map/ppermute | solution.py:26
  148.4 13.5 %all_to_all.15 = bf16[4,32,2048]{2,1,0:T(8,128)(2,1)S(1)} all-to-all(bf16[4,32,2048]{2,1,0:T(8,128)(2,1)S(1)} %add_convert_fusion), channel_id=1, replica_groups=mesh['z'=16,'y'=4,'x'=4,'c'=2] {'x'}, dimensions={0} | all-to-all | bytes 1048576 | tf_op jit(solution)/shard_map/all_to_all | solution.py:325
  162.0 11.1 %all-gather.3 = bf16[128,2048]{1,0:T(8,128)(2,1)S(1)} all-gather(bf16[32,2048]{1,0:T(8,128)(2,1)S(1)} %add_convert_fusion.1), channel_id=5, replica_groups=mesh['z'=16,'y'=4,'x'=4,'c'=2] {'x'}, dimensions={0}, use_global_device_ids=true | all-gather | bytes 655360 | tf_op jit(solution)/shard_map/all_gather | solution.py:328
  173.1 5.8 %collective-permute-start.3 = (bf16[4,32,2048]{2,1,0:T(8,128)(2,1)S(1)}, bf16[4,32,2048]{2,1,0:T(8,128)(2,1)S(1)}, u32[]{:S(2)}, u32[]{:S(2)}) collective-permute-start(bf16[4,32,2048]{2,1,0:T(8,128)(2,1)S(1)} %bitcast.38), channel_id=1, source_target_pairs={{0,1},{1,0},{2,3},{3,2},{4,5},{5,4},{6,7},{7,6},{8,9},{9,8},{10,11... | collective-permute-start | bytes 1572872 | tf_op jit(solution)/shard_map/ppermute | solution.py:26
  179.0 1.5 collective-permute-done.3
  (27 shorter events, 5.1 us)
Async XLA Ops:
  6.5 127.7 %all-gather.7.cloned.1.call-start = ((), (), s32[]{:S(2)}) async-start(), calls=%async_computation.3 | async-start | bytes 6684672 | tf_op jit(solution)/shard_map/all_gather | solution.py:288
  9.6 12.6 %copy-start.5 = (bf16[128,2048]{1,0:T(8,128)(2,1)S(1)}, bf16[128,2048]{1,0:T(8,128)(2,1)}, u32[]{:S(2)}) copy-start(bf16[128,2048]{1,0:T(8,128)(2,1)} %param.21) | copy-start | bytes 1572868
  21.3 2.5 %copy-start.3 = (bf16[192,1536]{1,0:T(8,128)(2,1)}, bf16[192,1536]{1,0:T(8,128)(2,1)S(1)}, u32[]{:S(2)}) copy-start(bf16[192,1536]{1,0:T(8,128)(2,1)S(1)} %all-gather) | copy-start | bytes 1769476
  23.8 62.8 %all-to-all-start = ((bf16[4,128,2048]{2,1,0:T(8,128)(2,1)}), bf16[4,128,2048]{2,1,0:T(8,128)(2,1)}, u32[]{:S(2)}, u32[]{:S(2)}) async-start(bf16[4,128,2048]{2,1,0:T(8,128)(2,1)} %broadcast_in_dim.6), calls=%async_computation | async-start | bytes 4194304 | tf_op jit(solution)/shard_map/all_to_all | solution.py:290
  86.5 36.6 %collective-permute-start.1 = (bf16[4,128,2048]{2,1,0:T(8,128)(2,1)}, bf16[4,128,2048]{2,1,0:T(8,128)(2,1)}, u32[]{:S(2)}, u32[]{:S(2)}) collective-permute-start(bf16[4,128,2048]{2,1,0:T(8,128)(2,1)} %all-to-all-done), channel_id=1, source_target_pairs={{0,1},{1,0},{2,3},{3,2},{4,5},{5,4},{6,7},{7,6},{8,9},{9,8},{10,11... | collective-permute-start | bytes 6291464 | tf_op jit(solution)/shard_map/ppermute | solution.py:26
  98.6 35.6 %all-to-all-start.1 = ((bf16[4,16,32,640]{3,2,1,0:T(8,128)(2,1)}), bf16[4,16,32,640]{3,2,1,0:T(8,128)(2,1)S(1)}, u32[]{:S(2)}, u32[]{:S(2)}) async-start(bf16[4,16,32,640]{3,2,1,0:T(8,128)(2,1)} %broadcast_in_dim.7), calls=%async_computation.1 | async-start | bytes 5242880 | tf_op jit(solution)/shard_map/all_to_all | solution.py:295
  116.8 6.3 %collective-permute-start = (bf16[4,256,128]{2,1,0:T(8,128)(2,1)S(1)}, bf16[4,256,128]{2,1,0:T(8,128)(2,1)S(1)}, u32[]{:S(2)}, u32[]{:S(2)}) collective-permute-start(bf16[4,256,128]{2,1,0:T(8,128)(2,1)S(1)} %bitcast.43), channel_id=1, source_target_pairs={{0,1},{1,0},{2,3},{3,2},{4,5},{5,4},{6,7},{7,6},{8,9},{9,8},{10,11... | collective-permute-start | bytes 786440 | tf_op jit(solution)/shard_map/ppermute | solution.py:26
  120.7 2.4 %copy-start.4 = (bf16[256,2048]{1,0:T(8,128)(2,1)S(1)}, bf16[256,2048]{1,0:T(8,128)(2,1)}, u32[]{:S(2)}) copy-start(bf16[256,2048]{1,0:T(8,128)(2,1)} %param.13) | copy-start | bytes 3145732
  123.1 11.1 %copy-start.2 = (f32[2048]{0:T(1024)S(1)}, f32[2048]{0:T(1024)}, u32[]{:S(2)}) copy-start(f32[2048]{0:T(1024)} %param.22) | copy-start | bytes 24580
  134.2 2.8 %copy-start = (bf16[2048,1536]{1,0:T(8,128)(2,1)S(1)}, bf16[2048,1536]{1,0:T(8,128)(2,1)}, u32[]{:S(2)}) copy-start(bf16[2048,1536]{1,0:T(8,128)(2,1)} %all-gather.7.cloned.1.call-done.bands) | copy-start | bytes 18874372
  137.0 1.2 copy-start.1
  143.8 4.5 %collective-permute-start.2 = (bf16[4,32,2048]{2,1,0:T(8,128)(2,1)}, bf16[4,32,2048]{2,1,0:T(8,128)(2,1)S(1)}, u32[]{:S(2)}, u32[]{:S(2)}) collective-permute-start(bf16[4,32,2048]{2,1,0:T(8,128)(2,1)} %get-tuple-element.24), channel_id=1, source_target_pairs={{0,1},{1,0},{2,3},{3,2},{4,5},{5,4},{6,7},{7,6},{8,9},{9,8},{10,11... | collective-permute-start | bytes 1572872 | tf_op jit(solution)/shard_map/ppermute | solution.py:26
  173.1 7.3 %collective-permute-start.3 = (bf16[4,32,2048]{2,1,0:T(8,128)(2,1)S(1)}, bf16[4,32,2048]{2,1,0:T(8,128)(2,1)S(1)}, u32[]{:S(2)}, u32[]{:S(2)}) collective-permute-start(bf16[4,32,2048]{2,1,0:T(8,128)(2,1)S(1)} %bitcast.38), channel_id=1, source_target_pairs={{0,1},{1,0},{2,3},{3,2},{4,5},{5,4},{6,7},{7,6},{8,9},{9,8},{10,11... | collective-permute-start | bytes 1572872 | tf_op jit(solution)/shard_map/ppermute | solution.py:26
Sparse Core Ops, SparseCore 0:
  22.2 102.6 all-gather.6
